TPU v7x, 128 devices: a whole 4x4x4 slice. The times are simulated.
128 devices in a mesh: gr: 2 (over z_hi), fs: 32 (over z_lo, y, x), tp: 2 (over core).
Axes of the slice: x: 4, y: 4, z: 4 (z_hi: 2, z_lo: 2; z = z_hi * 2 + z_lo), core: 2. Of those that a mesh axis runs over, the one named last changes fastest.
Arguments:
- tokens: bfloat16 [4, 2048, 2048], P(('gr', 'tp')), may hold values from -6 to 6
- gate_master: float32 [3, 2048, 7168], P(None, 'fs', ('gr', 'tp')), may hold values from -0.125 to 0.125
- up_master: float32 [3, 2048, 7168], P(None, 'fs', ('gr', 'tp')), may hold values from -0.125 to 0.125
- down_master: float32 [3, 7168, 2048], P(None, 'fs', ('gr', 'tp')), may hold values from -0.0625 to 0.0625
- norm_gain: float32 [2048], P('fs'), may hold values from 0.1 to 1.9
- route: int32 [4, 2048, 2], P(('gr', 'tp')), may hold values from 0 to 2, all different within a row
- route_weight: float32 [4, 2048, 2], P(('gr', 'tp')), may hold values from 0.05 to 1
Outputs:
- gate_out: bfloat16 [3, 2048, 7168], P(None, None, 'fs')
- up_out: bfloat16 [3, 2048, 7168], P(None, None, 'fs')
- down_out: bfloat16 [3, 7168, 2048], P(None, 'fs')
- mixed: bfloat16 [4, 2048, 2048], P(('gr', 'tp'), 'fs')
Inputs may be any that keep to these rules, and one draw needn't show every extreme that they name: `route`: each token names two different experts; every expert is named by some token.
All inputs are finite; a program needn't handle non-finite values.
Results may differ from a plain program's by a relative error of at most 0.024.
Values may be sent and summed in bfloat16 or wider, within the bound.
No kernel may reach another device: no remote copies, remote signals or barrier semaphores. Data moves between devices by JAX's collectives and lax.ppermute only.
A program may use at most 192 MiB of HBM per device.

v0:
```python
import jax
import jax.numpy as jnp
from jax import lax
from jax.experimental import pallas as pl
from jax.experimental.pallas import tpu as pltpu
from jax.sharding import Mesh
from jax.sharding import PartitionSpec as P

FS = ("fs_0", "fs_1", "fs_2")
PLANE = ("fs_1", "fs_2")
Z = ("gr", "fs_0")
UNITS = 256
MIB = 1024 * 1024


COLORS = (
    (((1, 1), (1, 3), (2, 1), (2, 3)), 512),
    (((2, 1), (2, 3), (1, 1), (1, 3)), 384),
    (((1, 3), (1, 1), (2, 3), (2, 1)), 384),
    (((2, 3), (2, 1), (1, 3), (1, 1)), 384),
    (((0, 1), (1, 1), (1, 3), (2, 3), (2, 1)), 384),
)
CALLS = ((0, 1), (2, 3, 4))


def call(kernel, grid, ins, outs, out_shape, args, flops, nbytes, scratch=(), vmem=60):
    return pl.pallas_call(
        kernel,
        out_shape=out_shape,
        grid_spec=pltpu.PrefetchScalarGridSpec(
            num_scalar_prefetch=1,
            grid=grid,
            in_specs=ins,
            out_specs=outs,
            scratch_shapes=list(scratch),
        ),
        compiler_params=pltpu.CompilerParams(vmem_limit_bytes=vmem * MIB),
        cost_estimate=pl.CostEstimate(
            flops=int(flops), bytes_accessed=int(nbytes), transcendentals=0
        ),
    )(*args)


def whole(shape):
    return pl.BlockSpec(shape, lambda *_: (0,) * len(shape))


def shaped(*shape, dtype=jnp.bfloat16):
    return jax.ShapeDtypeStruct(shape, dtype)


def pack_kernel(where_ref, gate_ref, up_ref, gain_ref, own_ref, send_ref):
    rows = jnp.concatenate([gate_ref[0], up_ref[0]], axis=0)
    gain = jnp.concatenate([gain_ref[...], gain_ref[...]], axis=1)
    cols = (rows.T * gain).astype(jnp.bfloat16)
    dests, _, half, lanes = own_ref.shape
    cols = cols.reshape(dests, 2, half, lanes)
    low, high = cols[:, 0], cols[:, 1]
    first = where_ref[1] == 0
    own_ref[:, 0] = jnp.where(first, low, high)
    send_ref[:, 0] = jnp.where(first, high, low)


def pack(where, gate, up, gain, dests):
    experts, depth, width = gate.shape
    half = width // dests // 2
    block = pl.BlockSpec((1, depth, width), lambda e, w: (e, 0, 0))
    out = pl.BlockSpec((dests, 1, half, 2 * depth), lambda e, w: (0, e, 0, 0))
    return call(
        pack_kernel, (experts,), [block, block, whole((1, depth))], [out] * 2,
        [shaped(dests, experts, half, 2 * depth)] * 2, (where, gate, up, gain), 3e9, 6e6,
    )


def unpack_kernel(where_ref, own_ref, down_ref, up_ref, far_ref, out_ref):
    z = where_ref[0]
    sources, half, lanes = own_ref.shape
    left = lax.broadcasted_iota(jnp.int32, (half, lanes), 1) < lanes // 2
    pick = ((own_ref, down_ref, far_ref, up_ref), (down_ref, far_ref, up_ref, own_ref))
    for plane in range(4):

        @pl.when(z == plane)
        def _():
            for part in range(2):
                ref = pick[part][plane]
                for pair in range(sources // 2):
                    one = ref[2 * pair].astype(jnp.float32)
                    other = ref[2 * pair + 1].astype(jnp.float32)
                    crossed = pltpu.roll(jnp.where(left, other, one), lanes // 2, 1)
                    start = part * sources * (lanes // 2) + pair * lanes
                    at = slice(start, start + lanes)
                    out_ref[0, :, at] = jnp.where(left, one, crossed).astype(jnp.bfloat16)
                    out_ref[1, :, at] = jnp.where(left, crossed, other).astype(jnp.bfloat16)


def unpack(where, pieces):
    sources, half, lanes = pieces[0].shape
    shape = (2, half, sources * lanes)
    return call(
        unpack_kernel, (1,), [whole(pieces[0].shape)] * 4, whole(shape),
        shaped(*shape), (where, *pieces), 1e9, 3e6,
    )


def assemble_kernel(where_ref, *refs):
    gate_ref, up_ref = refs[-2:]
    tp = where_ref[1]
    half = refs[0].shape[1]
    for index, ref in enumerate(refs[:-2]):
        side = tp if index % 2 == 0 else 1 - tp
        rows = pl.ds(pl.multiple_of(side * half, 16), half)
        gate_ref[index // 2, rows, :] = ref[0]
        up_ref[index // 2, rows, :] = ref[1]


def assemble(where, sides):
    _, half, width = sides[0].shape
    shape = (len(sides) // 2, 2 * half, width)
    return call(
        assemble_kernel, (1,), [whole(sides[0].shape)] * len(sides),
        [whole(shape)] * 2, [shaped(*shape)] * 2, (where, *sides), 4e9, 11e6,
    )


def join_kernel(where_ref, *refs):
    out_ref, padded_ref = refs[-2:]
    tp, gr = where_ref[1], where_ref[2]
    depth, width = refs[0].shape[1:]
    places = (gr * 2 + tp, (1 - gr) * 2 + tp, gr * 2 + 1 - tp, (1 - gr) * 2 + 1 - tp)
    for ref, place in zip(refs[:-2], places):
        at = pl.ds(pl.multiple_of(place * width, width), width)
        out_ref[0, :, at] = ref[0]
        padded_ref[0, :depth, at] = ref[0]
    rest = padded_ref.shape[1] - depth
    padded_ref[0, depth:, :] = jnp.zeros((rest, padded_ref.shape[2]), jnp.bfloat16)


def join(where, quarters):
    experts, depth, width = quarters[0].shape
    at = lambda e, w: (e, 0, 0)
    return call(
        join_kernel, (experts,), [pl.BlockSpec((1, depth, width), at)] * 4,
        [pl.BlockSpec((1, depth, 4 * width), at), pl.BlockSpec((1, UNITS, 4 * width), at)],
        [shaped(experts, depth, 4 * width), shaped(experts, UNITS, 4 * width)],
        (where, *quarters), 2e9, 8e6,
    )


def norm_kernel(where_ref, tokens_ref, mix_ref, out_ref, mix_out_ref):
    z, x = where_ref[0] % 2, where_ref[4]
    rows = tokens_ref.shape[3]
    for place in range(8):
        zz, xx = z ^ (place % 2), x ^ (place // 2)
        values = tokens_ref[zz, 0, xx].astype(jnp.float32)
        scale = lax.rsqrt(jnp.mean(values * values, axis=-1, keepdims=True) + 1e-06)
        at = slice(place * rows, (place + 1) * rows)
        out_ref[0, at, :] = (values * scale).astype(jnp.bfloat16)
        mix_out_ref[0, at, :] = mix_ref[zz, 0, xx]


def norm(where, tokens, mix):
    zs, ys, xs, rows, width = tokens.shape
    experts = mix.shape[-1]
    block = lambda last: pl.BlockSpec((zs, 1, xs, rows, last), lambda i, w: (0, w[3] ^ i, 0, 0, 0))
    out = lambda last: pl.BlockSpec((1, xs * zs * rows, last), lambda i, w: (i, 0, 0))
    return call(
        norm_kernel, (ys,), [block(width), block(experts)], [out(width), out(experts)],
        [
            shaped(ys, xs * zs * rows, width),
            shaped(ys, xs * zs * rows, experts, dtype=jnp.float32),
        ],
        (where, tokens, mix), 6e9, 17e6,
    )


def fill(where_ref, own_ref, other_ref, gate, up):
    tp = where_ref[1]
    half = own_ref.shape[1]
    for ref, side in ((own_ref, tp), (other_ref, 1 - tp)):
        rows = pl.ds(pl.multiple_of(side * half, 16), half)
        gate[rows, :] = ref[0]
        up[rows, :] = ref[1]
    rest = jnp.zeros((gate.shape[0] - 2 * half, gate.shape[1]), jnp.bfloat16)
    gate[2 * half :, :] = rest
    up[2 * half :, :] = rest


def hidden_of(normed, mix, gate, up):
    dims = (((1,), (1,)), ((), ()))
    gate_act = lax.dot_general(normed, gate, dims, preferred_element_type=jnp.float32)
    up_act = lax.dot_general(normed, up, dims, preferred_element_type=jnp.float32)
    return (gate_act / (1.0 + jnp.exp(-gate_act)) * up_act * mix).astype(jnp.bfloat16)


def hidden_kernel(expert, where_ref, normed_ref, mix_ref, own_ref, other_ref, out_ref, gate, up):
    @pl.when(pl.program_id(0) == 0)
    def _():
        fill(where_ref, own_ref, other_ref, gate, up)

    mix = mix_ref[0, :, expert : expert + 1]
    out_ref[0] = hidden_of(normed_ref[0], mix, gate[...], up[...])


def hidden_units(where, normed, mix, own, other, expert):
    groups, rows, width = normed.shape
    at = lambda g, w: (g, 0, 0)
    side = whole(own.shape)
    weight = pltpu.VMEM((UNITS, width), jnp.bfloat16)
    return call(
        lambda *refs: hidden_kernel(expert, *refs), (groups,),
        [pl.BlockSpec((1, rows, width), at), pl.BlockSpec((1, rows, mix.shape[-1]), at), side, side],
        pl.BlockSpec((1, rows, UNITS), at), shaped(groups, rows, UNITS),
        (where, normed, mix, own, other), 4 * groups * rows * width * UNITS, 12e6,
        scratch=(weight, weight),
    )


def down_kernel(colors, starts, where_ref, *refs):
    hidden, down_ref, outs = refs[:3], refs[3], refs[4:]
    ys, block, _ = hidden[0].shape
    for yy in range(ys):
        rows = jnp.concatenate([h[yy] for h in hidden], axis=1)
        for index, ((exchanges, width), start) in enumerate(zip(colors, starts)):
            at = slice(start, start + width)
            product = jnp.dot(rows, down_ref[:, at], preferred_element_type=jnp.float32)
            product = product.astype(jnp.bfloat16)
            send_ref, keep_ref = outs[2 * index : 2 * index + 2]
            axis, mask = exchanges[0]
            place = {0: (keep_ref, 0), 4 - mask: (keep_ref, 1), mask: (send_ref, 0), 2: (send_ref, 1)}
            if axis == 1:
                ref, k = place[yy]
                ref[k * block : (k + 1) * block] = product
            elif axis == 2:
                part = block // 4
                for xx in range(4):
                    ref, k = place[xx]
                    to = (k * ys + yy) * part
                    ref[to : to + part] = product[xx * part : (xx + 1) * part]
            else:
                part = block // 8
                for xx in range(4):
                    to, at_x = (yy * 4 + xx) * part, 2 * xx * part
                    keep_ref[to : to + part] = product[at_x : at_x + part]
                    send_ref[to : to + part] = product[at_x + part : at_x + 2 * part]


def down_product(where, hidden, down, chosen):
    ys, block, units = hidden[0].shape
    half = ys * block // 2
    colors = [COLORS[c] for c in chosen]
    starts = [sum(width for _, width in COLORS[:c]) for c in chosen]
    outs = [(half, width) for _, width in colors for _ in range(2)]
    columns = sum(width for _, width in colors)
    return call(
        lambda *refs: down_kernel(colors, starts, *refs), (1,),
        [whole(hidden[0].shape)] * 3 + [whole(down.shape)],
        [whole(out) for out in outs], [shaped(*out) for out in outs],
        (where, *hidden, down), 2 * ys * block * 3 * units * columns, 10e6,
    )


def swap(array, axis, mask):
    peers = lax.axis_size(axis)
    return lax.ppermute(array, axis, [(i, i ^ mask) for i in range(peers)])


def added(terms):
    total = terms[0].astype(jnp.float32)
    for term in terms[1:]:
        total = total + term.astype(jnp.float32)
    return total


class Sums:
    def __init__(self, send, keep, exchanges):
        axis, mask = exchanges[0]
        self.axes = (axis, *(a for a in (1, 2, 0) if a != axis))
        sizes = [2 if a == 0 else 4 for a in self.axes]
        sizes[0] //= 2
        shape = (*sizes, -1, send.shape[-1])
        came = swap(send, FS[axis], mask).reshape(shape)
        self.offsets = [[0, 1, 2, 3] if a else [0, 1] for a in self.axes]
        self.offsets[0] = [0, 4 - mask] if axis else [0]
        places = [list(range(size)) for size in sizes]
        self.terms = [(keep.reshape(shape), places), (came, [list(p) for p in places])]

    def at(self, dim, index):
        parts = []
        for array, places in self.terms:
            for d, place in enumerate(places):
                if d == dim:
                    array = lax.slice_in_dim(array, place[index], place[index] + 1, axis=d)
                elif len(place) < array.shape[d]:
                    array = lax.slice_in_dim(array, place[0], place[0] + 1, axis=d)
            parts.append(array)
        return added(parts)

    def exchange(self, axis, mask):
        dim = self.axes.index(axis)
        have = self.offsets[dim]
        going, staying = ([mask], [0]) if len(have) == 2 else ([mask, 2], [0, 4 - mask])
        send = [self.at(dim, have.index(o)).astype(jnp.bfloat16) for o in going]
        came = swap(jnp.concatenate(send, axis=dim), FS[axis], mask)
        for _, places in self.terms:
            places[dim] = [places[dim][have.index(o)] for o in staying]
        self.terms.append((came, [list(range(size)) for size in came.shape[:3]]))
        self.offsets[dim] = staying

    def block(self, dim, index):
        total = self.at(dim, index)
        return total.reshape(total.shape[-2:])


def mixing(chosen, weights, experts):
    share = weights / jnp.sum(weights, axis=-1, keepdims=True)
    labels = jnp.arange(experts, dtype=jnp.int32)
    match = (chosen[:, :, None] == labels[None, None, :]).astype(jnp.float32)
    return jnp.sum(share[:, :, None] * match, axis=1)


def program(tokens, gate_master, up_master, down_master, norm_gain, route, route_weight):
    z, tp = lax.axis_index(Z), lax.axis_index("tp")
    where = [z, tp, lax.axis_index("gr"), lax.axis_index("fs_1"), lax.axis_index("fs_2")]
    where = jnp.stack(where).astype(jnp.int32)
    experts = gate_master.shape[0]
    peers = lax.axis_size(PLANE)
    other_core = lambda v: swap(v, "tp", 1)
    gain = norm_gain[None, :]

    own, send = pack(where, gate_master, up_master, gain, peers // 2)
    came = other_core(send)
    blocks = jnp.where(
        tp == 0, jnp.concatenate([own, came], axis=0), jnp.concatenate([came, own], axis=0)
    )
    mine = lax.all_to_all(blocks, PLANE, split_axis=0, concat_axis=0, tiled=True)

    down_own = down_master.astype(jnp.bfloat16)
    down_far = swap(down_own, "gr", 1)
    down_own_core, down_far_core = other_core(down_own), other_core(down_far)

    _, width = tokens.shape[1:]
    places = [lax.axis_size(a) for a in FS]
    combine = mixing(route[0], route_weight[0], experts)
    normed, mix = norm(
        where, tokens.reshape(*places, -1, width), combine.reshape(*places, -1, experts)
    )
    quarters = (down_own, down_far, down_own_core, down_far_core)
    mine, normed, quarters = lax.optimization_barrier((mine, normed, quarters))
    down_out, down_padded = join(where, quarters)

    sides, hidden = [], []
    for e in range(experts):
        piece = mine[:, e]
        below = lax.ppermute(piece, Z, [(1, 0), (2, 1), (0, 3)])
        above = lax.ppermute(piece, Z, [(1, 2), (2, 3), (3, 0)])
        passed = jnp.where(z == 3, below, above)
        far = lax.ppermute(passed, Z, [(3, 2), (0, 1)])
        own = unpack(where, (piece, below, above, far))
        sides += [own, other_core(own)]
        hidden.append(hidden_units(where, normed, mix, sides[-2], sides[-1], e))

    flat_down = down_padded.reshape(-1, width)
    sums = []
    for chosen in CALLS:
        outs = down_product(where, hidden, flat_down, chosen)
        for index, color in enumerate(chosen):
            sums.append(Sums(outs[2 * index], outs[2 * index + 1], COLORS[color][0]))
    for step in range(1, 5):
        for color, (exchanges, _) in zip(sums, COLORS):
            if step < len(exchanges):
                color.exchange(*exchanges[step])
    late = sums[:-1]
    sent = jnp.concatenate([c.block(2, 1).astype(jnp.bfloat16) for c in late], axis=1)
    came = swap(sent, "fs_0", 1)
    columns, start = [], 0
    for color, (_, span) in zip(late, COLORS):
        columns.append(added([color.block(2, 0), came[:, start : start + span]]))
        start += span
    columns.append(sums[-1].block(0, 0))
    mixed = jnp.concatenate([c.astype(jnp.bfloat16) for c in columns], axis=1)[None]
    gate_t, up_t = assemble(where, sides)
    return (jnp.swapaxes(gate_t, 1, 2), jnp.swapaxes(up_t, 1, 2), down_out, mixed)


def solution(mesh):
    split = Mesh(
        mesh.devices.reshape(mesh.shape["gr"], 2, 4, 4, mesh.shape["tp"]),
        ("gr", "fs_0", "fs_1", "fs_2", "tp"),
    )
    in_specs = (
        P(("gr", "tp"), None, None),
        P(None, FS, ("gr", "tp")),
        P(None, FS, ("gr", "tp")),
        P(None, FS, ("gr", "tp")),
        P(FS),
        P(("gr", "tp"), None, None),
        P(("gr", "tp"), None, None),
    )
    out_specs = (P(None, None, FS), P(None, None, FS), P(None, FS, None), P(("gr", "tp"), FS, None))
    return jax.shard_map(
        program, mesh=split, in_specs=in_specs, out_specs=out_specs, check_vma=False
    )
```

profile of v0, /device:TPU:0, one launch (start us, length us, event | category | flops | bytes accessed | tf_op | source)
XLA Modules:
  0.0 239.5 jit_solution(12596084695739171909)
XLA Ops:
  1.2 4.9 %shard_map.102 = (bf16[8,3,112,128]{3,2,1,0:T(8,128)(2,1)}, bf16[8,3,112,128]{3,2,1,0:T(8,128)(2,1)}) custom-call(s32[5]{0:T(128)} %stack.23.where_ref.refs_0_, f32[3,64,1792]{2,1,0:T(8,128)} %gate_ref.1, f32[3,64,1792]{2,1,0:T(8,128)} %up_ref.1, f32[1,64]{1,0:T(1,128)} %bitcast.116), custom_call_target="tpu_custom_call" | custom-call | flops 3000000000 | bytes 6000000 | tf_op jit(solution)/shard_map/pallas_call | solution.py:27
  6.2 4.1 %collective-permute-start.1 = (bf16[3,224,512]{2,1,0:T(8,128)(2,1)S(1)}, bf16[3,224,512]{2,1,0:T(8,128)(2,1)}, u32[]{:S(2)}, u32[]{:S(2)}) collective-permute-start(bf16[3,224,512]{2,1,0:T(8,128)(2,1)S(1)} %convert_element_type.582.refs_0_), channel_id=1, source_target_pairs={{0,64},{64,0},{1,65},{65,1},{2,66},{66,2},{3,67},{67,3},{4,68},{68... | collective-permute-start | bytes 2064392 | tf_op jit(solution)/shard_map/ppermute | solution.py:264
  11.6 7.2 %all-to-all-start = ((bf16[16,3,112,128]{3,2,1,0:T(8,128)(2,1)}), bf16[16,3,112,128]{3,2,1,0:T(8,128)(2,1)S(1)}, u32[]{:S(2)}, u32[]{:S(2)}) async-start(bf16[16,3,112,128]{3,2,1,0:T(8,128)(2,1)} %maximum_select_fusion), calls=%async_computation | async-start | bytes 2752512 | tf_op jit(solution)/shard_map/all_to_all | solution.py:335
  18.9 7.6 %collective-permute-done.1.refs_1_ = bf16[3,224,512]{2,1,0:T(8,128)(2,1)} collective-permute-done((bf16[3,224,512]{2,1,0:T(8,128)(2,1)S(1)}, bf16[3,224,512]{2,1,0:T(8,128)(2,1)}, u32[]{:S(2)}, u32[]{:S(2)}) %collective-permute-start.1) | collective-permute-done | bytes 688160 | tf_op jit(solution)/shard_map/ppermute | solution.py:264
  27.9 9.0 %shard_map.103 = (bf16[4,512,2048]{2,1,0:T(8,128)(2,1)}, f32[4,512,3]{2,1,0:T(8,128)}) custom-call(s32[5]{0:T(128)} %stack.23.where_ref.refs_0_, bf16[2,4,4,64,2048]{4,3,2,1,0:T(8,128)(2,1)} %bitcast.115, f32[2,4,4,64,3]{4,3,2,1,0:T(8,128)} %bitcast.103), custom_call_target="tpu_custom_call" | custom-call | flops 6000000000 | bytes 17000000 | tf_op jit(solution)/shard_map/pallas_call | solution.py:27
  37.0 4.3 %all-to-all-done = bf16[16,3,112,128]{3,2,1,0:T(8,128)(2,1)S(1)} async-done(((bf16[16,3,112,128]{3,2,1,0:T(8,128)(2,1)}), bf16[16,3,112,128]{3,2,1,0:T(8,128)(2,1)S(1)}, u32[]{:S(2)}, u32[]{:S(2)}) %all-to-all-start) | async-done | bytes 1376288 | tf_op jit(solution)/shard_map/all_to_all | solution.py:335
  42.8 5.8 %collective-permute-start.12 = (bf16[16,112,128]{2,1,0:T(8,128)(2,1)S(1)}, bf16[16,112,128]{2,1,0:T(8,128)(2,1)S(1)}, u32[]{:S(2)}, u32[]{:S(2)}) collective-permute-start(bf16[16,112,128]{2,1,0:T(8,128)(2,1)S(1)} %get-tuple-element.58.own_ref), channel_id=1, source_target_pairs={{32,0},{64,32},{0,96},{33,1},{65,33},{1,97},{34,2},{66,34},{2,98},... | collective-permute-start | bytes 1376264 | tf_op jit(solution)/shard_map/ppermute | solution.py:354
  49.9 5.8 %collective-permute-start.8 = (bf16[16,112,128]{2,1,0:T(8,128)(2,1)S(1)}, bf16[16,112,128]{2,1,0:T(8,128)(2,1)S(1)}, u32[]{:S(2)}, u32[]{:S(2)}) collective-permute-start(bf16[16,112,128]{2,1,0:T(8,128)(2,1)S(1)} %get-tuple-element.59.own_ref), channel_id=1, source_target_pairs={{32,0},{64,32},{0,96},{33,1},{65,33},{1,97},{34,2},{66,34},{2,98},... | collective-permute-start | bytes 1376264 | tf_op jit(solution)/shard_map/ppermute | solution.py:354
  59.5 4.0 %collective-permute-start.14 = (bf16[16,112,128]{2,1,0:T(8,128)(2,1)S(1)}, bf16[16,112,128]{2,1,0:T(8,128)(2,1)}, u32[]{:S(2)}, u32[]{:S(2)}) collective-permute-start(bf16[16,112,128]{2,1,0:T(8,128)(2,1)S(1)} %broadcast_select_fusion), channel_id=1, source_target_pairs={{96,64},{0,32},{97,65},{1,33},{98,66},{2,34},{99,67},{3,35},{100,6... | collective-permute-start | bytes 1376264 | tf_op jit(solution)/shard_map/ppermute | solution.py:357
  64.7 5.8 %collective-permute-start.4 = (bf16[16,112,128]{2,1,0:T(8,128)(2,1)S(1)}, bf16[16,112,128]{2,1,0:T(8,128)(2,1)S(1)}, u32[]{:S(2)}, u32[]{:S(2)}) collective-permute-start(bf16[16,112,128]{2,1,0:T(8,128)(2,1)S(1)} %get-tuple-element.60.own_ref), channel_id=1, source_target_pairs={{32,0},{64,32},{0,96},{33,1},{65,33},{1,97},{34,2},{66,34},{2,98},... | collective-permute-start | bytes 1376264 | tf_op jit(solution)/shard_map/ppermute | solution.py:354
  83.1 5.3 %collective-permute-done.6.far_ref = bf16[16,112,128]{2,1,0:T(8,128)(2,1)S(1)} collective-permute-done((bf16[16,112,128]{2,1,0:T(8,128)(2,1)S(1)}, bf16[16,112,128]{2,1,0:T(8,128)(2,1)S(1)}, u32[]{:S(2)}, u32[]{:S(2)}) %collective-permute-start.6) | collective-permute-done | bytes 458784 | tf_op jit(solution)/shard_map/ppermute | solution.py:357
  92.7 5.6 %shard_map.108 = (bf16[3,224,2048]{2,1,0:T(8,128)(2,1)}, bf16[3,256,2048]{2,1,0:T(8,128)(2,1)}) custom-call(s32[5]{0:T(128)} %stack.23.where_ref.refs_0_, bf16[3,224,512]{2,1,0:T(8,128)(2,1)} %copy-done.6, bf16[3,224,512]{2,1,0:T(8,128)(2,1)} %collective-permute-done.1.refs_1_, bf16[3,224,512]{2,1,0:T(8,128)(2,1)} %copy-done.24, bf16[3,224,512]{2,1,0:T(8,128)(2,1)} %copy-done.25), custom_call_target="tpu_custom_call" | custom-call | flops 2000000000 | bytes 8000000 | tf_op jit(solution)/shard_map/pallas_call | solution.py:27
  99.3 9.5 %shard_map.111.refs_3_ = bf16[4,512,256]{2,1,0:T(8,128)(2,1)} custom-call(s32[5]{0:T(128)} %stack.23.where_ref.refs_0_, bf16[4,512,2048]{2,1,0:T(8,128)(2,1)} %get-tuple-element.39.refs_1_, f32[4,512,3]{2,1,0:T(8,128)} %get-tuple-element.40.refs_2_, bf16[2,112,2048]{2,1,0:T(8,128)(2,1)} %shard_map.106.refs_4_.refs_3_, bf16[2,112,2048]{2,1,0:T(8,128)(2,1)} %copy-done.21), custom_call_target="tpu_custom_call" | custom-call | flops 4294967296 | bytes 12000000 | tf_op jit(solution)/shard_map/pallas_call | solution.py:27
  109.7 9.5 %shard_map.110.refs_2_ = bf16[4,512,256]{2,1,0:T(8,128)(2,1)} custom-call(s32[5]{0:T(128)} %stack.23.where_ref.refs_0_, bf16[4,512,2048]{2,1,0:T(8,128)(2,1)} %get-tuple-element.39.refs_1_, f32[4,512,3]{2,1,0:T(8,128)} %get-tuple-element.40.refs_2_, bf16[2,112,2048]{2,1,0:T(8,128)(2,1)} %shard_map.105.refs_2_.refs_3_, bf16[2,112,2048]{2,1,0:T(8,128)(2,1)} %copy-done.22), custom_call_target="tpu_custom_call" | custom-call | flops 4294967296 | bytes 12000000 | tf_op jit(solution)/shard_map/pallas_call | solution.py:27
  120.1 9.5 %shard_map.109.refs_1_ = bf16[4,512,256]{2,1,0:T(8,128)(2,1)} custom-call(s32[5]{0:T(128)} %stack.23.where_ref.refs_0_, bf16[4,512,2048]{2,1,0:T(8,128)(2,1)} %get-tuple-element.39.refs_1_, f32[4,512,3]{2,1,0:T(8,128)} %get-tuple-element.40.refs_2_, bf16[2,112,2048]{2,1,0:T(8,128)(2,1)} %shard_map.104.refs_0_.refs_3_, bf16[2,112,2048]{2,1,0:T(8,128)(2,1)} %copy-done.23), custom_call_target="tpu_custom_call" | custom-call | flops 4294967296 | bytes 12000000 | tf_op jit(solution)/shard_map/pallas_call | solution.py:27
  129.6 8.1 %shard_map.112 = (bf16[1024,512]{1,0:T(8,128)(2,1)}, bf16[1024,512]{1,0:T(8,128)(2,1)}, bf16[1024,384]{1,0:T(8,128)(2,1)}, bf16[1024,384]{1,0:T(8,128)(2,1)}) custom-call(s32[5]{0:T(128)} %stack.23.where_ref.refs_0_, bf16[4,512,256]{2,1,0:T(8,128)(2,1)} %shard_map.109.refs_1_, bf16[4,512,256]{2,1,0:T(8,128)(2,1)} %shard_map.110.refs_2_, ...), custom_call_target="tpu_custom_call" | custom-call | flops 2818572288 | bytes 10000000 | tf_op jit(solution)/shard_map/pallas_call | solution.py:27
  139.6 9.8 %shard_map.113 = (bf16[1024,384]{1,0:T(8,128)(2,1)}, bf16[1024,384]{1,0:T(8,128)(2,1)}, bf16[1024,384]{1,0:T(8,128)(2,1)}, bf16[1024,384]{1,0:T(8,128)(2,1)}, bf...) custom-call(s32[5]{0:T(128)} %stack.23.where_ref.refs_0_, bf16[4,512,256]{2,1,0:T(8,128)(2,1)} %shard_map.109.refs_1_, ...), custom_call_target="tpu_custom_call" | custom-call | flops 3623878656 | bytes 10000000 | tf_op jit(solution)/shard_map/pallas_call | solution.py:27
  156.9 6.1 %shard_map.107 = (bf16[3,224,2048]{2,1,0:T(8,128)(2,1)}, bf16[3,224,2048]{2,1,0:T(8,128)(2,1)}) custom-call(s32[5]{0:T(128)} %stack.23.where_ref.refs_0_, bf16[2,112,2048]{2,1,0:T(8,128)(2,1)} %shard_map.104.refs_0_.refs_3_, bf16[2,112,2048]{2,1,0:T(8,128)(2,1)} %copy-done.23, bf16[2,112,2048]{2,1,0:T(8,128)(2,1)} %shard_map.105.refs_2_.refs_3_, ...), custom_call_target="tpu_custom_call" | custom-call | flops 4000000000 | bytes 11000000 | tf_op jit(solution)/shard_map/pallas_call | solution.py:27
  176.2 15.3 %collective-permute-done.16 = bf16[1024,512]{1,0:T(8,128)(2,1)S(1)} collective-permute-done((bf16[1024,512]{1,0:T(8,128)(2,1)S(1)}, bf16[1024,512]{1,0:T(8,128)(2,1)S(1)}, u32[]{:S(2)}, u32[]{:S(2)}) %collective-permute-start.16) | collective-permute-done | bytes 1048608 | tf_op jit(solution)/shard_map/ppermute | solution.py:264
  192.6 7.4 %collective-permute-done.25 = bf16[1,4,2,64,384]{4,3,2,1,0:T(8,128)(2,1)S(1)} collective-permute-done((bf16[1,4,2,64,384]{4,3,2,1,0:T(8,128)(2,1)S(1)}, bf16[1,4,2,64,384]{4,3,2,1,0:T(8,128)(2,1)S(1)}, u32[]{:S(2)}, u32[]{:S(2)}) %collective-permute-start.25) | collective-permute-done | bytes 393248 | tf_op jit(solution)/shard_map/ppermute | solution.py:264
  201.7 6.7 %collective-permute-done.34 = bf16[1,2,4,64,384]{4,3,2,1,0:T(8,128)(2,1)S(1)} collective-permute-done((bf16[1,2,4,64,384]{4,3,2,1,0:T(8,128)(2,1)S(1)}, bf16[1,2,4,64,384]{4,3,2,1,0:T(8,128)(2,1)S(1)}, u32[]{:S(2)}, u32[]{:S(2)}) %collective-permute-start.34) | collective-permute-done | bytes 393248 | tf_op jit(solution)/shard_map/ppermute | solution.py:264
  219.1 6.2 %collective-permute-done.18 = bf16[1,2,2,64,512]{4,3,2,1,0:T(8,128)(2,1)S(1)} collective-permute-done((bf16[1,2,2,64,512]{4,3,2,1,0:T(8,128)(2,1)S(1)}, bf16[1,2,2,64,512]{4,3,2,1,0:T(8,128)(2,1)S(1)}, u32[]{:S(2)}, u32[]{:S(2)}) %collective-permute-start.18) | collective-permute-done | bytes 262176 | tf_op jit(solution)/shard_map/ppermute | solution.py:264
  227.6 4.0 %collective-permute-done.19 = bf16[1,1,2,64,512]{4,3,2,1,0:T(8,128)(2,1)S(1)} collective-permute-done((bf16[1,1,2,64,512]{4,3,2,1,0:T(8,128)(2,1)S(1)}, bf16[1,1,2,64,512]{4,3,2,1,0:T(8,128)(2,1)S(1)}, u32[]{:S(2)}, u32[]{:S(2)}) %collective-permute-start.19) | collective-permute-done | bytes 131104 | tf_op jit(solution)/shard_map/ppermute | solution.py:264
  233.3 4.4 %collective-permute-done.32 = bf16[64,1664]{1,0:T(8,128)(2,1)S(1)} collective-permute-done((bf16[64,1664]{1,0:T(8,128)(2,1)S(1)}, bf16[64,1664]{1,0:T(8,128)(2,1)S(1)}, u32[]{:S(2)}, u32[]{:S(2)}) %collective-permute-start.32) | collective-permute-done | bytes 213024 | tf_op jit(solution)/shard_map/ppermute | solution.py:264
  (171 shorter events, 72.5 us)
Async XLA Ops:
  6.2 20.3 %collective-permute-start.1 = (bf16[3,224,512]{2,1,0:T(8,128)(2,1)S(1)}, bf16[3,224,512]{2,1,0:T(8,128)(2,1)}, u32[]{:S(2)}, u32[]{:S(2)}) collective-permute-start(bf16[3,224,512]{2,1,0:T(8,128)(2,1)S(1)} %convert_element_type.582.refs_0_), channel_id=1, source_target_pairs={{0,64},{64,0},{1,65},{65,1},{2,66},{66,2},{3,67},{67,3},{4,68},{68... | collective-permute-start | bytes 2064392 | tf_op jit(solution)/shard_map/ppermute | solution.py:264
  11.6 29.7 %all-to-all-start = ((bf16[16,3,112,128]{3,2,1,0:T(8,128)(2,1)}), bf16[16,3,112,128]{3,2,1,0:T(8,128)(2,1)S(1)}, u32[]{:S(2)}, u32[]{:S(2)}) async-start(bf16[16,3,112,128]{3,2,1,0:T(8,128)(2,1)} %maximum_select_fusion), calls=%async_computation | async-start | bytes 2752512 | tf_op jit(solution)/shard_map/all_to_all | solution.py:335
  18.8 18.2 %collective-permute-start.2 = (bf16[3,224,512]{2,1,0:T(8,128)(2,1)S(1)}, bf16[3,224,512]{2,1,0:T(8,128)(2,1)S(1)}, u32[]{:S(2)}, u32[]{:S(2)}) collective-permute-start(bf16[3,224,512]{2,1,0:T(8,128)(2,1)S(1)} %convert_element_type.582.refs_0_), channel_id=1, source_target_pairs={{0,1},{1,0},{2,3},{3,2},{4,5},{5,4},{6,7},{7,6},{8,9},{9,8},{10,11... | collective-permute-start | bytes 2064392 | tf_op jit(solution)/shard_map/ppermute | solution.py:264
  41.5 16.5 %collective-permute-start.13 = (bf16[16,112,128]{2,1,0:T(8,128)(2,1)S(1)}, bf16[16,112,128]{2,1,0:T(8,128)(2,1)S(1)}, u32[]{:S(2)}, u32[]{:S(2)}) collective-permute-start(bf16[16,112,128]{2,1,0:T(8,128)(2,1)S(1)} %get-tuple-element.58.own_ref), channel_id=1, source_target_pairs={{32,64},{64,96},{96,0},{33,65},{65,97},{97,1},{34,66},{66,98},{98,... | collective-permute-start | bytes 1376264 | tf_op jit(solution)/shard_map/ppermute | solution.py:355
  42.8 16.7 %collective-permute-start.12 = (bf16[16,112,128]{2,1,0:T(8,128)(2,1)S(1)}, bf16[16,112,128]{2,1,0:T(8,128)(2,1)S(1)}, u32[]{:S(2)}, u32[]{:S(2)}) collective-permute-start(bf16[16,112,128]{2,1,0:T(8,128)(2,1)S(1)} %get-tuple-element.58.own_ref), channel_id=1, source_target_pairs={{32,0},{64,32},{0,96},{33,1},{65,33},{1,97},{34,2},{66,34},{2,98},... | collective-permute-start | bytes 1376264 | tf_op jit(solution)/shard_map/ppermute | solution.py:354
  48.6 22.0 %collective-permute-start.9 = (bf16[16,112,128]{2,1,0:T(8,128)(2,1)S(1)}, bf16[16,112,128]{2,1,0:T(8,128)(2,1)S(1)}, u32[]{:S(2)}, u32[]{:S(2)}) collective-permute-start(bf16[16,112,128]{2,1,0:T(8,128)(2,1)S(1)} %get-tuple-element.59.own_ref), channel_id=1, source_target_pairs={{32,64},{64,96},{96,0},{33,65},{65,97},{97,1},{34,66},{66,98},{98,... | collective-permute-start | bytes 1376264 | tf_op jit(solution)/shard_map/ppermute | solution.py:355
  49.9 20.7 %collective-permute-start.8 = (bf16[16,112,128]{2,1,0:T(8,128)(2,1)S(1)}, bf16[16,112,128]{2,1,0:T(8,128)(2,1)S(1)}, u32[]{:S(2)}, u32[]{:S(2)}) collective-permute-start(bf16[16,112,128]{2,1,0:T(8,128)(2,1)S(1)} %get-tuple-element.59.own_ref), channel_id=1, source_target_pairs={{32,0},{64,32},{0,96},{33,1},{65,33},{1,97},{34,2},{66,34},{2,98},... | collective-permute-start | bytes 1376264 | tf_op jit(solution)/shard_map/ppermute | solution.py:354
  59.5 13.5 %collective-permute-start.14 = (bf16[16,112,128]{2,1,0:T(8,128)(2,1)S(1)}, bf16[16,112,128]{2,1,0:T(8,128)(2,1)}, u32[]{:S(2)}, u32[]{:S(2)}) collective-permute-start(bf16[16,112,128]{2,1,0:T(8,128)(2,1)S(1)} %broadcast_select_fusion), channel_id=1, source_target_pairs={{96,64},{0,32},{97,65},{1,33},{98,66},{2,34},{99,67},{3,35},{100,6... | collective-permute-start | bytes 1376264 | tf_op jit(solution)/shard_map/ppermute | solution.py:357
  76.4 21.9 %collective-permute-start.15 = (bf16[2,112,2048]{2,1,0:T(8,128)(2,1)}, bf16[2,112,2048]{2,1,0:T(8,128)(2,1)S(1)}, u32[]{:S(2)}, u32[]{:S(2)}) collective-permute-start(bf16[2,112,2048]{2,1,0:T(8,128)(2,1)} %shard_map.106.refs_4_.refs_3_), channel_id=1, source_target_pairs={{0,1},{1,0},{2,3},{3,2},{4,5},{5,4},{6,7},{7,6},{8,9},{9,8},{10,11... | collective-permute-start | bytes 2752520 | tf_op jit(solution)/shard_map/ppermute | solution.py:264
  83.1 25.6 %collective-permute-start.11 = (bf16[2,112,2048]{2,1,0:T(8,128)(2,1)}, bf16[2,112,2048]{2,1,0:T(8,128)(2,1)S(1)}, u32[]{:S(2)}, u32[]{:S(2)}) collective-permute-start(bf16[2,112,2048]{2,1,0:T(8,128)(2,1)} %shard_map.105.refs_2_.refs_3_), channel_id=1, source_target_pairs={{0,1},{1,0},{2,3},{3,2},{4,5},{5,4},{6,7},{7,6},{8,9},{9,8},{10,11... | collective-permute-start | bytes 2752520 | tf_op jit(solution)/shard_map/ppermute | solution.py:264
  92.7 26.5 %collective-permute-start.7 = (bf16[2,112,2048]{2,1,0:T(8,128)(2,1)}, bf16[2,112,2048]{2,1,0:T(8,128)(2,1)S(1)}, u32[]{:S(2)}, u32[]{:S(2)}) collective-permute-start(bf16[2,112,2048]{2,1,0:T(8,128)(2,1)} %shard_map.104.refs_0_.refs_3_), channel_id=1, source_target_pairs={{0,1},{1,0},{2,3},{3,2},{4,5},{5,4},{6,7},{7,6},{8,9},{9,8},{10,11... | collective-permute-start | bytes 2752520 | tf_op jit(solution)/shard_map/ppermute | solution.py:264
  137.7 27.9 %collective-permute-start.20 = (bf16[1024,384]{1,0:T(8,128)(2,1)}, bf16[1024,384]{1,0:T(8,128)(2,1)S(1)}, u32[]{:S(2)}, u32[]{:S(2)}) collective-permute-start(bf16[1024,384]{1,0:T(8,128)(2,1)} %get-tuple-element.45), channel_id=1, source_target_pairs={{0,2},{2,0},{4,6},{6,4},{1,3},{3,1},{5,7},{7,5},{8,10},{10,8},{12,... | collective-permute-start | bytes 2359304 | tf_op jit(solution)/shard_map/ppermute | solution.py:264
  149.3 21.1 %collective-permute-start.24 = (bf16[1024,384]{1,0:T(8,128)(2,1)}, bf16[1024,384]{1,0:T(8,128)(2,1)S(1)}, u32[]{:S(2)}, u32[]{:S(2)}) collective-permute-start(bf16[1024,384]{1,0:T(8,128)(2,1)} %get-tuple-element.47), channel_id=1, source_target_pairs={{0,24},{8,16},{16,8},{24,0},{1,25},{9,17},{17,9},{25,1},{2,26},{10... | collective-permute-start | bytes 2359304 | tf_op jit(solution)/shard_map/ppermute | solution.py:264
  152.4 21.8 %collective-permute-start.28 = (bf16[1024,384]{1,0:T(8,128)(2,1)}, bf16[1024,384]{1,0:T(8,128)(2,1)S(1)}, u32[]{:S(2)}, u32[]{:S(2)}) collective-permute-start(bf16[1024,384]{1,0:T(8,128)(2,1)} %get-tuple-element.49), channel_id=1, source_target_pairs={{0,6},{2,4},{4,2},{6,0},{1,7},{3,5},{5,3},{7,1},{8,14},{10,12},{12... | collective-permute-start | bytes 2359304 | tf_op jit(solution)/shard_map/ppermute | solution.py:264
  154.5 20.2 %collective-permute-start.33 = (bf16[1024,384]{1,0:T(8,128)(2,1)}, bf16[1024,384]{1,0:T(8,128)(2,1)}, u32[]{:S(2)}, u32[]{:S(2)}) collective-permute-start(bf16[1024,384]{1,0:T(8,128)(2,1)} %get-tuple-element.51), channel_id=1, source_target_pairs={{0,32},{32,0},{1,33},{33,1},{2,34},{34,2},{3,35},{35,3},{4,36},{36... | collective-permute-start | bytes 2359304 | tf_op jit(solution)/shard_map/ppermute | solution.py:264
  165.5 26.0 %collective-permute-start.16 = (bf16[1024,512]{1,0:T(8,128)(2,1)S(1)}, bf16[1024,512]{1,0:T(8,128)(2,1)S(1)}, u32[]{:S(2)}, u32[]{:S(2)}) collective-permute-start(bf16[1024,512]{1,0:T(8,128)(2,1)S(1)} %copy-done.20), channel_id=1, source_target_pairs={{0,8},{8,0},{16,24},{24,16},{1,9},{9,1},{17,25},{25,17},{2,10},{10... | collective-permute-start | bytes 3145736 | tf_op jit(solution)/shard_map/ppermute | solution.py:264
  165.8 26.2 %collective-permute-start.21 = (bf16[1,4,2,64,384]{4,3,2,1,0:T(8,128)(2,1)S(1)}, bf16[1,4,2,64,384]{4,3,2,1,0:T(8,128)(2,1)S(1)}, u32[]{:S(2)}, u32[]{:S(2)}) collective-permute-start(bf16[1,4,2,64,384]{4,3,2,1,0:T(8,128)(2,1)S(1)} %bitcast.112), channel_id=1, source_target_pairs={{0,6},{2,4},{4,2},{6,0},{1,7},{3,5},{5,3},{7,1},{8,14},{10,12},{12... | collective-permute-start | bytes 1179656 | tf_op jit(solution)/shard_map/ppermute | solution.py:264
  170.6 29.3 %collective-permute-start.25 = (bf16[1,4,2,64,384]{4,3,2,1,0:T(8,128)(2,1)S(1)}, bf16[1,4,2,64,384]{4,3,2,1,0:T(8,128)(2,1)S(1)}, u32[]{:S(2)}, u32[]{:S(2)}) collective-permute-start(bf16[1,4,2,64,384]{4,3,2,1,0:T(8,128)(2,1)S(1)} %bitcast.111), channel_id=1, source_target_pairs={{0,8},{8,0},{16,24},{24,16},{1,9},{9,1},{17,25},{25,17},{2,10},{10... | collective-permute-start | bytes 1179656 | tf_op jit(solution)/shard_map/ppermute | solution.py:264
  174.3 27.0 %collective-permute-start.29 = (bf16[1,4,2,64,384]{4,3,2,1,0:T(8,128)(2,1)S(1)}, bf16[1,4,2,64,384]{4,3,2,1,0:T(8,128)(2,1)S(1)}, u32[]{:S(2)}, u32[]{:S(2)}) collective-permute-start(bf16[1,4,2,64,384]{4,3,2,1,0:T(8,128)(2,1)S(1)} %bitcast.110), channel_id=1, source_target_pairs={{0,2},{2,0},{4,6},{6,4},{1,3},{3,1},{5,7},{7,5},{8,10},{10,8},{12,... | collective-permute-start | bytes 1179656 | tf_op jit(solution)/shard_map/ppermute | solution.py:264
  175.8 32.6 %collective-permute-start.34 = (bf16[1,2,4,64,384]{4,3,2,1,0:T(8,128)(2,1)S(1)}, bf16[1,2,4,64,384]{4,3,2,1,0:T(8,128)(2,1)S(1)}, u32[]{:S(2)}, u32[]{:S(2)}) collective-permute-start(bf16[1,2,4,64,384]{4,3,2,1,0:T(8,128)(2,1)S(1)} %pad_maximum_fusion), channel_id=1, source_target_pairs={{0,8},{8,0},{16,24},{24,16},{1,9},{9,1},{17,25},{25,17},{2,10},{10... | collective-permute-start | bytes 1179656 | tf_op jit(solution)/shard_map/ppermute | solution.py:264
  191.6 27.1 %collective-permute-start.17 = (bf16[1,4,2,64,512]{4,3,2,1,0:T(8,128)(2,1)S(1)}, bf16[1,4,2,64,512]{4,3,2,1,0:T(8,128)(2,1)S(1)}, u32[]{:S(2)}, u32[]{:S(2)}) collective-permute-start(bf16[1,4,2,64,512]{4,3,2,1,0:T(8,128)(2,1)S(1)} %bitcast.109), channel_id=1, source_target_pairs={{0,24},{8,16},{16,8},{24,0},{1,25},{9,17},{17,9},{25,1},{2,26},{10... | collective-permute-start | bytes 1572872 | tf_op jit(solution)/shard_map/ppermute | solution.py:264
  192.1 18.9 %collective-permute-start.22 = (bf16[1,2,2,64,384]{4,3,2,1,0:T(8,128)(2,1)S(1)}, bf16[1,2,2,64,384]{4,3,2,1,0:T(8,128)(2,1)S(1)}, u32[]{:S(2)}, u32[]{:S(2)}) collective-permute-start(bf16[1,2,2,64,384]{4,3,2,1,0:T(8,128)(2,1)S(1)} %pad_maximum_fusion.3), channel_id=1, source_target_pairs={{0,8},{8,0},{16,24},{24,16},{1,9},{9,1},{17,25},{25,17},{2,10},{10... | collective-permute-start | bytes 589832 | tf_op jit(solution)/shard_map/ppermute | solution.py:264
  213.6 14.0 %collective-permute-start.31 = (bf16[1,1,2,64,384]{4,3,2,1,0:T(8,128)(2,1)S(1)}, bf16[1,1,2,64,384]{4,3,2,1,0:T(8,128)(2,1)S(1)}, u32[]{:S(2)}, u32[]{:S(2)}) collective-permute-start(bf16[1,1,2,64,384]{4,3,2,1,0:T(8,128)(2,1)S(1)} %add_convert_fusion.10), channel_id=1, source_target_pairs={{0,8},{8,0},{16,24},{24,16},{1,9},{9,1},{17,25},{25,17},{2,10},{10... | collective-permute-start | bytes 294920 | tf_op jit(solution)/shard_map/ppermute | solution.py:264
  217.5 14.9 %collective-permute-start.36 = (bf16[1,1,2,64,384]{4,3,2,1,0:T(8,128)(2,1)S(1)}, bf16[1,1,2,64,384]{4,3,2,1,0:T(8,128)(2,1)S(1)}, u32[]{:S(2)}, u32[]{:S(2)}) collective-permute-start(bf16[1,1,2,64,384]{4,3,2,1,0:T(8,128)(2,1)S(1)} %pad_maximum_fusion.6), channel_id=1, source_target_pairs={{0,6},{2,4},{4,2},{6,0},{1,7},{3,5},{5,3},{7,1},{8,14},{10,12},{12... | collective-permute-start | bytes 294920 | tf_op jit(solution)/shard_map/ppermute | solution.py:264
  (42 other events, 353.2 us)
where the time goes:
time: 241 us; the launch traced here: 239 us
  Pallas kernels  82.2 us (34%)
  waiting for transfers between devices  76.3 us (32%)
  starting transfers between devices  62.8 us (26%)
  local copies, waits for them, and re-layouts  8.96 us (4%)
  other arithmetic  7.9 us (3%)
    pallas_call x12, Pallas kernels, call(): pl.pallas_call(kernel, out_shape=out_shape, grid_spec=pltpu.PrefetchScala...  82.2 us
    ppermute x29, waiting for transfers between devices, swap(): return lax.ppermute(array, axis, [(i, i ^ mask) for i in range(peers)])  62.6 us
    ppermute x29, starting transfers between devices, swap(): return lax.ppermute(array, axis, [(i, i ^ mask) for i in range(peers)])  25.3 us
    ppermute x3, starting transfers between devices, program(): below = lax.ppermute(piece, Z, [(1, 0), (2, 1), (0, 3)])  17.3 us
    ppermute x3, starting transfers between devices, program(): far = lax.ppermute(passed, Z, [(3, 2), (0, 1)])  9.28 us
    all_to_all x1, starting transfers between devices, program(): lax.all_to_all(blocks, PLANE, split_axis=0, concat_axis=0, tiled=True)  7.17 us
    unnamed x54, local copies, waits for them, and re-layouts  5.56 us
    ppermute x3, waiting for transfers between devices, program(): far = lax.ppermute(passed, Z, [(3, 2), (0, 1)])  5.35 us
  transfers between devices with their start and end apart: 39, of which 17 were waited for; matrix products, arithmetic and copies ran while one was open for 4% of the time, Pallas kernels for 25%

commit v1 on v0

--- a/solution.py
+++ b/solution.py
@@ -14,13 +14,11 @@
 
 
 COLORS = (
-    (((1, 1), (1, 3), (2, 1), (2, 3)), 512),
-    (((2, 1), (2, 3), (1, 1), (1, 3)), 384),
-    (((1, 3), (1, 1), (2, 3), (2, 1)), 384),
-    (((2, 3), (2, 1), (1, 3), (1, 1)), 384),
-    (((0, 1), (1, 1), (1, 3), (2, 3), (2, 1)), 384),
+    ((1, 1), (1, 3), (2, 1), (2, 3)),
+    ((2, 1), (2, 3), (1, 1), (1, 3)),
+    ((1, 3), (1, 1), (2, 3), (2, 1)),
+    ((2, 3), (2, 1), (1, 3), (1, 1)),
 )
-CALLS = ((0, 1), (2, 3, 4))
 
 
 def call(kernel, grid, ins, outs, out_shape, args, flops, nbytes, scratch=(), vmem=60):
@@ -50,9 +48,10 @@
 
 
 def pack_kernel(where_ref, gate_ref, up_ref, gain_ref, own_ref, send_ref):
-    rows = jnp.concatenate([gate_ref[0], up_ref[0]], axis=0)
-    gain = jnp.concatenate([gain_ref[...], gain_ref[...]], axis=1)
-    cols = (rows.T * gain).astype(jnp.bfloat16)
+    depth = gain_ref.shape[1]
+    gain = jnp.broadcast_to(gain_ref[...], (128, depth)).T[:, :1]
+    rows = jnp.concatenate([gate_ref[0] * gain, up_ref[0] * gain], axis=0)
+    cols = rows.astype(jnp.bfloat16).T
     dests, _, half, lanes = own_ref.shape
     cols = cols.reshape(dests, 2, half, lanes)
     low, high = cols[:, 0], cols[:, 1]
@@ -98,7 +97,7 @@
     shape = (2, half, sources * lanes)
     return call(
         unpack_kernel, (1,), [whole(pieces[0].shape)] * 4, whole(shape),
-        shaped(*shape), (where, *pieces), 1e9, 3e6,
+        shaped(*shape), (where, *pieces), 1e9, 3e6, vmem=12,
     )
 
 
@@ -118,7 +117,7 @@
     shape = (len(sides) // 2, 2 * half, width)
     return call(
         assemble_kernel, (1,), [whole(sides[0].shape)] * len(sides),
-        [whole(shape)] * 2, [shaped(*shape)] * 2, (where, *sides), 4e9, 11e6,
+        [whole(shape)] * 2, [shaped(*shape)] * 2, (where, *sides), 4e9, 11e6, vmem=26,
     )
 
 
@@ -142,7 +141,7 @@
         join_kernel, (experts,), [pl.BlockSpec((1, depth, width), at)] * 4,
         [pl.BlockSpec((1, depth, 4 * width), at), pl.BlockSpec((1, UNITS, 4 * width), at)],
         [shaped(experts, depth, 4 * width), shaped(experts, UNITS, 4 * width)],
-        (where, *quarters), 2e9, 8e6,
+        (where, *quarters), 2e9, 8e6, vmem=16,
     )
 
 
@@ -211,51 +210,65 @@
         [pl.BlockSpec((1, rows, width), at), pl.BlockSpec((1, rows, mix.shape[-1]), at), side, side],
         pl.BlockSpec((1, rows, UNITS), at), shaped(groups, rows, UNITS),
         (where, normed, mix, own, other), 4 * groups * rows * width * UNITS, 12e6,
-        scratch=(weight, weight),
-    )
-
-
-def down_kernel(colors, starts, where_ref, *refs):
-    hidden, down_ref, outs = refs[:3], refs[3], refs[4:]
-    ys, block, _ = hidden[0].shape
-    for yy in range(ys):
-        rows = jnp.concatenate([h[yy] for h in hidden], axis=1)
-        for index, ((exchanges, width), start) in enumerate(zip(colors, starts)):
-            at = slice(start, start + width)
-            product = jnp.dot(rows, down_ref[:, at], preferred_element_type=jnp.float32)
-            product = product.astype(jnp.bfloat16)
-            send_ref, keep_ref = outs[2 * index : 2 * index + 2]
-            axis, mask = exchanges[0]
-            place = {0: (keep_ref, 0), 4 - mask: (keep_ref, 1), mask: (send_ref, 0), 2: (send_ref, 1)}
-            if axis == 1:
-                ref, k = place[yy]
-                ref[k * block : (k + 1) * block] = product
-            elif axis == 2:
-                part = block // 4
-                for xx in range(4):
-                    ref, k = place[xx]
-                    to = (k * ys + yy) * part
-                    ref[to : to + part] = product[xx * part : (xx + 1) * part]
-            else:
-                part = block // 8
-                for xx in range(4):
-                    to, at_x = (yy * 4 + xx) * part, 2 * xx * part
-                    keep_ref[to : to + part] = product[at_x : at_x + part]
-                    send_ref[to : to + part] = product[at_x + part : at_x + 2 * part]
-
-
-def down_product(where, hidden, down, chosen):
-    ys, block, units = hidden[0].shape
-    half = ys * block // 2
-    colors = [COLORS[c] for c in chosen]
-    starts = [sum(width for _, width in COLORS[:c]) for c in chosen]
-    outs = [(half, width) for _, width in colors for _ in range(2)]
-    columns = sum(width for _, width in colors)
-    return call(
-        lambda *refs: down_kernel(colors, starts, *refs), (1,),
-        [whole(hidden[0].shape)] * 3 + [whole(down.shape)],
-        [whole(out) for out in outs], [shaped(*out) for out in outs],
-        (where, *hidden, down), 2 * ys * block * 3 * units * columns, 10e6,
+        scratch=(weight, weight), vmem=48,
+    )
+
+
+def last_kernel(where_ref, normed_ref, mix_ref, *refs):
+    earlier, (own_ref, other_ref, down_ref) = refs[:2], refs[2:5]
+    outs, (gate, up) = refs[5:-2], refs[-2:]
+    yy = pl.program_id(0)
+
+    @pl.when(yy == 0)
+    def _():
+        fill(where_ref, own_ref, other_ref, gate, up)
+
+    experts = len(earlier) + 1
+    mix = mix_ref[0, :, experts - 1 : experts]
+    hidden = hidden_of(normed_ref[0], mix, gate[...], up[...])
+    rows = jnp.concatenate([r[0] for r in earlier] + [hidden], axis=1)
+    block = rows.shape[0]
+    ys = pl.num_programs(0)
+    width = outs[0].shape[1]
+    for color, exchanges in enumerate(COLORS):
+        at = slice(color * width, (color + 1) * width)
+        product = jnp.dot(rows, down_ref[:, at], preferred_element_type=jnp.float32)
+        product = product.astype(jnp.bfloat16)
+        send_ref, keep_ref = outs[2 * color : 2 * color + 2]
+        axis, mask = exchanges[0]
+        if axis == 1:
+            kept = (yy == 0) | (yy == 4 - mask)
+            later = jnp.where((yy == 4 - mask) | (yy == 2), block, 0)
+            to = pl.ds(pl.multiple_of(later, block), block)
+
+            @pl.when(kept)
+            def _():
+                keep_ref[to, :] = product
+
+            @pl.when(jnp.logical_not(kept))
+            def _():
+                send_ref[to, :] = product
+
+        else:
+            part = block // 4
+            for xx, ref, k in ((0, keep_ref, 0), (4 - mask, keep_ref, 1), (mask, send_ref, 0), (2, send_ref, 1)):
+                to = pl.ds(pl.multiple_of((k * ys + yy) * part, part), part)
+                ref[to, :] = product[xx * part : (xx + 1) * part]
+
+
+def last(where, normed, mix, earlier, own, other, down):
+    ys, rows, width = normed.shape
+    half = (ys * rows // 2, width // len(COLORS))
+    at = lambda i, w: (i, 0, 0)
+    side = whole(own.shape)
+    weight = pltpu.VMEM((UNITS, width), jnp.bfloat16)
+    return call(
+        last_kernel, (ys,),
+        [pl.BlockSpec((1, rows, width), at), pl.BlockSpec((1, rows, mix.shape[-1]), at)]
+        + [pl.BlockSpec((1, rows, UNITS), at)] * 2 + [side, side, whole(down.shape)],
+        [whole(half)] * (2 * len(COLORS)), [shaped(*half)] * (2 * len(COLORS)),
+        (where, normed, mix, *earlier, own, other, down), 10 * ys * rows * width * UNITS, 25e6,
+        scratch=(weight, weight), vmem=48,
     )
 
 
@@ -345,8 +358,8 @@
         where, tokens.reshape(*places, -1, width), combine.reshape(*places, -1, experts)
     )
     quarters = (down_own, down_far, down_own_core, down_far_core)
-    mine, normed, quarters = lax.optimization_barrier((mine, normed, quarters))
     down_out, down_padded = join(where, quarters)
+    mine, normed = lax.optimization_barrier((mine, normed))
 
     sides, hidden = [], []
     for e in range(experts):
@@ -357,27 +370,21 @@
         far = lax.ppermute(passed, Z, [(3, 2), (0, 1)])
         own = unpack(where, (piece, below, above, far))
         sides += [own, other_core(own)]
-        hidden.append(hidden_units(where, normed, mix, sides[-2], sides[-1], e))
+        if e < experts - 1:
+            hidden.append(hidden_units(where, normed, mix, sides[-2], sides[-1], e))
 
     flat_down = down_padded.reshape(-1, width)
+    outs = last(where, normed, mix, hidden, sides[-2], sides[-1], flat_down)
     sums = []
-    for chosen in CALLS:
-        outs = down_product(where, hidden, flat_down, chosen)
-        for index, color in enumerate(chosen):
-            sums.append(Sums(outs[2 * index], outs[2 * index + 1], COLORS[color][0]))
-    for step in range(1, 5):
-        for color, (exchanges, _) in zip(sums, COLORS):
-            if step < len(exchanges):
-                color.exchange(*exchanges[step])
-    late = sums[:-1]
-    sent = jnp.concatenate([c.block(2, 1).astype(jnp.bfloat16) for c in late], axis=1)
+    for color, exchanges in enumerate(COLORS):
+        sums.append(Sums(outs[2 * color], outs[2 * color + 1], exchanges))
+    for step in range(1, 4):
+        for color, exchanges in zip(sums, COLORS):
+            color.exchange(*exchanges[step])
+    sent = jnp.concatenate([c.block(2, 1).astype(jnp.bfloat16) for c in sums], axis=1)
     came = swap(sent, "fs_0", 1)
-    columns, start = [], 0
-    for color, (_, span) in zip(late, COLORS):
-        columns.append(added([color.block(2, 0), came[:, start : start + span]]))
-        start += span
-    columns.append(sums[-1].block(0, 0))
-    mixed = jnp.concatenate([c.astype(jnp.bfloat16) for c in columns], axis=1)[None]
+    mine = jnp.concatenate([c.block(2, 0) for c in sums], axis=1)
+    mixed = added([mine, came]).astype(jnp.bfloat16)[None]
     gate_t, up_t = assemble(where, sides)
     return (jnp.swapaxes(gate_t, 1, 2), jnp.swapaxes(up_t, 1, 2), down_out, mixed)
 

time: 241 us -> 216 us (0.90)
  the two profiles are of different devices: /device:TPU:0 before, /device:TPU:34 now
where the time goes in v1:
time: 216 us
  waiting for transfers between devices  93.4 us (43%)
  Pallas kernels  58.2 us (27%)
  starting transfers between devices  51.3 us (24%)
  local copies, waits for them, and re-layouts  6.01 us (3%)
  other arithmetic  5.5 us (3%)
    pallas_call x10, Pallas kernels, call(): pl.pallas_call(kernel, out_shape=out_shape, grid_spec=pltpu.PrefetchScala...  58.2 us
    ppermute x24, waiting for transfers between devices, swap(): return lax.ppermute(array, axis, [(i, i ^ mask) for i in range(peers)])  42.2 us
    ppermute x24, starting transfers between devices, swap(): return lax.ppermute(array, axis, [(i, i ^ mask) for i in range(peers)])  20.8 us
    ppermute x3, waiting for transfers between devices, program(): above = lax.ppermute(piece, Z, [(1, 2), (2, 3), (3, 0)])  16.5 us
    ppermute x3, waiting for transfers between devices, program(): far = lax.ppermute(passed, Z, [(3, 2), (0, 1)])  15.3 us
    ppermute x3, starting transfers between devices, program(): above = lax.ppermute(piece, Z, [(1, 2), (2, 3), (3, 0)])  10.8 us
    ppermute x3, waiting for transfers between devices, program(): below = lax.ppermute(piece, Z, [(1, 0), (2, 1), (0, 3)])  10.3 us
    all_to_all x1, waiting for transfers between devices, program(): lax.all_to_all(blocks, PLANE, split_axis=0, concat_axis=0, tiled=True)  9.2 us
  transfers between devices with their start and end apart: 34, of which 19 were waited for; matrix products, arithmetic and copies ran while one was open for 2% of the time, Pallas kernels for 16%

profile of v1, /device:TPU:34, one launch (start us, length us, event | category | flops | bytes accessed | tf_op | source)
XLA Modules:
  0.0 215.6 jit_solution(6515878230866139740)
XLA Ops:
  1.2 4.8 %shard_map.102 = (bf16[8,3,112,128]{3,2,1,0:T(8,128)(2,1)}, bf16[8,3,112,128]{3,2,1,0:T(8,128)(2,1)}) custom-call(s32[5]{0:T(128)} %stack.23.where_ref.refs_0_, f32[3,64,1792]{2,1,0:T(8,128)} %gate_ref.1, f32[3,64,1792]{2,1,0:T(8,128)} %up_ref.1, f32[1,64]{1,0:T(1,128)} %bitcast.82), custom_call_target="tpu_custom_call" | custom-call | flops 3000000000 | bytes 6000000 | tf_op jit(solution)/shard_map/pallas_call | solution.py:25
  8.4 2.6 %maximum_select_fusion = bf16[16,3,112,128]{3,2,1,0:T(8,128)(2,1)} fusion(bf16[8,3,112,128]{3,2,1,0:T(8,128)(2,1)S(1)} %collective-permute-done, bf16[8,3,112,128]{3,2,1,0:T(8,128)(2,1)} %get-tuple-element.22, pred[]{:T(512)S(6)} %eq.23), kind=kLoop, calls=%fused_computation | loop fusion | flops 2064384 | bytes 2752513 | tf_op jit(solution)/shard_map/jit(_where)/select_n | solution.py:345
  11.0 7.6 %all-to-all-start = ((bf16[16,3,112,128]{3,2,1,0:T(8,128)(2,1)}), bf16[16,3,112,128]{3,2,1,0:T(8,128)(2,1)S(1)}, u32[]{:S(2)}, u32[]{:S(2)}) async-start(bf16[16,3,112,128]{3,2,1,0:T(8,128)(2,1)} %maximum_select_fusion), calls=%async_computation | async-start | bytes 2752512 | tf_op jit(solution)/shard_map/all_to_all | solution.py:348
  20.1 9.0 %shard_map.103 = (bf16[4,512,2048]{2,1,0:T(8,128)(2,1)}, f32[4,512,3]{2,1,0:T(8,128)}) custom-call(s32[5]{0:T(128)} %stack.23.where_ref.refs_0_, bf16[2,4,4,64,2048]{4,3,2,1,0:T(8,128)(2,1)} %bitcast.81, f32[2,4,4,64,3]{4,3,2,1,0:T(8,128)} %bitcast.75), custom_call_target="tpu_custom_call" | custom-call | flops 6000000000 | bytes 17000000 | tf_op jit(solution)/shard_map/pallas_call | solution.py:25
  29.1 9.2 %all-to-all-done = bf16[16,3,112,128]{3,2,1,0:T(8,128)(2,1)S(1)} async-done(((bf16[16,3,112,128]{3,2,1,0:T(8,128)(2,1)}), bf16[16,3,112,128]{3,2,1,0:T(8,128)(2,1)S(1)}, u32[]{:S(2)}, u32[]{:S(2)}) %all-to-all-start) | async-done | bytes 1376288 | tf_op jit(solution)/shard_map/all_to_all | solution.py:348
  38.4 4.0 %collective-permute-start.6 = (bf16[16,112,128]{2,1,0:T(8,128)(2,1)S(1)}, bf16[16,112,128]{2,1,0:T(8,128)(2,1)S(1)}, u32[]{:S(2)}, u32[]{:S(2)}) collective-permute-start(bf16[16,112,128]{2,1,0:T(8,128)(2,1)S(1)} %get-tuple-element.57.own_ref), channel_id=1, source_target_pairs={{32,64},{64,96},{96,0},{33,65},{65,97},{97,1},{34,66},{66,98},{98,... | collective-permute-start | bytes 1376264 | tf_op jit(solution)/shard_map/ppermute | solution.py:368
  44.9 5.3 %collective-permute-start.2 = (bf16[16,112,128]{2,1,0:T(8,128)(2,1)S(1)}, bf16[16,112,128]{2,1,0:T(8,128)(2,1)S(1)}, u32[]{:S(2)}, u32[]{:S(2)}) collective-permute-start(bf16[16,112,128]{2,1,0:T(8,128)(2,1)S(1)} %get-tuple-element.58.own_ref), channel_id=1, source_target_pairs={{32,64},{64,96},{96,0},{33,65},{65,97},{97,1},{34,66},{66,98},{98,... | collective-permute-start | bytes 1376264 | tf_op jit(solution)/shard_map/ppermute | solution.py:368
  52.2 15.8 %collective-permute-done.6.up_ref = bf16[16,112,128]{2,1,0:T(8,128)(2,1)S(1)} collective-permute-done((bf16[16,112,128]{2,1,0:T(8,128)(2,1)S(1)}, bf16[16,112,128]{2,1,0:T(8,128)(2,1)S(1)}, u32[]{:S(2)}, u32[]{:S(2)}) %collective-permute-start.6) | collective-permute-done | bytes 458784 | tf_op jit(solution)/shard_map/ppermute | solution.py:368
  68.0 3.6 %collective-permute-done.5.down_ref = bf16[16,112,128]{2,1,0:T(8,128)(2,1)S(1)} collective-permute-done((bf16[16,112,128]{2,1,0:T(8,128)(2,1)S(1)}, bf16[16,112,128]{2,1,0:T(8,128)(2,1)S(1)}, u32[]{:S(2)}, u32[]{:S(2)}) %collective-permute-start.5) | collective-permute-done | bytes 458784 | tf_op jit(solution)/shard_map/ppermute | solution.py:367
  74.5 4.4 %collective-permute-start.9 = (bf16[16,112,128]{2,1,0:T(8,128)(2,1)S(1)}, bf16[16,112,128]{2,1,0:T(8,128)(2,1)S(1)}, u32[]{:S(2)}, u32[]{:S(2)}) collective-permute-start(bf16[16,112,128]{2,1,0:T(8,128)(2,1)S(1)} %get-tuple-element.56.own_ref), channel_id=1, source_target_pairs={{32,0},{64,32},{0,96},{33,1},{65,33},{1,97},{34,2},{66,34},{2,98},... | collective-permute-start | bytes 1376264 | tf_op jit(solution)/shard_map/ppermute | solution.py:367
  85.3 4.1 %collective-permute-done.9.down_ref = bf16[16,112,128]{2,1,0:T(8,128)(2,1)S(1)} collective-permute-done((bf16[16,112,128]{2,1,0:T(8,128)(2,1)S(1)}, bf16[16,112,128]{2,1,0:T(8,128)(2,1)S(1)}, u32[]{:S(2)}, u32[]{:S(2)}) %collective-permute-start.9) | collective-permute-done | bytes 458784 | tf_op jit(solution)/shard_map/ppermute | solution.py:367
  90.8 6.9 %collective-permute-done.3.far_ref = bf16[16,112,128]{2,1,0:T(8,128)(2,1)S(1)} collective-permute-done((bf16[16,112,128]{2,1,0:T(8,128)(2,1)S(1)}, bf16[16,112,128]{2,1,0:T(8,128)(2,1)S(1)}, u32[]{:S(2)}, u32[]{:S(2)}) %collective-permute-start.3) | collective-permute-done | bytes 458784 | tf_op jit(solution)/shard_map/ppermute | solution.py:370
  98.8 7.4 %collective-permute-done.11.far_ref = bf16[16,112,128]{2,1,0:T(8,128)(2,1)S(1)} collective-permute-done((bf16[16,112,128]{2,1,0:T(8,128)(2,1)S(1)}, bf16[16,112,128]{2,1,0:T(8,128)(2,1)S(1)}, u32[]{:S(2)}, u32[]{:S(2)}) %collective-permute-start.11) | collective-permute-done | bytes 458784 | tf_op jit(solution)/shard_map/ppermute | solution.py:370
  107.4 3.9 %shard_map.108 = (bf16[3,224,2048]{2,1,0:T(8,128)(2,1)}, bf16[3,256,2048]{2,1,0:T(8,128)(2,1)S(1)}) custom-call(s32[5]{0:T(128)S(1)} %copy-done, bf16[3,224,512]{2,1,0:T(8,128)(2,1)S(1)} %convert_element_type.462.refs_0_, bf16[3,224,512]{2,1,0:T(8,128)(2,1)} %collective-permute-done.13.refs_1_, bf16[3,224,512]{2,1,0:T(8,128)(2,1)S(1)} %collective-permute-done.14.refs_2_, ...), custom_call_target="tpu_custom_call" | custom-call | flops 2000000000 | bytes 8000000 | tf_op jit(solution)/shard_map/pallas_call | solution.py:25
  113.0 7.9 %shard_map.110.refs_1_ = bf16[4,512,256]{2,1,0:T(8,128)(2,1)S(1)} custom-call(s32[5]{0:T(128)S(1)} %copy-done, bf16[4,512,2048]{2,1,0:T(8,128)(2,1)} %get-tuple-element.29.refs_1_.normed_ref, f32[4,512,3]{2,1,0:T(8,128)S(1)} %copy-done.2, bf16[2,112,2048]{2,1,0:T(8,128)(2,1)S(1)} %shard_map.105.refs_2_.refs_3_, ...), custom_call_target="tpu_custom_call" | custom-call | flops 4294967296 | bytes 12000000 | tf_op jit(solution)/shard_map/pallas_call | solution.py:25
  120.9 7.9 %shard_map.109.refs_0_ = bf16[4,512,256]{2,1,0:T(8,128)(2,1)S(1)} custom-call(s32[5]{0:T(128)S(1)} %copy-done, bf16[4,512,2048]{2,1,0:T(8,128)(2,1)} %get-tuple-element.29.refs_1_.normed_ref, f32[4,512,3]{2,1,0:T(8,128)S(1)} %copy-done.2, bf16[2,112,2048]{2,1,0:T(8,128)(2,1)S(1)} %shard_map.104.refs_0_.refs_3_, ...), custom_call_target="tpu_custom_call" | custom-call | flops 4294967296 | bytes 12000000 | tf_op jit(solution)/shard_map/pallas_call | solution.py:25
  129.9 18.5 %shard_map.111 = (bf16[1024,512]{1,0:T(8,128)(2,1)S(1)}, bf16[1024,512]{1,0:T(8,128)(2,1)S(1)}, bf16[1024,512]{1,0:T(8,128)(2,1)S(1)}, bf16[1024,512]{1,0:T(8,12...) custom-call(s32[5]{0:T(128)S(1)} %copy-done, ...), custom_call_target="tpu_custom_call" | custom-call | flops 10737418240 | bytes 25000000 | tf_op jit(solution)/shard_map/pallas_call | solution.py:25
  148.4 2.9 %collective-permute-start.20 = (bf16[1024,512]{1,0:T(8,128)(2,1)S(1)}, bf16[1024,512]{1,0:T(8,128)(2,1)S(1)}, u32[]{:S(2)}, u32[]{:S(2)}) collective-permute-start(bf16[1024,512]{1,0:T(8,128)(2,1)S(1)} %get-tuple-element.35), channel_id=1, source_target_pairs={{0,2},{2,0},{4,6},{6,4},{1,3},{3,1},{5,7},{7,5},{8,10},{10,8},{12,... | collective-permute-start | bytes 3145736 | tf_op jit(solution)/shard_map/ppermute | solution.py:277
  153.9 20.0 %collective-permute-done.16 = bf16[1024,512]{1,0:T(8,128)(2,1)S(1)} collective-permute-done((bf16[1024,512]{1,0:T(8,128)(2,1)S(1)}, bf16[1024,512]{1,0:T(8,128)(2,1)S(1)}, u32[]{:S(2)}, u32[]{:S(2)}) %collective-permute-start.16) | collective-permute-done | bytes 1048608 | tf_op jit(solution)/shard_map/ppermute | solution.py:277
  180.1 9.1 %collective-permute-done.17 = bf16[1,4,2,64,512]{4,3,2,1,0:T(8,128)(2,1)S(1)} collective-permute-done((bf16[1,4,2,64,512]{4,3,2,1,0:T(8,128)(2,1)S(1)}, bf16[1,4,2,64,512]{4,3,2,1,0:T(8,128)(2,1)S(1)}, u32[]{:S(2)}, u32[]{:S(2)}) %collective-permute-start.17) | collective-permute-done | bytes 524320 | tf_op jit(solution)/shard_map/ppermute | solution.py:277
  189.3 2.5 %collective-permute-start.18 = (bf16[1,2,2,64,512]{4,3,2,1,0:T(8,128)(2,1)S(1)}, bf16[1,2,2,64,512]{4,3,2,1,0:T(8,128)(2,1)S(1)}, u32[]{:S(2)}, u32[]{:S(2)}) collective-permute-start(bf16[1,2,2,64,512]{4,3,2,1,0:T(8,128)(2,1)S(1)} %pad_maximum_fusion), channel_id=1, source_target_pairs={{0,2},{2,0},{4,6},{6,4},{1,3},{3,1},{5,7},{7,5},{8,10},{10,8},{12,... | collective-permute-start | bytes 786440 | tf_op jit(solution)/shard_map/ppermute | solution.py:277
  193.9 3.3 %collective-permute-done.18 = bf16[1,2,2,64,512]{4,3,2,1,0:T(8,128)(2,1)S(1)} collective-permute-done((bf16[1,2,2,64,512]{4,3,2,1,0:T(8,128)(2,1)S(1)}, bf16[1,2,2,64,512]{4,3,2,1,0:T(8,128)(2,1)S(1)}, u32[]{:S(2)}, u32[]{:S(2)}) %collective-permute-start.18) | collective-permute-done | bytes 262176 | tf_op jit(solution)/shard_map/ppermute | solution.py:277
  208.5 3.3 %shard_map.107 = (bf16[3,224,2048]{2,1,0:T(8,128)(2,1)}, bf16[3,224,2048]{2,1,0:T(8,128)(2,1)}) custom-call(s32[5]{0:T(128)S(1)} %copy-done, bf16[2,112,2048]{2,1,0:T(8,128)(2,1)S(1)} %shard_map.104.refs_0_.refs_3_, bf16[2,112,2048]{2,1,0:T(8,128)(2,1)S(1)} %collective-permute-done.4.refs_1_.refs_4_, bf16[2,112,2048]{2,1,0:T(8,128)(2,1)S(1)} %shard_map.105.refs_2_.refs_3_, ...), custom_call_target="tpu_custom_call" | custom-call | flops 4000000000 | bytes 11000000 | tf_op jit(solution)/shard_map/pallas_call | solution.py:25
  211.8 3.0 %collective-permute-done.32 = bf16[64,2048]{1,0:T(8,128)(2,1)S(1)} collective-permute-done((bf16[64,2048]{1,0:T(8,128)(2,1)S(1)}, bf16[64,2048]{1,0:T(8,128)(2,1)S(1)}, u32[]{:S(2)}, u32[]{:S(2)}) %collective-permute-start.32) | collective-permute-done | bytes 262176 | tf_op jit(solution)/shard_map/ppermute | solution.py:277
  (115 shorter events, 47.2 us)
Async XLA Ops:
  11.0 27.3 %all-to-all-start = ((bf16[16,3,112,128]{3,2,1,0:T(8,128)(2,1)}), bf16[16,3,112,128]{3,2,1,0:T(8,128)(2,1)S(1)}, u32[]{:S(2)}, u32[]{:S(2)}) async-start(bf16[16,3,112,128]{3,2,1,0:T(8,128)(2,1)} %maximum_select_fusion), calls=%async_computation | async-start | bytes 2752512 | tf_op jit(solution)/shard_map/all_to_all | solution.py:348
  38.4 29.6 %collective-permute-start.6 = (bf16[16,112,128]{2,1,0:T(8,128)(2,1)S(1)}, bf16[16,112,128]{2,1,0:T(8,128)(2,1)S(1)}, u32[]{:S(2)}, u32[]{:S(2)}) collective-permute-start(bf16[16,112,128]{2,1,0:T(8,128)(2,1)S(1)} %get-tuple-element.57.own_ref), channel_id=1, source_target_pairs={{32,64},{64,96},{96,0},{33,65},{65,97},{97,1},{34,66},{66,98},{98,... | collective-permute-start | bytes 1376264 | tf_op jit(solution)/shard_map/ppermute | solution.py:368
  42.4 29.3 %collective-permute-start.5 = (bf16[16,112,128]{2,1,0:T(8,128)(2,1)S(1)}, bf16[16,112,128]{2,1,0:T(8,128)(2,1)S(1)}, u32[]{:S(2)}, u32[]{:S(2)}) collective-permute-start(bf16[16,112,128]{2,1,0:T(8,128)(2,1)S(1)} %get-tuple-element.57.own_ref), channel_id=1, source_target_pairs={{32,0},{64,32},{0,96},{33,1},{65,33},{1,97},{34,2},{66,34},{2,98},... | collective-permute-start | bytes 1376264 | tf_op jit(solution)/shard_map/ppermute | solution.py:367
  44.4 30.1 %collective-permute-start.13 = (bf16[3,224,512]{2,1,0:T(8,128)(2,1)S(1)}, bf16[3,224,512]{2,1,0:T(8,128)(2,1)}, u32[]{:S(2)}, u32[]{:S(2)}) collective-permute-start(bf16[3,224,512]{2,1,0:T(8,128)(2,1)S(1)} %convert_element_type.462.refs_0_), channel_id=1, source_target_pairs={{0,64},{64,0},{1,65},{65,1},{2,66},{66,2},{3,67},{67,3},{4,68},{68... | collective-permute-start | bytes 2064392 | tf_op jit(solution)/shard_map/ppermute | solution.py:277
  44.9 34.0 %collective-permute-start.2 = (bf16[16,112,128]{2,1,0:T(8,128)(2,1)S(1)}, bf16[16,112,128]{2,1,0:T(8,128)(2,1)S(1)}, u32[]{:S(2)}, u32[]{:S(2)}) collective-permute-start(bf16[16,112,128]{2,1,0:T(8,128)(2,1)S(1)} %get-tuple-element.58.own_ref), channel_id=1, source_target_pairs={{32,64},{64,96},{96,0},{33,65},{65,97},{97,1},{34,66},{66,98},{98,... | collective-permute-start | bytes 1376264 | tf_op jit(solution)/shard_map/ppermute | solution.py:368
  50.2 31.2 %collective-permute-start.1 = (bf16[16,112,128]{2,1,0:T(8,128)(2,1)S(1)}, bf16[16,112,128]{2,1,0:T(8,128)(2,1)S(1)}, u32[]{:S(2)}, u32[]{:S(2)}) collective-permute-start(bf16[16,112,128]{2,1,0:T(8,128)(2,1)S(1)} %get-tuple-element.58.own_ref), channel_id=1, source_target_pairs={{32,0},{64,32},{0,96},{33,1},{65,33},{1,97},{34,2},{66,34},{2,98},... | collective-permute-start | bytes 1376264 | tf_op jit(solution)/shard_map/ppermute | solution.py:367
  71.7 10.8 %collective-permute-start.7 = (bf16[16,112,128]{2,1,0:T(8,128)(2,1)S(1)}, bf16[16,112,128]{2,1,0:T(8,128)(2,1)S(1)}, u32[]{:S(2)}, u32[]{:S(2)}) collective-permute-start(bf16[16,112,128]{2,1,0:T(8,128)(2,1)S(1)} %broadcast_select_fusion.1), channel_id=1, source_target_pairs={{96,64},{0,32},{97,65},{1,33},{98,66},{2,34},{99,67},{3,35},{100,6... | collective-permute-start | bytes 1376264 | tf_op jit(solution)/shard_map/ppermute | solution.py:370
  73.0 12.3 %collective-permute-start.10 = (bf16[16,112,128]{2,1,0:T(8,128)(2,1)S(1)}, bf16[16,112,128]{2,1,0:T(8,128)(2,1)S(1)}, u32[]{:S(2)}, u32[]{:S(2)}) collective-permute-start(bf16[16,112,128]{2,1,0:T(8,128)(2,1)S(1)} %get-tuple-element.56.own_ref), channel_id=1, source_target_pairs={{32,64},{64,96},{96,0},{33,65},{65,97},{97,1},{34,66},{66,98},{98,... | collective-permute-start | bytes 1376264 | tf_op jit(solution)/shard_map/ppermute | solution.py:368
  74.5 15.0 %collective-permute-start.9 = (bf16[16,112,128]{2,1,0:T(8,128)(2,1)S(1)}, bf16[16,112,128]{2,1,0:T(8,128)(2,1)S(1)}, u32[]{:S(2)}, u32[]{:S(2)}) collective-permute-start(bf16[16,112,128]{2,1,0:T(8,128)(2,1)S(1)} %get-tuple-element.56.own_ref), channel_id=1, source_target_pairs={{32,0},{64,32},{0,96},{33,1},{65,33},{1,97},{34,2},{66,34},{2,98},... | collective-permute-start | bytes 1376264 | tf_op jit(solution)/shard_map/ppermute | solution.py:367
  78.9 28.5 %collective-permute-start.14 = (bf16[3,224,512]{2,1,0:T(8,128)(2,1)S(1)}, bf16[3,224,512]{2,1,0:T(8,128)(2,1)S(1)}, u32[]{:S(2)}, u32[]{:S(2)}) collective-permute-start(bf16[3,224,512]{2,1,0:T(8,128)(2,1)S(1)} %convert_element_type.462.refs_0_), channel_id=1, source_target_pairs={{0,1},{1,0},{2,3},{3,2},{4,5},{5,4},{6,7},{7,6},{8,9},{9,8},{10,11... | collective-permute-start | bytes 2064392 | tf_op jit(solution)/shard_map/ppermute | solution.py:277
  81.5 26.0 %collective-permute-start.15 = (bf16[3,224,512]{2,1,0:T(8,128)(2,1)}, bf16[3,224,512]{2,1,0:T(8,128)(2,1)S(1)}, u32[]{:S(2)}, u32[]{:S(2)}) collective-permute-start(bf16[3,224,512]{2,1,0:T(8,128)(2,1)} %collective-permute-done.13.refs_1_), channel_id=1, source_target_pairs={{0,1},{1,0},{2,3},{3,2},{4,5},{5,4},{6,7},{7,6},{8,9},{9,8},{10,11... | collective-permute-start | bytes 2064392 | tf_op jit(solution)/shard_map/ppermute | solution.py:277
  82.5 15.3 %collective-permute-start.3 = (bf16[16,112,128]{2,1,0:T(8,128)(2,1)S(1)}, bf16[16,112,128]{2,1,0:T(8,128)(2,1)S(1)}, u32[]{:S(2)}, u32[]{:S(2)}) collective-permute-start(bf16[16,112,128]{2,1,0:T(8,128)(2,1)S(1)} %broadcast_select_fusion.2), channel_id=1, source_target_pairs={{96,64},{0,32},{97,65},{1,33},{98,66},{2,34},{99,67},{3,35},{100,6... | collective-permute-start | bytes 1376264 | tf_op jit(solution)/shard_map/ppermute | solution.py:370
  85.3 27.6 %collective-permute-start.8 = (bf16[2,112,2048]{2,1,0:T(8,128)(2,1)S(1)}, bf16[2,112,2048]{2,1,0:T(8,128)(2,1)S(1)}, u32[]{:S(2)}, u32[]{:S(2)}) collective-permute-start(bf16[2,112,2048]{2,1,0:T(8,128)(2,1)S(1)} %shard_map.105.refs_2_.refs_3_), channel_id=1, source_target_pairs={{0,1},{1,0},{2,3},{3,2},{4,5},{5,4},{6,7},{7,6},{8,9},{9,8},{10,11... | collective-permute-start | bytes 2752520 | tf_op jit(solution)/shard_map/ppermute | solution.py:277
  89.5 16.7 %collective-permute-start.11 = (bf16[16,112,128]{2,1,0:T(8,128)(2,1)S(1)}, bf16[16,112,128]{2,1,0:T(8,128)(2,1)S(1)}, u32[]{:S(2)}, u32[]{:S(2)}) collective-permute-start(bf16[16,112,128]{2,1,0:T(8,128)(2,1)S(1)} %broadcast_select_fusion), channel_id=1, source_target_pairs={{96,64},{0,32},{97,65},{1,33},{98,66},{2,34},{99,67},{3,35},{100,6... | collective-permute-start | bytes 1376264 | tf_op jit(solution)/shard_map/ppermute | solution.py:370
  98.7 22.2 %collective-permute-start.4 = (bf16[2,112,2048]{2,1,0:T(8,128)(2,1)S(1)}, bf16[2,112,2048]{2,1,0:T(8,128)(2,1)S(1)}, u32[]{:S(2)}, u32[]{:S(2)}) collective-permute-start(bf16[2,112,2048]{2,1,0:T(8,128)(2,1)S(1)} %shard_map.104.refs_0_.refs_3_), channel_id=1, source_target_pairs={{0,1},{1,0},{2,3},{3,2},{4,5},{5,4},{6,7},{7,6},{8,9},{9,8},{10,11... | collective-permute-start | bytes 2752520 | tf_op jit(solution)/shard_map/ppermute | solution.py:277
  107.1 22.7 %collective-permute-start.12 = (bf16[2,112,2048]{2,1,0:T(8,128)(2,1)S(1)}, bf16[2,112,2048]{2,1,0:T(8,128)(2,1)S(1)}, u32[]{:S(2)}, u32[]{:S(2)}) collective-permute-start(bf16[2,112,2048]{2,1,0:T(8,128)(2,1)S(1)} %shard_map.106.refs_4_.refs_2_), channel_id=1, source_target_pairs={{0,1},{1,0},{2,3},{3,2},{4,5},{5,4},{6,7},{7,6},{8,9},{9,8},{10,11... | collective-permute-start | bytes 2752520 | tf_op jit(solution)/shard_map/ppermute | solution.py:277
  148.3 25.6 %collective-permute-start.16 = (bf16[1024,512]{1,0:T(8,128)(2,1)S(1)}, bf16[1024,512]{1,0:T(8,128)(2,1)S(1)}, u32[]{:S(2)}, u32[]{:S(2)}) collective-permute-start(bf16[1024,512]{1,0:T(8,128)(2,1)S(1)} %get-tuple-element.33), channel_id=1, source_target_pairs={{0,8},{8,0},{16,24},{24,16},{1,9},{9,1},{17,25},{25,17},{2,10},{10... | collective-permute-start | bytes 3145736 | tf_op jit(solution)/shard_map/ppermute | solution.py:277
  148.4 27.0 %collective-permute-start.20 = (bf16[1024,512]{1,0:T(8,128)(2,1)S(1)}, bf16[1024,512]{1,0:T(8,128)(2,1)S(1)}, u32[]{:S(2)}, u32[]{:S(2)}) collective-permute-start(bf16[1024,512]{1,0:T(8,128)(2,1)S(1)} %get-tuple-element.35), channel_id=1, source_target_pairs={{0,2},{2,0},{4,6},{6,4},{1,3},{3,1},{5,7},{7,5},{8,10},{10,8},{12,... | collective-permute-start | bytes 3145736 | tf_op jit(solution)/shard_map/ppermute | solution.py:277
  151.3 27.0 %collective-permute-start.24 = (bf16[1024,512]{1,0:T(8,128)(2,1)}, bf16[1024,512]{1,0:T(8,128)(2,1)S(1)}, u32[]{:S(2)}, u32[]{:S(2)}) collective-permute-start(bf16[1024,512]{1,0:T(8,128)(2,1)} %get-tuple-element.37), channel_id=1, source_target_pairs={{0,24},{8,16},{16,8},{24,0},{1,25},{9,17},{17,9},{25,1},{2,26},{10... | collective-permute-start | bytes 3145736 | tf_op jit(solution)/shard_map/ppermute | solution.py:277
  152.6 27.1 %collective-permute-start.28 = (bf16[1024,512]{1,0:T(8,128)(2,1)}, bf16[1024,512]{1,0:T(8,128)(2,1)S(1)}, u32[]{:S(2)}, u32[]{:S(2)}) collective-permute-start(bf16[1024,512]{1,0:T(8,128)(2,1)} %get-tuple-element.39), channel_id=1, source_target_pairs={{0,6},{2,4},{4,2},{6,0},{1,7},{3,5},{5,3},{7,1},{8,14},{10,12},{12... | collective-permute-start | bytes 3145736 | tf_op jit(solution)/shard_map/ppermute | solution.py:277
  174.1 15.1 %collective-permute-start.17 = (bf16[1,4,2,64,512]{4,3,2,1,0:T(8,128)(2,1)S(1)}, bf16[1,4,2,64,512]{4,3,2,1,0:T(8,128)(2,1)S(1)}, u32[]{:S(2)}, u32[]{:S(2)}) collective-permute-start(bf16[1,4,2,64,512]{4,3,2,1,0:T(8,128)(2,1)S(1)} %bitcast.79), channel_id=1, source_target_pairs={{0,24},{8,16},{16,8},{24,0},{1,25},{9,17},{17,9},{25,1},{2,26},{10... | collective-permute-start | bytes 1572872 | tf_op jit(solution)/shard_map/ppermute | solution.py:277
  175.6 16.2 %collective-permute-start.21 = (bf16[1,4,2,64,512]{4,3,2,1,0:T(8,128)(2,1)S(1)}, bf16[1,4,2,64,512]{4,3,2,1,0:T(8,128)(2,1)S(1)}, u32[]{:S(2)}, u32[]{:S(2)}) collective-permute-start(bf16[1,4,2,64,512]{4,3,2,1,0:T(8,128)(2,1)S(1)} %bitcast.78), channel_id=1, source_target_pairs={{0,6},{2,4},{4,2},{6,0},{1,7},{3,5},{5,3},{7,1},{8,14},{10,12},{12... | collective-permute-start | bytes 1572872 | tf_op jit(solution)/shard_map/ppermute | solution.py:277
  178.5 13.6 %collective-permute-start.25 = (bf16[1,4,2,64,512]{4,3,2,1,0:T(8,128)(2,1)S(1)}, bf16[1,4,2,64,512]{4,3,2,1,0:T(8,128)(2,1)S(1)}, u32[]{:S(2)}, u32[]{:S(2)}) collective-permute-start(bf16[1,4,2,64,512]{4,3,2,1,0:T(8,128)(2,1)S(1)} %bitcast.77), channel_id=1, source_target_pairs={{0,8},{8,0},{16,24},{24,16},{1,9},{9,1},{17,25},{25,17},{2,10},{10... | collective-permute-start | bytes 1572872 | tf_op jit(solution)/shard_map/ppermute | solution.py:277
  179.8 12.5 %collective-permute-start.29 = (bf16[1,4,2,64,512]{4,3,2,1,0:T(8,128)(2,1)S(1)}, bf16[1,4,2,64,512]{4,3,2,1,0:T(8,128)(2,1)S(1)}, u32[]{:S(2)}, u32[]{:S(2)}) collective-permute-start(bf16[1,4,2,64,512]{4,3,2,1,0:T(8,128)(2,1)S(1)} %bitcast.76), channel_id=1, source_target_pairs={{0,2},{2,0},{4,6},{6,4},{1,3},{3,1},{5,7},{7,5},{8,10},{10,8},{12,... | collective-permute-start | bytes 1572872 | tf_op jit(solution)/shard_map/ppermute | solution.py:277
  (20 other events, 148.4 us)

commit v2 on v1

--- a/solution.py
+++ b/solution.py
@@ -11,6 +11,7 @@
 Z = ("gr", "fs_0")
 UNITS = 256
 MIB = 1024 * 1024
+LAST_VMEM = 40
 
 
 COLORS = (
@@ -214,19 +215,21 @@
     )
 
 
-def last_kernel(where_ref, normed_ref, mix_ref, *refs):
-    earlier, (own_ref, other_ref, down_ref) = refs[:2], refs[2:5]
-    outs, (gate, up) = refs[5:-2], refs[-2:]
+def last_kernel(where_ref, normed_ref, mix_ref, early_ref, *refs):
+    sides, down_ref = (refs[0:2], refs[2:4]), refs[4]
+    outs, weights = refs[5:-4], (refs[-4:-2], refs[-2:])
     yy = pl.program_id(0)
 
     @pl.when(yy == 0)
     def _():
-        fill(where_ref, own_ref, other_ref, gate, up)
-
-    experts = len(earlier) + 1
-    mix = mix_ref[0, :, experts - 1 : experts]
-    hidden = hidden_of(normed_ref[0], mix, gate[...], up[...])
-    rows = jnp.concatenate([r[0] for r in earlier] + [hidden], axis=1)
+        for side, weight in zip(sides, weights):
+            fill(where_ref, *side, *weight)
+
+    hidden = [early_ref[0]]
+    for expert, (gate, up) in enumerate(weights, 1):
+        mix = mix_ref[0, :, expert : expert + 1]
+        hidden.append(hidden_of(normed_ref[0], mix, gate[...], up[...]))
+    rows = jnp.concatenate(hidden, axis=1)
     block = rows.shape[0]
     ys = pl.num_programs(0)
     width = outs[0].shape[1]
@@ -256,19 +259,19 @@
                 ref[to, :] = product[xx * part : (xx + 1) * part]
 
 
-def last(where, normed, mix, earlier, own, other, down):
+def last(where, normed, mix, early, sides, down):
     ys, rows, width = normed.shape
     half = (ys * rows // 2, width // len(COLORS))
     at = lambda i, w: (i, 0, 0)
-    side = whole(own.shape)
+    side = whole(sides[0].shape)
     weight = pltpu.VMEM((UNITS, width), jnp.bfloat16)
     return call(
         last_kernel, (ys,),
         [pl.BlockSpec((1, rows, width), at), pl.BlockSpec((1, rows, mix.shape[-1]), at)]
-        + [pl.BlockSpec((1, rows, UNITS), at)] * 2 + [side, side, whole(down.shape)],
+        + [pl.BlockSpec((1, rows, UNITS), at)] + [side] * 4 + [whole(down.shape)],
         [whole(half)] * (2 * len(COLORS)), [shaped(*half)] * (2 * len(COLORS)),
-        (where, normed, mix, *earlier, own, other, down), 10 * ys * rows * width * UNITS, 25e6,
-        scratch=(weight, weight), vmem=48,
+        (where, normed, mix, early, *sides, down), 14 * ys * rows * width * UNITS, 25e6,
+        scratch=(weight,) * 4, vmem=LAST_VMEM,
     )
 
 
@@ -361,7 +364,7 @@
     down_out, down_padded = join(where, quarters)
     mine, normed = lax.optimization_barrier((mine, normed))
 
-    sides, hidden = [], []
+    sides = []
     for e in range(experts):
         piece = mine[:, e]
         below = lax.ppermute(piece, Z, [(1, 0), (2, 1), (0, 3)])
@@ -370,11 +373,8 @@
         far = lax.ppermute(passed, Z, [(3, 2), (0, 1)])
         own = unpack(where, (piece, below, above, far))
         sides += [own, other_core(own)]
-        if e < experts - 1:
-            hidden.append(hidden_units(where, normed, mix, sides[-2], sides[-1], e))
-
-    flat_down = down_padded.reshape(-1, width)
-    outs = last(where, normed, mix, hidden, sides[-2], sides[-1], flat_down)
+    early = hidden_units(where, normed, mix, sides[0], sides[1], 0)
+    outs = last(where, normed, mix, early, sides[2:], down_padded.reshape(-1, width))
     sums = []
     for color, exchanges in enumerate(COLORS):
         sums.append(Sums(outs[2 * color], outs[2 * color + 1], exchanges))

time: 216 us -> 215 us (level)
  the two profiles are of different devices: /device:TPU:34 before, /device:TPU:66 now
where the time goes in v2:
time: 215 us; the launch traced here: 214 us
  waiting for transfers between devices  90.6 us (42%)
  starting transfers between devices  56.9 us (26%)
  Pallas kernels  54.9 us (26%)
  other arithmetic  5.49 us (3%)
  local copies, waits for them, and re-layouts  5.27 us (2%)
    pallas_call x9, Pallas kernels, call(): pl.pallas_call(kernel, out_shape=out_shape, grid_spec=pltpu.PrefetchScala...  54.9 us
    ppermute x24, waiting for transfers between devices, swap(): return lax.ppermute(array, axis, [(i, i ^ mask) for i in range(peers)])  40.3 us
    ppermute x24, starting transfers between devices, swap(): return lax.ppermute(array, axis, [(i, i ^ mask) for i in range(peers)])  27.7 us
    ppermute x3, waiting for transfers between devices, program(): above = lax.ppermute(piece, Z, [(1, 2), (2, 3), (3, 0)])  24 us
    ppermute x3, waiting for transfers between devices, program(): far = lax.ppermute(passed, Z, [(3, 2), (0, 1)])  15.7 us
    ppermute x3, starting transfers between devices, program(): below = lax.ppermute(piece, Z, [(1, 0), (2, 1), (0, 3)])  10.3 us
    all_to_all x1, waiting for transfers between devices, program(): lax.all_to_all(blocks, PLANE, split_axis=0, concat_axis=0, tiled=True)  9.2 us
    all_to_all x1, starting transfers between devices, program(): lax.all_to_all(blocks, PLANE, split_axis=0, concat_axis=0, tiled=True)  7.61 us
  transfers between devices with their start and end apart: 34, of which 19 were waited for; matrix products, arithmetic and copies ran while one was open for 2% of the time, Pallas kernels for 13%

profile of v2, /device:TPU:66, one launch (start us, length us, event | category | flops | bytes accessed | tf_op | source)
XLA Modules:
  0.0 214.2 jit_solution(4395055309740234009)
XLA Ops:
  1.2 4.8 %shard_map.102 = (bf16[8,3,112,128]{3,2,1,0:T(8,128)(2,1)}, bf16[8,3,112,128]{3,2,1,0:T(8,128)(2,1)}) custom-call(s32[5]{0:T(128)} %stack.23.where_ref.refs_0_, f32[3,64,1792]{2,1,0:T(8,128)} %gate_ref.1, f32[3,64,1792]{2,1,0:T(8,128)} %up_ref.1, f32[1,64]{1,0:T(1,128)} %bitcast.82), custom_call_target="tpu_custom_call" | custom-call | flops 3000000000 | bytes 6000000 | tf_op jit(solution)/shard_map/pallas_call | solution.py:26
  11.0 7.6 %all-to-all-start = ((bf16[16,3,112,128]{3,2,1,0:T(8,128)(2,1)}), bf16[16,3,112,128]{3,2,1,0:T(8,128)(2,1)S(1)}, u32[]{:S(2)}, u32[]{:S(2)}) async-start(bf16[16,3,112,128]{3,2,1,0:T(8,128)(2,1)} %maximum_select_fusion), calls=%async_computation | async-start | bytes 2752512 | tf_op jit(solution)/shard_map/all_to_all | solution.py:351
  20.1 9.0 %shard_map.103 = (bf16[4,512,2048]{2,1,0:T(8,128)(2,1)}, f32[4,512,3]{2,1,0:T(8,128)}) custom-call(s32[5]{0:T(128)} %stack.23.where_ref.refs_0_, bf16[2,4,4,64,2048]{4,3,2,1,0:T(8,128)(2,1)} %bitcast.81, f32[2,4,4,64,3]{4,3,2,1,0:T(8,128)} %bitcast.75), custom_call_target="tpu_custom_call" | custom-call | flops 6000000000 | bytes 17000000 | tf_op jit(solution)/shard_map/pallas_call | solution.py:26
  29.1 9.2 %all-to-all-done = bf16[16,3,112,128]{3,2,1,0:T(8,128)(2,1)S(1)} async-done(((bf16[16,3,112,128]{3,2,1,0:T(8,128)(2,1)}), bf16[16,3,112,128]{3,2,1,0:T(8,128)(2,1)S(1)}, u32[]{:S(2)}, u32[]{:S(2)}) %all-to-all-start) | async-done | bytes 1376288 | tf_op jit(solution)/shard_map/all_to_all | solution.py:351
  39.1 3.5 %collective-permute-start.2 = (bf16[16,112,128]{2,1,0:T(8,128)(2,1)}, bf16[16,112,128]{2,1,0:T(8,128)(2,1)S(1)}, u32[]{:S(2)}, u32[]{:S(2)}) collective-permute-start(bf16[16,112,128]{2,1,0:T(8,128)(2,1)} %get-tuple-element.58.own_ref), channel_id=1, source_target_pairs={{32,64},{64,96},{96,0},{33,65},{65,97},{97,1},{34,66},{66,98},{98,... | collective-permute-start | bytes 1376264 | tf_op jit(solution)/shard_map/ppermute | solution.py:371
  47.0 4.0 %collective-permute-start.5 = (bf16[16,112,128]{2,1,0:T(8,128)(2,1)S(1)}, bf16[16,112,128]{2,1,0:T(8,128)(2,1)S(1)}, u32[]{:S(2)}, u32[]{:S(2)}) collective-permute-start(bf16[16,112,128]{2,1,0:T(8,128)(2,1)S(1)} %get-tuple-element.57.own_ref), channel_id=1, source_target_pairs={{32,0},{64,32},{0,96},{33,1},{65,33},{1,97},{34,2},{66,34},{2,98},... | collective-permute-start | bytes 1376264 | tf_op jit(solution)/shard_map/ppermute | solution.py:370
  51.0 2.9 %collective-permute-start.13 = (bf16[3,224,512]{2,1,0:T(8,128)(2,1)S(1)}, bf16[3,224,512]{2,1,0:T(8,128)(2,1)}, u32[]{:S(2)}, u32[]{:S(2)}) collective-permute-start(bf16[3,224,512]{2,1,0:T(8,128)(2,1)S(1)} %convert_element_type.462.refs_0_), channel_id=1, source_target_pairs={{0,64},{64,0},{1,65},{65,1},{2,66},{66,2},{3,67},{67,3},{4,68},{68... | collective-permute-start | bytes 2064392 | tf_op jit(solution)/shard_map/ppermute | solution.py:280
  53.9 15.5 %collective-permute-done.2.up_ref = bf16[16,112,128]{2,1,0:T(8,128)(2,1)S(1)} collective-permute-done((bf16[16,112,128]{2,1,0:T(8,128)(2,1)}, bf16[16,112,128]{2,1,0:T(8,128)(2,1)S(1)}, u32[]{:S(2)}, u32[]{:S(2)}) %collective-permute-start.2) | collective-permute-done | bytes 458784 | tf_op jit(solution)/shard_map/ppermute | solution.py:371
  71.3 4.0 %collective-permute-start.9 = (bf16[16,112,128]{2,1,0:T(8,128)(2,1)S(1)}, bf16[16,112,128]{2,1,0:T(8,128)(2,1)S(1)}, u32[]{:S(2)}, u32[]{:S(2)}) collective-permute-start(bf16[16,112,128]{2,1,0:T(8,128)(2,1)S(1)} %get-tuple-element.56.own_ref), channel_id=1, source_target_pairs={{32,0},{64,32},{0,96},{33,1},{65,33},{1,97},{34,2},{66,34},{2,98},... | collective-permute-start | bytes 1376264 | tf_op jit(solution)/shard_map/ppermute | solution.py:370
  75.3 3.9 %collective-permute-done.6.up_ref = bf16[16,112,128]{2,1,0:T(8,128)(2,1)S(1)} collective-permute-done((bf16[16,112,128]{2,1,0:T(8,128)(2,1)S(1)}, bf16[16,112,128]{2,1,0:T(8,128)(2,1)S(1)}, u32[]{:S(2)}, u32[]{:S(2)}) %collective-permute-start.6) | collective-permute-done | bytes 458784 | tf_op jit(solution)/shard_map/ppermute | solution.py:371
  82.0 4.7 %collective-permute-done.10.up_ref = bf16[16,112,128]{2,1,0:T(8,128)(2,1)S(1)} collective-permute-done((bf16[16,112,128]{2,1,0:T(8,128)(2,1)S(1)}, bf16[16,112,128]{2,1,0:T(8,128)(2,1)S(1)}, u32[]{:S(2)}, u32[]{:S(2)}) %collective-permute-start.10) | collective-permute-done | bytes 458784 | tf_op jit(solution)/shard_map/ppermute | solution.py:371
  89.3 5.2 %collective-permute-done.3.far_ref = bf16[16,112,128]{2,1,0:T(8,128)(2,1)S(1)} collective-permute-done((bf16[16,112,128]{2,1,0:T(8,128)(2,1)S(1)}, bf16[16,112,128]{2,1,0:T(8,128)(2,1)S(1)}, u32[]{:S(2)}, u32[]{:S(2)}) %collective-permute-start.3) | collective-permute-done | bytes 458784 | tf_op jit(solution)/shard_map/ppermute | solution.py:373
  97.1 6.6 %collective-permute-done.7.far_ref = bf16[16,112,128]{2,1,0:T(8,128)(2,1)S(1)} collective-permute-done((bf16[16,112,128]{2,1,0:T(8,128)(2,1)S(1)}, bf16[16,112,128]{2,1,0:T(8,128)(2,1)S(1)}, u32[]{:S(2)}, u32[]{:S(2)}) %collective-permute-start.7) | collective-permute-done | bytes 458784 | tf_op jit(solution)/shard_map/ppermute | solution.py:373
  104.7 3.9 %collective-permute-done.11.far_ref = bf16[16,112,128]{2,1,0:T(8,128)(2,1)S(1)} collective-permute-done((bf16[16,112,128]{2,1,0:T(8,128)(2,1)S(1)}, bf16[16,112,128]{2,1,0:T(8,128)(2,1)S(1)}, u32[]{:S(2)}, u32[]{:S(2)}) %collective-permute-start.11) | collective-permute-done | bytes 458784 | tf_op jit(solution)/shard_map/ppermute | solution.py:373
  109.9 3.9 %shard_map.108 = (bf16[3,224,2048]{2,1,0:T(8,128)(2,1)}, bf16[3,256,2048]{2,1,0:T(8,128)(2,1)S(1)}) custom-call(s32[5]{0:T(128)S(1)} %copy-done, bf16[3,224,512]{2,1,0:T(8,128)(2,1)S(1)} %convert_element_type.462.refs_0_, bf16[3,224,512]{2,1,0:T(8,128)(2,1)} %collective-permute-done.13.refs_1_, bf16[3,224,512]{2,1,0:T(8,128)(2,1)S(1)} %collective-permute-done.14.refs_2_, ...), custom_call_target="tpu_custom_call" | custom-call | flops 2000000000 | bytes 8000000 | tf_op jit(solution)/shard_map/pallas_call | solution.py:26
  113.8 8.8 %shard_map.109.early_ref = bf16[4,512,256]{2,1,0:T(8,128)(2,1)S(1)} custom-call(s32[5]{0:T(128)S(1)} %copy-done, bf16[4,512,2048]{2,1,0:T(8,128)(2,1)} %get-tuple-element.29.refs_1_.normed_ref, f32[4,512,3]{2,1,0:T(8,128)S(1)} %copy-done.2, bf16[2,112,2048]{2,1,0:T(8,128)(2,1)S(1)} %shard_map.104.refs_0_.refs_3_, ...), custom_call_target="tpu_custom_call" | custom-call | flops 4294967296 | bytes 12000000 | tf_op jit(solution)/shard_map/pallas_call | solution.py:26
  124.8 21.2 %shard_map.110 = (bf16[1024,512]{1,0:T(8,128)(2,1)S(1)}, bf16[1024,512]{1,0:T(8,128)(2,1)S(1)}, bf16[1024,512]{1,0:T(8,128)(2,1)S(1)}, bf16[1024,512]{1,0:T(8,12...) custom-call(s32[5]{0:T(128)S(1)} %copy-done, ...), custom_call_target="tpu_custom_call" | custom-call | flops 15032385536 | bytes 25000000 | tf_op jit(solution)/shard_map/pallas_call | solution.py:26
  146.3 2.7 %collective-permute-start.20 = (bf16[1024,512]{1,0:T(8,128)(2,1)S(1)}, bf16[1024,512]{1,0:T(8,128)(2,1)S(1)}, u32[]{:S(2)}, u32[]{:S(2)}) collective-permute-start(bf16[1024,512]{1,0:T(8,128)(2,1)S(1)} %get-tuple-element.35), channel_id=1, source_target_pairs={{0,2},{2,0},{4,6},{6,4},{1,3},{3,1},{5,7},{7,5},{8,10},{10,8},{12,... | collective-permute-start | bytes 3145736 | tf_op jit(solution)/shard_map/ppermute | solution.py:280
  152.5 19.2 %collective-permute-done.16 = bf16[1024,512]{1,0:T(8,128)(2,1)S(1)} collective-permute-done((bf16[1024,512]{1,0:T(8,128)(2,1)S(1)}, bf16[1024,512]{1,0:T(8,128)(2,1)S(1)}, u32[]{:S(2)}, u32[]{:S(2)}) %collective-permute-start.16) | collective-permute-done | bytes 1048608 | tf_op jit(solution)/shard_map/ppermute | solution.py:280
  173.5 4.1 %collective-permute-start.21 = (bf16[1,4,2,64,512]{4,3,2,1,0:T(8,128)(2,1)S(1)}, bf16[1,4,2,64,512]{4,3,2,1,0:T(8,128)(2,1)S(1)}, u32[]{:S(2)}, u32[]{:S(2)}) collective-permute-start(bf16[1,4,2,64,512]{4,3,2,1,0:T(8,128)(2,1)S(1)} %bitcast.78), channel_id=1, source_target_pairs={{0,6},{2,4},{4,2},{6,0},{1,7},{3,5},{5,3},{7,1},{8,14},{10,12},{12... | collective-permute-start | bytes 1572872 | tf_op jit(solution)/shard_map/ppermute | solution.py:280
  178.4 8.3 %collective-permute-done.17 = bf16[1,4,2,64,512]{4,3,2,1,0:T(8,128)(2,1)S(1)} collective-permute-done((bf16[1,4,2,64,512]{4,3,2,1,0:T(8,128)(2,1)S(1)}, bf16[1,4,2,64,512]{4,3,2,1,0:T(8,128)(2,1)S(1)}, u32[]{:S(2)}, u32[]{:S(2)}) %collective-permute-start.17) | collective-permute-done | bytes 524320 | tf_op jit(solution)/shard_map/ppermute | solution.py:280
  186.8 2.7 %collective-permute-start.18 = (bf16[1,2,2,64,512]{4,3,2,1,0:T(8,128)(2,1)S(1)}, bf16[1,2,2,64,512]{4,3,2,1,0:T(8,128)(2,1)S(1)}, u32[]{:S(2)}, u32[]{:S(2)}) collective-permute-start(bf16[1,2,2,64,512]{4,3,2,1,0:T(8,128)(2,1)S(1)} %pad_maximum_fusion), channel_id=1, source_target_pairs={{0,2},{2,0},{4,6},{6,4},{1,3},{3,1},{5,7},{7,5},{8,10},{10,8},{12,... | collective-permute-start | bytes 786440 | tf_op jit(solution)/shard_map/ppermute | solution.py:280
  207.1 3.3 %shard_map.107 = (bf16[3,224,2048]{2,1,0:T(8,128)(2,1)}, bf16[3,224,2048]{2,1,0:T(8,128)(2,1)}) custom-call(s32[5]{0:T(128)S(1)} %copy-done, bf16[2,112,2048]{2,1,0:T(8,128)(2,1)S(1)} %shard_map.104.refs_0_.refs_3_, bf16[2,112,2048]{2,1,0:T(8,128)(2,1)S(1)} %collective-permute-done.4.refs_1_.refs_4_, bf16[2,112,2048]{2,1,0:T(8,128)(2,1)S(1)} %shard_map.105.refs_2_.refs_0_, ...), custom_call_target="tpu_custom_call" | custom-call | flops 4000000000 | bytes 11000000 | tf_op jit(solution)/shard_map/pallas_call | solution.py:26
  210.4 3.0 %collective-permute-done.32 = bf16[64,2048]{1,0:T(8,128)(2,1)S(1)} collective-permute-done((bf16[64,2048]{1,0:T(8,128)(2,1)S(1)}, bf16[64,2048]{1,0:T(8,128)(2,1)S(1)}, u32[]{:S(2)}, u32[]{:S(2)}) %collective-permute-start.32) | collective-permute-done | bytes 262176 | tf_op jit(solution)/shard_map/ppermute | solution.py:280
  (112 shorter events, 51.2 us)
Async XLA Ops:
  11.0 27.3 %all-to-all-start = ((bf16[16,3,112,128]{3,2,1,0:T(8,128)(2,1)}), bf16[16,3,112,128]{3,2,1,0:T(8,128)(2,1)S(1)}, u32[]{:S(2)}, u32[]{:S(2)}) async-start(bf16[16,3,112,128]{3,2,1,0:T(8,128)(2,1)} %maximum_select_fusion), calls=%async_computation | async-start | bytes 2752512 | tf_op jit(solution)/shard_map/all_to_all | solution.py:351
  39.1 30.2 %collective-permute-start.2 = (bf16[16,112,128]{2,1,0:T(8,128)(2,1)}, bf16[16,112,128]{2,1,0:T(8,128)(2,1)S(1)}, u32[]{:S(2)}, u32[]{:S(2)}) collective-permute-start(bf16[16,112,128]{2,1,0:T(8,128)(2,1)} %get-tuple-element.58.own_ref), channel_id=1, source_target_pairs={{32,64},{64,96},{96,0},{33,65},{65,97},{97,1},{34,66},{66,98},{98,... | collective-permute-start | bytes 1376264 | tf_op jit(solution)/shard_map/ppermute | solution.py:371
  42.7 28.6 %collective-permute-start.1 = (bf16[16,112,128]{2,1,0:T(8,128)(2,1)}, bf16[16,112,128]{2,1,0:T(8,128)(2,1)S(1)}, u32[]{:S(2)}, u32[]{:S(2)}) collective-permute-start(bf16[16,112,128]{2,1,0:T(8,128)(2,1)} %get-tuple-element.58.own_ref), channel_id=1, source_target_pairs={{32,0},{64,32},{0,96},{33,1},{65,33},{1,97},{34,2},{66,34},{2,98},... | collective-permute-start | bytes 1376264 | tf_op jit(solution)/shard_map/ppermute | solution.py:370
  45.0 34.2 %collective-permute-start.6 = (bf16[16,112,128]{2,1,0:T(8,128)(2,1)S(1)}, bf16[16,112,128]{2,1,0:T(8,128)(2,1)S(1)}, u32[]{:S(2)}, u32[]{:S(2)}) collective-permute-start(bf16[16,112,128]{2,1,0:T(8,128)(2,1)S(1)} %get-tuple-element.57.own_ref), channel_id=1, source_target_pairs={{32,64},{64,96},{96,0},{33,65},{65,97},{97,1},{34,66},{66,98},{98,... | collective-permute-start | bytes 1376264 | tf_op jit(solution)/shard_map/ppermute | solution.py:371
  47.0 33.7 %collective-permute-start.5 = (bf16[16,112,128]{2,1,0:T(8,128)(2,1)S(1)}, bf16[16,112,128]{2,1,0:T(8,128)(2,1)S(1)}, u32[]{:S(2)}, u32[]{:S(2)}) collective-permute-start(bf16[16,112,128]{2,1,0:T(8,128)(2,1)S(1)} %get-tuple-element.57.own_ref), channel_id=1, source_target_pairs={{32,0},{64,32},{0,96},{33,1},{65,33},{1,97},{34,2},{66,34},{2,98},... | collective-permute-start | bytes 1376264 | tf_op jit(solution)/shard_map/ppermute | solution.py:370
  51.0 46.0 %collective-permute-start.13 = (bf16[3,224,512]{2,1,0:T(8,128)(2,1)S(1)}, bf16[3,224,512]{2,1,0:T(8,128)(2,1)}, u32[]{:S(2)}, u32[]{:S(2)}) collective-permute-start(bf16[3,224,512]{2,1,0:T(8,128)(2,1)S(1)} %convert_element_type.462.refs_0_), channel_id=1, source_target_pairs={{0,64},{64,0},{1,65},{65,1},{2,66},{66,2},{3,67},{67,3},{4,68},{68... | collective-permute-start | bytes 2064392 | tf_op jit(solution)/shard_map/ppermute | solution.py:280
  69.4 17.3 %collective-permute-start.10 = (bf16[16,112,128]{2,1,0:T(8,128)(2,1)S(1)}, bf16[16,112,128]{2,1,0:T(8,128)(2,1)S(1)}, u32[]{:S(2)}, u32[]{:S(2)}) collective-permute-start(bf16[16,112,128]{2,1,0:T(8,128)(2,1)S(1)} %get-tuple-element.56.own_ref), channel_id=1, source_target_pairs={{32,64},{64,96},{96,0},{33,65},{65,97},{97,1},{34,66},{66,98},{98,... | collective-permute-start | bytes 1376264 | tf_op jit(solution)/shard_map/ppermute | solution.py:371
  71.3 16.6 %collective-permute-start.9 = (bf16[16,112,128]{2,1,0:T(8,128)(2,1)S(1)}, bf16[16,112,128]{2,1,0:T(8,128)(2,1)S(1)}, u32[]{:S(2)}, u32[]{:S(2)}) collective-permute-start(bf16[16,112,128]{2,1,0:T(8,128)(2,1)S(1)} %get-tuple-element.56.own_ref), channel_id=1, source_target_pairs={{32,0},{64,32},{0,96},{33,1},{65,33},{1,97},{34,2},{66,34},{2,98},... | collective-permute-start | bytes 1376264 | tf_op jit(solution)/shard_map/ppermute | solution.py:370
  79.2 15.3 %collective-permute-start.3 = (bf16[16,112,128]{2,1,0:T(8,128)(2,1)S(1)}, bf16[16,112,128]{2,1,0:T(8,128)(2,1)S(1)}, u32[]{:S(2)}, u32[]{:S(2)}) collective-permute-start(bf16[16,112,128]{2,1,0:T(8,128)(2,1)S(1)} %broadcast_select_fusion.2), channel_id=1, source_target_pairs={{96,64},{0,32},{97,65},{1,33},{98,66},{2,34},{99,67},{3,35},{100,6... | collective-permute-start | bytes 1376264 | tf_op jit(solution)/shard_map/ppermute | solution.py:373
  80.7 23.0 %collective-permute-start.7 = (bf16[16,112,128]{2,1,0:T(8,128)(2,1)S(1)}, bf16[16,112,128]{2,1,0:T(8,128)(2,1)S(1)}, u32[]{:S(2)}, u32[]{:S(2)}) collective-permute-start(bf16[16,112,128]{2,1,0:T(8,128)(2,1)S(1)} %broadcast_select_fusion.1), channel_id=1, source_target_pairs={{96,64},{0,32},{97,65},{1,33},{98,66},{2,34},{99,67},{3,35},{100,6... | collective-permute-start | bytes 1376264 | tf_op jit(solution)/shard_map/ppermute | solution.py:373
  88.0 20.7 %collective-permute-start.11 = (bf16[16,112,128]{2,1,0:T(8,128)(2,1)S(1)}, bf16[16,112,128]{2,1,0:T(8,128)(2,1)S(1)}, u32[]{:S(2)}, u32[]{:S(2)}) collective-permute-start(bf16[16,112,128]{2,1,0:T(8,128)(2,1)S(1)} %broadcast_select_fusion), channel_id=1, source_target_pairs={{96,64},{0,32},{97,65},{1,33},{98,66},{2,34},{99,67},{3,35},{100,6... | collective-permute-start | bytes 1376264 | tf_op jit(solution)/shard_map/ppermute | solution.py:373
  96.4 17.4 %collective-permute-start.4 = (bf16[2,112,2048]{2,1,0:T(8,128)(2,1)S(1)}, bf16[2,112,2048]{2,1,0:T(8,128)(2,1)S(1)}, u32[]{:S(2)}, u32[]{:S(2)}) collective-permute-start(bf16[2,112,2048]{2,1,0:T(8,128)(2,1)S(1)} %shard_map.104.refs_0_.refs_3_), channel_id=1, source_target_pairs={{0,1},{1,0},{2,3},{3,2},{4,5},{5,4},{6,7},{7,6},{8,9},{9,8},{10,11... | collective-permute-start | bytes 2752520 | tf_op jit(solution)/shard_map/ppermute | solution.py:280
  96.5 13.4 %collective-permute-start.14 = (bf16[3,224,512]{2,1,0:T(8,128)(2,1)S(1)}, bf16[3,224,512]{2,1,0:T(8,128)(2,1)S(1)}, u32[]{:S(2)}, u32[]{:S(2)}) collective-permute-start(bf16[3,224,512]{2,1,0:T(8,128)(2,1)S(1)} %convert_element_type.462.refs_0_), channel_id=1, source_target_pairs={{0,1},{1,0},{2,3},{3,2},{4,5},{5,4},{6,7},{7,6},{8,9},{9,8},{10,11... | collective-permute-start | bytes 2064392 | tf_op jit(solution)/shard_map/ppermute | solution.py:280
  97.0 12.9 %collective-permute-start.15 = (bf16[3,224,512]{2,1,0:T(8,128)(2,1)}, bf16[3,224,512]{2,1,0:T(8,128)(2,1)S(1)}, u32[]{:S(2)}, u32[]{:S(2)}) collective-permute-start(bf16[3,224,512]{2,1,0:T(8,128)(2,1)} %collective-permute-done.13.refs_1_), channel_id=1, source_target_pairs={{0,1},{1,0},{2,3},{3,2},{4,5},{5,4},{6,7},{7,6},{8,9},{9,8},{10,11... | collective-permute-start | bytes 2064392 | tf_op jit(solution)/shard_map/ppermute | solution.py:280
  104.7 18.9 %collective-permute-start.8 = (bf16[2,112,2048]{2,1,0:T(8,128)(2,1)S(1)}, bf16[2,112,2048]{2,1,0:T(8,128)(2,1)S(1)}, u32[]{:S(2)}, u32[]{:S(2)}) collective-permute-start(bf16[2,112,2048]{2,1,0:T(8,128)(2,1)S(1)} %shard_map.105.refs_2_.refs_0_), channel_id=1, source_target_pairs={{0,1},{1,0},{2,3},{3,2},{4,5},{5,4},{6,7},{7,6},{8,9},{9,8},{10,11... | collective-permute-start | bytes 2752520 | tf_op jit(solution)/shard_map/ppermute | solution.py:280
  109.6 14.0 %collective-permute-start.12 = (bf16[2,112,2048]{2,1,0:T(8,128)(2,1)S(1)}, bf16[2,112,2048]{2,1,0:T(8,128)(2,1)S(1)}, u32[]{:S(2)}, u32[]{:S(2)}) collective-permute-start(bf16[2,112,2048]{2,1,0:T(8,128)(2,1)S(1)} %shard_map.106.refs_4_.refs_2_), channel_id=1, source_target_pairs={{0,1},{1,0},{2,3},{3,2},{4,5},{5,4},{6,7},{7,6},{8,9},{9,8},{10,11... | collective-permute-start | bytes 2752520 | tf_op jit(solution)/shard_map/ppermute | solution.py:280
  146.1 25.6 %collective-permute-start.16 = (bf16[1024,512]{1,0:T(8,128)(2,1)S(1)}, bf16[1024,512]{1,0:T(8,128)(2,1)S(1)}, u32[]{:S(2)}, u32[]{:S(2)}) collective-permute-start(bf16[1024,512]{1,0:T(8,128)(2,1)S(1)} %get-tuple-element.33), channel_id=1, source_target_pairs={{0,8},{8,0},{16,24},{24,16},{1,9},{9,1},{17,25},{25,17},{2,10},{10... | collective-permute-start | bytes 3145736 | tf_op jit(solution)/shard_map/ppermute | solution.py:280
  146.3 27.0 %collective-permute-start.20 = (bf16[1024,512]{1,0:T(8,128)(2,1)S(1)}, bf16[1024,512]{1,0:T(8,128)(2,1)S(1)}, u32[]{:S(2)}, u32[]{:S(2)}) collective-permute-start(bf16[1024,512]{1,0:T(8,128)(2,1)S(1)} %get-tuple-element.35), channel_id=1, source_target_pairs={{0,2},{2,0},{4,6},{6,4},{1,3},{3,1},{5,7},{7,5},{8,10},{10,8},{12,... | collective-permute-start | bytes 3145736 | tf_op jit(solution)/shard_map/ppermute | solution.py:280
  149.0 28.6 %collective-permute-start.24 = (bf16[1024,512]{1,0:T(8,128)(2,1)S(1)}, bf16[1024,512]{1,0:T(8,128)(2,1)S(1)}, u32[]{:S(2)}, u32[]{:S(2)}) collective-permute-start(bf16[1024,512]{1,0:T(8,128)(2,1)S(1)} %get-tuple-element.37), channel_id=1, source_target_pairs={{0,24},{8,16},{16,8},{24,0},{1,25},{9,17},{17,9},{25,1},{2,26},{10... | collective-permute-start | bytes 3145736 | tf_op jit(solution)/shard_map/ppermute | solution.py:280
  150.3 27.7 %collective-permute-start.28 = (bf16[1024,512]{1,0:T(8,128)(2,1)S(1)}, bf16[1024,512]{1,0:T(8,128)(2,1)S(1)}, u32[]{:S(2)}, u32[]{:S(2)}) collective-permute-start(bf16[1024,512]{1,0:T(8,128)(2,1)S(1)} %get-tuple-element.39), channel_id=1, source_target_pairs={{0,6},{2,4},{4,2},{6,0},{1,7},{3,5},{5,3},{7,1},{8,14},{10,12},{12... | collective-permute-start | bytes 3145736 | tf_op jit(solution)/shard_map/ppermute | solution.py:280
  171.9 14.8 %collective-permute-start.17 = (bf16[1,4,2,64,512]{4,3,2,1,0:T(8,128)(2,1)S(1)}, bf16[1,4,2,64,512]{4,3,2,1,0:T(8,128)(2,1)S(1)}, u32[]{:S(2)}, u32[]{:S(2)}) collective-permute-start(bf16[1,4,2,64,512]{4,3,2,1,0:T(8,128)(2,1)S(1)} %bitcast.79), channel_id=1, source_target_pairs={{0,24},{8,16},{16,8},{24,0},{1,25},{9,17},{17,9},{25,1},{2,26},{10... | collective-permute-start | bytes 1572872 | tf_op jit(solution)/shard_map/ppermute | solution.py:280
  173.5 16.1 %collective-permute-start.21 = (bf16[1,4,2,64,512]{4,3,2,1,0:T(8,128)(2,1)S(1)}, bf16[1,4,2,64,512]{4,3,2,1,0:T(8,128)(2,1)S(1)}, u32[]{:S(2)}, u32[]{:S(2)}) collective-permute-start(bf16[1,4,2,64,512]{4,3,2,1,0:T(8,128)(2,1)S(1)} %bitcast.78), channel_id=1, source_target_pairs={{0,6},{2,4},{4,2},{6,0},{1,7},{3,5},{5,3},{7,1},{8,14},{10,12},{12... | collective-permute-start | bytes 1572872 | tf_op jit(solution)/shard_map/ppermute | solution.py:280
  177.7 13.0 %collective-permute-start.25 = (bf16[1,4,2,64,512]{4,3,2,1,0:T(8,128)(2,1)S(1)}, bf16[1,4,2,64,512]{4,3,2,1,0:T(8,128)(2,1)S(1)}, u32[]{:S(2)}, u32[]{:S(2)}) collective-permute-start(bf16[1,4,2,64,512]{4,3,2,1,0:T(8,128)(2,1)S(1)} %bitcast.77), channel_id=1, source_target_pairs={{0,8},{8,0},{16,24},{24,16},{1,9},{9,1},{17,25},{25,17},{2,10},{10... | collective-permute-start | bytes 1572872 | tf_op jit(solution)/shard_map/ppermute | solution.py:280
  178.1 14.6 %collective-permute-start.29 = (bf16[1,4,2,64,512]{4,3,2,1,0:T(8,128)(2,1)S(1)}, bf16[1,4,2,64,512]{4,3,2,1,0:T(8,128)(2,1)S(1)}, u32[]{:S(2)}, u32[]{:S(2)}) collective-permute-start(bf16[1,4,2,64,512]{4,3,2,1,0:T(8,128)(2,1)S(1)} %bitcast.76), channel_id=1, source_target_pairs={{0,2},{2,0},{4,6},{6,4},{1,3},{3,1},{5,7},{7,5},{8,10},{10,8},{12,... | collective-permute-start | bytes 1572872 | tf_op jit(solution)/shard_map/ppermute | solution.py:280
  (19 other events, 138.7 us)

commit v3 on v2

--- a/solution.py
+++ b/solution.py
@@ -48,56 +48,80 @@
     return jax.ShapeDtypeStruct(shape, dtype)
 
 
-def pack_kernel(where_ref, gate_ref, up_ref, gain_ref, own_ref, send_ref):
+def pack_kernel(where_ref, gate_ref, up_ref, gain_ref, *out_refs):
     depth = gain_ref.shape[1]
     gain = jnp.broadcast_to(gain_ref[...], (128, depth)).T[:, :1]
     rows = jnp.concatenate([gate_ref[0] * gain, up_ref[0] * gain], axis=0)
     cols = rows.astype(jnp.bfloat16).T
-    dests, _, half, lanes = own_ref.shape
+    dests, half, lanes = out_refs[-1].shape
     cols = cols.reshape(dests, 2, half, lanes)
     low, high = cols[:, 0], cols[:, 1]
     first = where_ref[1] == 0
-    own_ref[:, 0] = jnp.where(first, low, high)
-    send_ref[:, 0] = jnp.where(first, high, low)
+    own, send = jnp.where(first, low, high), jnp.where(first, high, low)
+    final = pl.program_id(0) == pl.num_programs(0) - 1
+
+    @pl.when(jnp.logical_not(final))
+    def _():
+        out_refs[0][:, 0] = own
+        out_refs[1][:, 0] = send
+
+    @pl.when(final)
+    def _():
+        out_refs[2][...] = own
+        out_refs[3][...] = send
 
 
 def pack(where, gate, up, gain, dests):
     experts, depth, width = gate.shape
     half = width // dests // 2
     block = pl.BlockSpec((1, depth, width), lambda e, w: (e, 0, 0))
-    out = pl.BlockSpec((dests, 1, half, 2 * depth), lambda e, w: (0, e, 0, 0))
-    return call(
-        pack_kernel, (experts,), [block, block, whole((1, depth))], [out] * 2,
-        [shaped(dests, experts, half, 2 * depth)] * 2, (where, gate, up, gain), 3e9, 6e6,
-    )
-
-
-def unpack_kernel(where_ref, own_ref, down_ref, up_ref, far_ref, out_ref):
-    z = where_ref[0]
-    sources, half, lanes = own_ref.shape
+    one = (dests, half, 2 * depth)
+    some = pl.BlockSpec((dests, 1, half, 2 * depth), lambda e, w: (0, jnp.minimum(e, experts - 2), 0, 0))
+    return call(
+        pack_kernel, (experts,), [block, block, whole((1, depth))],
+        [some, some, whole(one), whole(one)],
+        [shaped(dests, experts - 1, half, 2 * depth)] * 2 + [shaped(*one)] * 2,
+        (where, gate, up, gain), 3e9, 6e6,
+    )
+
+
+def unpack_kernel(where_ref, *refs):
+    out_ref = refs[-1]
+    if len(refs) == 2:
+        sources = refs[0].shape[0]
+        choices = [[lambda s, part=part: refs[0][s, part] for part in range(2)]]
+    else:
+        own, below, above, far = refs[:-1]
+        sources = own.shape[0]
+        pick = ((own, below), (below, far), (far, above), (above, own))
+        choices = [[lambda s, ref=ref: ref[s] for ref in two] for two in pick]
+    half, lanes = refs[0].shape[-2:]
     left = lax.broadcasted_iota(jnp.int32, (half, lanes), 1) < lanes // 2
-    pick = ((own_ref, down_ref, far_ref, up_ref), (down_ref, far_ref, up_ref, own_ref))
-    for plane in range(4):
-
-        @pl.when(z == plane)
-        def _():
-            for part in range(2):
-                ref = pick[part][plane]
-                for pair in range(sources // 2):
-                    one = ref[2 * pair].astype(jnp.float32)
-                    other = ref[2 * pair + 1].astype(jnp.float32)
-                    crossed = pltpu.roll(jnp.where(left, other, one), lanes // 2, 1)
-                    start = part * sources * (lanes // 2) + pair * lanes
-                    at = slice(start, start + lanes)
-                    out_ref[0, :, at] = jnp.where(left, one, crossed).astype(jnp.bfloat16)
-                    out_ref[1, :, at] = jnp.where(left, crossed, other).astype(jnp.bfloat16)
+
+    def place(blocks):
+        for part, block in enumerate(blocks):
+            for pair in range(sources // 2):
+                one = block(2 * pair).astype(jnp.float32)
+                other = block(2 * pair + 1).astype(jnp.float32)
+                crossed = pltpu.roll(jnp.where(left, other, one), lanes // 2, 1)
+                start = part * sources * (lanes // 2) + pair * lanes
+                at = slice(start, start + lanes)
+                out_ref[0, :, at] = jnp.where(left, one, crossed).astype(jnp.bfloat16)
+                out_ref[1, :, at] = jnp.where(left, crossed, other).astype(jnp.bfloat16)
+
+    if len(choices) == 1:
+        place(choices[0])
+    else:
+        for plane, blocks in enumerate(choices):
+            pl.when(where_ref[0] == plane)(lambda blocks=blocks: place(blocks))
 
 
 def unpack(where, pieces):
-    sources, half, lanes = pieces[0].shape
+    sources = pieces[0].shape[0]
+    half, lanes = pieces[0].shape[-2:]
     shape = (2, half, sources * lanes)
     return call(
-        unpack_kernel, (1,), [whole(pieces[0].shape)] * 4, whole(shape),
+        unpack_kernel, (1,), [whole(piece.shape) for piece in pieces], whole(shape),
         shaped(*shape), (where, *pieces), 1e9, 3e6, vmem=12,
     )
 
@@ -192,32 +216,11 @@
     return (gate_act / (1.0 + jnp.exp(-gate_act)) * up_act * mix).astype(jnp.bfloat16)
 
 
-def hidden_kernel(expert, where_ref, normed_ref, mix_ref, own_ref, other_ref, out_ref, gate, up):
-    @pl.when(pl.program_id(0) == 0)
-    def _():
-        fill(where_ref, own_ref, other_ref, gate, up)
-
-    mix = mix_ref[0, :, expert : expert + 1]
-    out_ref[0] = hidden_of(normed_ref[0], mix, gate[...], up[...])
-
-
-def hidden_units(where, normed, mix, own, other, expert):
-    groups, rows, width = normed.shape
-    at = lambda g, w: (g, 0, 0)
-    side = whole(own.shape)
-    weight = pltpu.VMEM((UNITS, width), jnp.bfloat16)
-    return call(
-        lambda *refs: hidden_kernel(expert, *refs), (groups,),
-        [pl.BlockSpec((1, rows, width), at), pl.BlockSpec((1, rows, mix.shape[-1]), at), side, side],
-        pl.BlockSpec((1, rows, UNITS), at), shaped(groups, rows, UNITS),
-        (where, normed, mix, own, other), 4 * groups * rows * width * UNITS, 12e6,
-        scratch=(weight, weight), vmem=48,
-    )
-
-
-def last_kernel(where_ref, normed_ref, mix_ref, early_ref, *refs):
-    sides, down_ref = (refs[0:2], refs[2:4]), refs[4]
-    outs, weights = refs[5:-4], (refs[-4:-2], refs[-2:])
+def last_kernel(experts, where_ref, normed_ref, mix_ref, *refs):
+    sides = [refs[2 * e : 2 * e + 2] for e in range(experts)]
+    down_ref, outs = refs[2 * experts], refs[2 * experts + 1 : -2 * experts]
+    scratch = refs[-2 * experts :]
+    weights = [scratch[2 * e : 2 * e + 2] for e in range(experts)]
     yy = pl.program_id(0)
 
     @pl.when(yy == 0)
@@ -225,8 +228,8 @@
         for side, weight in zip(sides, weights):
             fill(where_ref, *side, *weight)
 
-    hidden = [early_ref[0]]
-    for expert, (gate, up) in enumerate(weights, 1):
+    hidden = []
+    for expert, (gate, up) in enumerate(weights):
         mix = mix_ref[0, :, expert : expert + 1]
         hidden.append(hidden_of(normed_ref[0], mix, gate[...], up[...]))
     rows = jnp.concatenate(hidden, axis=1)
@@ -259,19 +262,20 @@
                 ref[to, :] = product[xx * part : (xx + 1) * part]
 
 
-def last(where, normed, mix, early, sides, down):
+def last(where, normed, mix, sides, down):
     ys, rows, width = normed.shape
+    experts = len(sides) // 2
     half = (ys * rows // 2, width // len(COLORS))
     at = lambda i, w: (i, 0, 0)
     side = whole(sides[0].shape)
     weight = pltpu.VMEM((UNITS, width), jnp.bfloat16)
     return call(
-        last_kernel, (ys,),
-        [pl.BlockSpec((1, rows, width), at), pl.BlockSpec((1, rows, mix.shape[-1]), at)]
-        + [pl.BlockSpec((1, rows, UNITS), at)] + [side] * 4 + [whole(down.shape)],
+        lambda *refs: last_kernel(experts, *refs), (ys,),
+        [pl.BlockSpec((1, rows, width), at), pl.BlockSpec((1, rows, experts), at)]
+        + [side] * (2 * experts) + [whole(down.shape)],
         [whole(half)] * (2 * len(COLORS)), [shaped(*half)] * (2 * len(COLORS)),
-        (where, normed, mix, early, *sides, down), 14 * ys * rows * width * UNITS, 25e6,
-        scratch=(weight,) * 4, vmem=LAST_VMEM,
+        (where, normed, mix, *sides, down), 6 * experts * ys * rows * width * UNITS, 25e6,
+        scratch=(weight,) * (2 * experts), vmem=LAST_VMEM,
     )
 
 
@@ -343,12 +347,18 @@
     other_core = lambda v: swap(v, "tp", 1)
     gain = norm_gain[None, :]
 
-    own, send = pack(where, gate_master, up_master, gain, peers // 2)
-    came = other_core(send)
-    blocks = jnp.where(
-        tp == 0, jnp.concatenate([own, came], axis=0), jnp.concatenate([came, own], axis=0)
-    )
-    mine = lax.all_to_all(blocks, PLANE, split_axis=0, concat_axis=0, tiled=True)
+    own, send, own_last, send_last = pack(where, gate_master, up_master, gain, peers // 2)
+
+    def whole_plane(own, send):
+        came = other_core(send)
+        orders = [jnp.concatenate(two, axis=0) for two in ((own, came), (came, own))]
+        return jnp.where(tp == 0, *orders)
+
+    blocks, blocks_last = whole_plane(own, send), whole_plane(own_last, send_last)
+    combine = mixing(route[0], route_weight[0], experts)
+    blocks, combine = lax.optimization_barrier((blocks, combine))
+    plane = lambda v: lax.all_to_all(v, PLANE, split_axis=0, concat_axis=0, tiled=True)
+    mine = plane(blocks)
 
     down_own = down_master.astype(jnp.bfloat16)
     down_far = swap(down_own, "gr", 1)
@@ -356,25 +366,29 @@
 
     _, width = tokens.shape[1:]
     places = [lax.axis_size(a) for a in FS]
-    combine = mixing(route[0], route_weight[0], experts)
     normed, mix = norm(
         where, tokens.reshape(*places, -1, width), combine.reshape(*places, -1, experts)
     )
     quarters = (down_own, down_far, down_own_core, down_far_core)
     down_out, down_padded = join(where, quarters)
-    mine, normed = lax.optimization_barrier((mine, normed))
-
-    sides = []
-    for e in range(experts):
-        piece = mine[:, e]
+
+    def along_z(piece):
         below = lax.ppermute(piece, Z, [(1, 0), (2, 1), (0, 3)])
         above = lax.ppermute(piece, Z, [(1, 2), (2, 3), (3, 0)])
         passed = jnp.where(z == 3, below, above)
         far = lax.ppermute(passed, Z, [(3, 2), (0, 1)])
-        own = unpack(where, (piece, below, above, far))
+        return piece, below, above, far
+
+    own, below, above, far = along_z(blocks_last)
+    pick = lambda a, b, c, d: jnp.where(z < 2, jnp.where(z < 1, a, b), jnp.where(z < 3, c, d))
+    raw = jnp.stack([pick(own, below, far, above), pick(below, far, above, own)], axis=1)
+    both = plane(raw)
+    pieces = [along_z(mine[:, e]) for e in range(experts - 1)] + [(both,)]
+    sides = []
+    for e in range(experts):
+        own = unpack(where, pieces[e])
         sides += [own, other_core(own)]
-    early = hidden_units(where, normed, mix, sides[0], sides[1], 0)
-    outs = last(where, normed, mix, early, sides[2:], down_padded.reshape(-1, width))
+    outs = last(where, normed, mix, sides, down_padded.reshape(-1, width))
     sums = []
     for color, exchanges in enumerate(COLORS):
         sums.append(Sums(outs[2 * color], outs[2 * color + 1], exchanges))

time: 215 us -> 214 us (level)
  the two profiles are of different devices: /device:TPU:66 before, /device:TPU:1 now
where the time goes in v3:
time: 214 us; the launch traced here: 210 us
  starting transfers between devices  82.2 us (38%)
  Pallas kernels  59.1 us (28%)
  waiting for transfers between devices  50.8 us (24%)
  other arithmetic  13.3 us (6%)
  local copies, waits for them, and re-layouts  3.93 us (2%)
    pallas_call x8, Pallas kernels, call(): pl.pallas_call(kernel, out_shape=out_shape, grid_spec=pltpu.PrefetchScala...  59.1 us
    ppermute x25, starting transfers between devices, swap(): return lax.ppermute(array, axis, [(i, i ^ mask) for i in range(peers)])  42.2 us
    ppermute x25, waiting for transfers between devices, swap(): return lax.ppermute(array, axis, [(i, i ^ mask) for i in range(peers)])  36.8 us
    ppermute x3, starting transfers between devices, along_z(): below = lax.ppermute(piece, Z, [(1, 0), (2, 1), (0, 3)])  15.9 us
    all_to_all x2, starting transfers between devices, program(): lax.all_to_all(v, PLANE, split_axis=0, concat_axis=0, tiled=True)  10.8 us
    ppermute x3, starting transfers between devices, along_z(): far = lax.ppermute(passed, Z, [(3, 2), (0, 1)])  9.49 us
    all_to_all x2, waiting for transfers between devices, program(): lax.all_to_all(v, PLANE, split_axis=0, concat_axis=0, tiled=True)  7.5 us
    ppermute x3, waiting for transfers between devices, along_z(): above = lax.ppermute(piece, Z, [(1, 2), (2, 3), (3, 0)])  6.51 us
  transfers between devices with their start and end apart: 36, of which 12 were waited for; matrix products, arithmetic and copies ran while one was open for 7% of the time, Pallas kernels for 13%

profile of v3, /device:TPU:1, one launch (start us, length us, event | category | flops | bytes accessed | tf_op | source)
XLA Modules:
  0.0 210.4 jit_solution(12150768079828768019)
XLA Ops:
  1.3 5.0 %shard_map.102 = (bf16[8,2,112,128]{3,2,1,0:T(8,128)(2,1)}, bf16[8,2,112,128]{3,2,1,0:T(8,128)(2,1)}, bf16[8,112,128]{2,1,0:T(8,128)(2,1)}, bf16[8,112,128]{2,1,0:T(8,128)(2,1)}) custom-call(s32[5]{0:T(128)} %stack.32.where_ref.refs_0_, f32[3,64,1792]{2,1,0:T(8,128)} %gate_ref.1, f32[3,64,1792]{2,1,0:T(8,128)} %up_ref.1, f32[1,64]{1,0:T(1,128)} %bitcast.90), custom_call_target="tpu_custom_call" | custom-call | flops 3000000000 | bytes 6000000 | tf_op jit(solution)/shard_map/pallas_call | solution.py:26
  10.2 5.8 %collective-permute-start.10 = (bf16[16,112,128]{2,1,0:T(8,128)(2,1)S(1)}, bf16[16,112,128]{2,1,0:T(8,128)(2,1)S(1)}, u32[]{:S(2)}, u32[]{:S(2)}) collective-permute-start(bf16[16,112,128]{2,1,0:T(8,128)(2,1)S(1)} %maximum_select_fusion.1), channel_id=1, source_target_pairs={{32,0},{64,32},{0,96},{33,1},{65,33},{1,97},{34,2},{66,34},{2,98},... | collective-permute-start | bytes 1376264 | tf_op jit(solution)/shard_map/ppermute | solution.py:376
  19.5 6.8 %all-to-all-start = ((bf16[16,2,112,128]{3,2,1,0:T(8,128)(2,1)}), bf16[16,2,112,128]{3,2,1,0:T(8,128)(2,1)S(1)}, u32[]{:S(2)}, u32[]{:S(2)}) async-start(bf16[16,2,112,128]{3,2,1,0:T(8,128)(2,1)} %maximum_select_fusion), calls=%async_computation | async-start | bytes 1835008 | tf_op jit(solution)/shard_map/all_to_all | solution.py:360
  26.3 4.2 %collective-permute-done.11 = bf16[16,112,128]{2,1,0:T(8,128)(2,1)S(1)} collective-permute-done((bf16[16,112,128]{2,1,0:T(8,128)(2,1)S(1)}, bf16[16,112,128]{2,1,0:T(8,128)(2,1)S(1)}, u32[]{:S(2)}, u32[]{:S(2)}) %collective-permute-start.11) | collective-permute-done | bytes 458784 | tf_op jit(solution)/shard_map/ppermute | solution.py:377
  33.4 7.5 %all-to-all-done = bf16[16,2,112,128]{3,2,1,0:T(8,128)(2,1)S(1)} async-done(((bf16[16,2,112,128]{3,2,1,0:T(8,128)(2,1)}), bf16[16,2,112,128]{3,2,1,0:T(8,128)(2,1)S(1)}, u32[]{:S(2)}, u32[]{:S(2)}) %all-to-all-start) | async-done | bytes 917536 | tf_op jit(solution)/shard_map/all_to_all | solution.py:360
  41.0 4.9 %collective-permute-start.5 = (bf16[16,112,128]{2,1,0:T(8,128)(2,1)S(1)}, bf16[16,112,128]{2,1,0:T(8,128)(2,1)S(1)}, u32[]{:S(2)}, u32[]{:S(2)}) collective-permute-start(bf16[16,112,128]{2,1,0:T(8,128)(2,1)S(1)} %get-tuple-element.62.refs_0_), channel_id=1, source_target_pairs={{32,0},{64,32},{0,96},{33,1},{65,33},{1,97},{34,2},{66,34},{2,98},... | collective-permute-start | bytes 1376264 | tf_op jit(solution)/shard_map/ppermute | solution.py:376
  48.6 5.2 %collective-permute-start.1 = (bf16[16,112,128]{2,1,0:T(8,128)(2,1)S(1)}, bf16[16,112,128]{2,1,0:T(8,128)(2,1)}, u32[]{:S(2)}, u32[]{:S(2)}) collective-permute-start(bf16[16,112,128]{2,1,0:T(8,128)(2,1)S(1)} %get-tuple-element.63.refs_0_), channel_id=1, source_target_pairs={{32,0},{64,32},{0,96},{33,1},{65,33},{1,97},{34,2},{66,34},{2,98},... | collective-permute-start | bytes 1376264 | tf_op jit(solution)/shard_map/ppermute | solution.py:376
  56.1 4.0 %all-to-all-start.1 = ((bf16[16,2,112,128]{3,2,1,0:T(8,128)(2,1)}), bf16[16,2,112,128]{3,2,1,0:T(8,128)(2,1)S(1)}, u32[]{:S(2)}, u32[]{:S(2)}) async-start(bf16[16,2,112,128]{3,2,1,0:T(8,128)(2,1)} %pad_maximum_fusion), calls=%async_computation.1 | async-start | bytes 1835008 | tf_op jit(solution)/shard_map/all_to_all | solution.py:360
  63.7 5.4 %collective-permute-start.7 = (bf16[16,112,128]{2,1,0:T(8,128)(2,1)}, bf16[16,112,128]{2,1,0:T(8,128)(2,1)}, u32[]{:S(2)}, u32[]{:S(2)}) collective-permute-start(bf16[16,112,128]{2,1,0:T(8,128)(2,1)} %broadcast_select_fusion.1), channel_id=1, source_target_pairs={{96,64},{0,32},{97,65},{1,33},{98,66},{2,34},{99,67},{3,35},{100,6... | collective-permute-start | bytes 1376264 | tf_op jit(solution)/shard_map/ppermute | solution.py:379
  69.1 2.3 %collective-permute-done.2.refs_2_ = bf16[16,112,128]{2,1,0:T(8,128)(2,1)} collective-permute-done((bf16[16,112,128]{2,1,0:T(8,128)(2,1)S(1)}, bf16[16,112,128]{2,1,0:T(8,128)(2,1)}, u32[]{:S(2)}, u32[]{:S(2)}) %collective-permute-start.2) | collective-permute-done | bytes 458784 | tf_op jit(solution)/shard_map/ppermute | solution.py:377
  77.1 15.3 %collective-permute-start.13 = (bf16[2,112,2048]{2,1,0:T(8,128)(2,1)}, bf16[2,112,2048]{2,1,0:T(8,128)(2,1)S(1)}, u32[]{:S(2)}, u32[]{:S(2)}) collective-permute-start(bf16[2,112,2048]{2,1,0:T(8,128)(2,1)} %shard_map.105.refs_4_.refs_7_), channel_id=1, source_target_pairs={{0,1},{1,0},{2,3},{3,2},{4,5},{5,4},{6,7},{7,6},{8,9},{9,8},{10,11... | collective-permute-start | bytes 2752520 | tf_op jit(solution)/shard_map/ppermute | solution.py:284
  92.4 2.9 %shard_map.104.refs_2_.refs_5_ = bf16[2,112,2048]{2,1,0:T(8,128)(2,1)} custom-call(s32[5]{0:T(128)S(1)} %copy-done, bf16[16,112,128]{2,1,0:T(8,128)(2,1)S(1)} %get-tuple-element.62.refs_0_, bf16[16,112,128]{2,1,0:T(8,128)(2,1)S(1)} %collective-permute-done.5.refs_1_, bf16[16,112,128]{2,1,0:T(8,128)(2,1)S(1)} %collective-permute-done.6.refs_2_, ...), custom_call_target="tpu_custom_call" | custom-call | flops 1000000000 | bytes 3000000 | tf_op jit(solution)/shard_map/pallas_call | solution.py:26
  95.3 3.2 %shard_map.103.refs_0_.refs_3_ = bf16[2,112,2048]{2,1,0:T(8,128)(2,1)} custom-call(s32[5]{0:T(128)S(1)} %copy-done, bf16[16,112,128]{2,1,0:T(8,128)(2,1)S(1)} %get-tuple-element.63.refs_0_, bf16[16,112,128]{2,1,0:T(8,128)(2,1)} %collective-permute-done.1.refs_1_, bf16[16,112,128]{2,1,0:T(8,128)(2,1)} %collective-permute-done.2.refs_2_, ...), custom_call_target="tpu_custom_call" | custom-call | flops 1000000000 | bytes 3000000 | tf_op jit(solution)/shard_map/pallas_call | solution.py:26
  98.5 3.0 %collective-permute-start.4 = (bf16[2,112,2048]{2,1,0:T(8,128)(2,1)}, bf16[2,112,2048]{2,1,0:T(8,128)(2,1)}, u32[]{:S(2)}, u32[]{:S(2)}) collective-permute-start(bf16[2,112,2048]{2,1,0:T(8,128)(2,1)} %shard_map.103.refs_0_.refs_3_), channel_id=1, source_target_pairs={{0,1},{1,0},{2,3},{3,2},{4,5},{5,4},{6,7},{7,6},{8,9},{9,8},{10,11... | collective-permute-start | bytes 2752520 | tf_op jit(solution)/shard_map/ppermute | solution.py:284
  103.4 9.1 %shard_map.108 = (bf16[4,512,2048]{2,1,0:T(8,128)(2,1)}, f32[4,512,3]{2,1,0:T(8,128)}) custom-call(s32[5]{0:T(128)} %stack.32.where_ref.refs_0_, bf16[2,4,4,64,2048]{4,3,2,1,0:T(8,128)(2,1)} %bitcast.89, f32[2,4,4,64,3]{4,3,2,1,0:T(8,128)} %bitcast.83), custom_call_target="tpu_custom_call" | custom-call | flops 6000000000 | bytes 17000000 | tf_op jit(solution)/shard_map/pallas_call | solution.py:26
  112.5 4.7 %shard_map.107 = (bf16[3,224,2048]{2,1,0:T(8,128)(2,1)}, bf16[3,256,2048]{2,1,0:T(8,128)(2,1)S(1)}) custom-call(s32[5]{0:T(128)S(1)} %copy-done.1, bf16[3,224,512]{2,1,0:T(8,128)(2,1)S(1)} %convert_element_type.462.refs_0_, bf16[3,224,512]{2,1,0:T(8,128)(2,1)} %collective-permute-done.14.refs_1_, bf16[3,224,512]{2,1,0:T(8,128)(2,1)} %collective-permute-done.15.refs_2_, ...), custom_call_target="tpu_custom_call" | custom-call | flops 2000000000 | bytes 8000000 | tf_op jit(solution)/shard_map/pallas_call | solution.py:26
  118.8 27.0 %shard_map.109 = (bf16[1024,512]{1,0:T(8,128)(2,1)S(1)}, bf16[1024,512]{1,0:T(8,128)(2,1)S(1)}, bf16[1024,512]{1,0:T(8,128)(2,1)S(1)}, bf16[1024,512]{1,0:T(8,12...) custom-call(s32[5]{0:T(128)S(1)} %copy-done.1, ...), custom_call_target="tpu_custom_call" | custom-call | flops 19327352832 | bytes 25000000 | tf_op jit(solution)/shard_map/pallas_call | solution.py:26
  152.1 18.5 %collective-permute-done.17 = bf16[1024,512]{1,0:T(8,128)(2,1)S(1)} collective-permute-done((bf16[1024,512]{1,0:T(8,128)(2,1)S(1)}, bf16[1024,512]{1,0:T(8,128)(2,1)S(1)}, u32[]{:S(2)}, u32[]{:S(2)}) %collective-permute-start.17) | collective-permute-done | bytes 1048608 | tf_op jit(solution)/shard_map/ppermute | solution.py:284
  170.7 2.6 %collective-permute-start.18 = (bf16[1,4,2,64,512]{4,3,2,1,0:T(8,128)(2,1)S(1)}, bf16[1,4,2,64,512]{4,3,2,1,0:T(8,128)(2,1)S(1)}, u32[]{:S(2)}, u32[]{:S(2)}) collective-permute-start(bf16[1,4,2,64,512]{4,3,2,1,0:T(8,128)(2,1)S(1)} %bitcast.87), channel_id=1, source_target_pairs={{0,24},{8,16},{16,8},{24,0},{1,25},{9,17},{17,9},{25,1},{2,26},{10... | collective-permute-start | bytes 1572872 | tf_op jit(solution)/shard_map/ppermute | solution.py:284
  173.5 2.5 %collective-permute-start.22 = (bf16[1,4,2,64,512]{4,3,2,1,0:T(8,128)(2,1)S(1)}, bf16[1,4,2,64,512]{4,3,2,1,0:T(8,128)(2,1)S(1)}, u32[]{:S(2)}, u32[]{:S(2)}) collective-permute-start(bf16[1,4,2,64,512]{4,3,2,1,0:T(8,128)(2,1)S(1)} %bitcast.86), channel_id=1, source_target_pairs={{0,6},{2,4},{4,2},{6,0},{1,7},{3,5},{5,3},{7,1},{8,14},{10,12},{12... | collective-permute-start | bytes 1572872 | tf_op jit(solution)/shard_map/ppermute | solution.py:284
  176.6 8.1 %collective-permute-done.18 = bf16[1,4,2,64,512]{4,3,2,1,0:T(8,128)(2,1)S(1)} collective-permute-done((bf16[1,4,2,64,512]{4,3,2,1,0:T(8,128)(2,1)S(1)}, bf16[1,4,2,64,512]{4,3,2,1,0:T(8,128)(2,1)S(1)}, u32[]{:S(2)}, u32[]{:S(2)}) %collective-permute-start.18) | collective-permute-done | bytes 524320 | tf_op jit(solution)/shard_map/ppermute | solution.py:284
  191.1 2.7 %collective-permute-done.19 = bf16[1,2,2,64,512]{4,3,2,1,0:T(8,128)(2,1)S(1)} collective-permute-done((bf16[1,2,2,64,512]{4,3,2,1,0:T(8,128)(2,1)S(1)}, bf16[1,2,2,64,512]{4,3,2,1,0:T(8,128)(2,1)S(1)}, u32[]{:S(2)}, u32[]{:S(2)}) %collective-permute-start.19) | collective-permute-done | bytes 262176 | tf_op jit(solution)/shard_map/ppermute | solution.py:284
  202.0 2.3 %collective-permute-start.33 = (bf16[64,2048]{1,0:T(8,128)(2,1)S(1)}, bf16[64,2048]{1,0:T(8,128)(2,1)S(1)}, u32[]{:S(2)}, u32[]{:S(2)}) collective-permute-start(bf16[64,2048]{1,0:T(8,128)(2,1)S(1)} %pad_maximum_fusion.5), channel_id=1, source_target_pairs={{0,32},{32,0},{1,33},{33,1},{2,34},{34,2},{3,35},{35,3},{4,36},{36... | collective-permute-start | bytes 786440 | tf_op jit(solution)/shard_map/ppermute | solution.py:284
  204.3 5.3 %shard_map.106 = (bf16[3,224,2048]{2,1,0:T(8,128)(2,1)}, bf16[3,224,2048]{2,1,0:T(8,128)(2,1)}) custom-call(s32[5]{0:T(128)S(1)} %copy-done.1, bf16[2,112,2048]{2,1,0:T(8,128)(2,1)} %shard_map.103.refs_0_.refs_3_, bf16[2,112,2048]{2,1,0:T(8,128)(2,1)} %collective-permute-done.4.refs_1_.refs_4_, bf16[2,112,2048]{2,1,0:T(8,128)(2,1)} %shard_map.104.refs_2_.refs_5_, ...), custom_call_target="tpu_custom_call" | custom-call | flops 4000000000 | bytes 11000000 | tf_op jit(solution)/shard_map/pallas_call | solution.py:26
  (114 shorter events, 51.1 us)
Async XLA Ops:
  10.2 16.1 %collective-permute-start.10 = (bf16[16,112,128]{2,1,0:T(8,128)(2,1)S(1)}, bf16[16,112,128]{2,1,0:T(8,128)(2,1)S(1)}, u32[]{:S(2)}, u32[]{:S(2)}) collective-permute-start(bf16[16,112,128]{2,1,0:T(8,128)(2,1)S(1)} %maximum_select_fusion.1), channel_id=1, source_target_pairs={{32,0},{64,32},{0,96},{33,1},{65,33},{1,97},{34,2},{66,34},{2,98},... | collective-permute-start | bytes 1376264 | tf_op jit(solution)/shard_map/ppermute | solution.py:376
  16.0 14.5 %collective-permute-start.11 = (bf16[16,112,128]{2,1,0:T(8,128)(2,1)S(1)}, bf16[16,112,128]{2,1,0:T(8,128)(2,1)S(1)}, u32[]{:S(2)}, u32[]{:S(2)}) collective-permute-start(bf16[16,112,128]{2,1,0:T(8,128)(2,1)S(1)} %maximum_select_fusion.1), channel_id=1, source_target_pairs={{32,64},{64,96},{96,0},{33,65},{65,97},{97,1},{34,66},{66,98},{98,... | collective-permute-start | bytes 1376264 | tf_op jit(solution)/shard_map/ppermute | solution.py:377
  19.5 21.4 %all-to-all-start = ((bf16[16,2,112,128]{3,2,1,0:T(8,128)(2,1)}), bf16[16,2,112,128]{3,2,1,0:T(8,128)(2,1)S(1)}, u32[]{:S(2)}, u32[]{:S(2)}) async-start(bf16[16,2,112,128]{3,2,1,0:T(8,128)(2,1)} %maximum_select_fusion), calls=%async_computation | async-start | bytes 1835008 | tf_op jit(solution)/shard_map/all_to_all | solution.py:360
  31.4 15.9 %collective-permute-start.12 = (bf16[16,112,128]{2,1,0:T(8,128)(2,1)}, bf16[16,112,128]{2,1,0:T(8,128)(2,1)}, u32[]{:S(2)}, u32[]{:S(2)}) collective-permute-start(bf16[16,112,128]{2,1,0:T(8,128)(2,1)} %broadcast_select_fusion), channel_id=1, source_target_pairs={{96,64},{0,32},{97,65},{1,33},{98,66},{2,34},{99,67},{3,35},{100,6... | collective-permute-start | bytes 1376264 | tf_op jit(solution)/shard_map/ppermute | solution.py:379
  41.0 21.9 %collective-permute-start.5 = (bf16[16,112,128]{2,1,0:T(8,128)(2,1)S(1)}, bf16[16,112,128]{2,1,0:T(8,128)(2,1)S(1)}, u32[]{:S(2)}, u32[]{:S(2)}) collective-permute-start(bf16[16,112,128]{2,1,0:T(8,128)(2,1)S(1)} %get-tuple-element.62.refs_0_), channel_id=1, source_target_pairs={{32,0},{64,32},{0,96},{33,1},{65,33},{1,97},{34,2},{66,34},{2,98},... | collective-permute-start | bytes 1376264 | tf_op jit(solution)/shard_map/ppermute | solution.py:376
  45.9 17.0 %collective-permute-start.6 = (bf16[16,112,128]{2,1,0:T(8,128)(2,1)S(1)}, bf16[16,112,128]{2,1,0:T(8,128)(2,1)S(1)}, u32[]{:S(2)}, u32[]{:S(2)}) collective-permute-start(bf16[16,112,128]{2,1,0:T(8,128)(2,1)S(1)} %get-tuple-element.62.refs_0_), channel_id=1, source_target_pairs={{32,64},{64,96},{96,0},{33,65},{65,97},{97,1},{34,66},{66,98},{98,... | collective-permute-start | bytes 1376264 | tf_op jit(solution)/shard_map/ppermute | solution.py:377
  48.6 20.4 %collective-permute-start.1 = (bf16[16,112,128]{2,1,0:T(8,128)(2,1)S(1)}, bf16[16,112,128]{2,1,0:T(8,128)(2,1)}, u32[]{:S(2)}, u32[]{:S(2)}) collective-permute-start(bf16[16,112,128]{2,1,0:T(8,128)(2,1)S(1)} %get-tuple-element.63.refs_0_), channel_id=1, source_target_pairs={{32,0},{64,32},{0,96},{33,1},{65,33},{1,97},{34,2},{66,34},{2,98},... | collective-permute-start | bytes 1376264 | tf_op jit(solution)/shard_map/ppermute | solution.py:376
  53.8 17.5 %collective-permute-start.2 = (bf16[16,112,128]{2,1,0:T(8,128)(2,1)S(1)}, bf16[16,112,128]{2,1,0:T(8,128)(2,1)}, u32[]{:S(2)}, u32[]{:S(2)}) collective-permute-start(bf16[16,112,128]{2,1,0:T(8,128)(2,1)S(1)} %get-tuple-element.63.refs_0_), channel_id=1, source_target_pairs={{32,64},{64,96},{96,0},{33,65},{65,97},{97,1},{34,66},{66,98},{98,... | collective-permute-start | bytes 1376264 | tf_op jit(solution)/shard_map/ppermute | solution.py:377
  56.1 19.1 %all-to-all-start.1 = ((bf16[16,2,112,128]{3,2,1,0:T(8,128)(2,1)}), bf16[16,2,112,128]{3,2,1,0:T(8,128)(2,1)S(1)}, u32[]{:S(2)}, u32[]{:S(2)}) async-start(bf16[16,2,112,128]{3,2,1,0:T(8,128)(2,1)} %pad_maximum_fusion), calls=%async_computation.1 | async-start | bytes 1835008 | tf_op jit(solution)/shard_map/all_to_all | solution.py:360
  61.6 39.9 %collective-permute-start.14 = (bf16[3,224,512]{2,1,0:T(8,128)(2,1)S(1)}, bf16[3,224,512]{2,1,0:T(8,128)(2,1)}, u32[]{:S(2)}, u32[]{:S(2)}) collective-permute-start(bf16[3,224,512]{2,1,0:T(8,128)(2,1)S(1)} %convert_element_type.462.refs_0_), channel_id=1, source_target_pairs={{0,64},{64,0},{1,65},{65,1},{2,66},{66,2},{3,67},{67,3},{4,68},{68... | collective-permute-start | bytes 2064392 | tf_op jit(solution)/shard_map/ppermute | solution.py:284
  63.7 28.7 %collective-permute-start.7 = (bf16[16,112,128]{2,1,0:T(8,128)(2,1)}, bf16[16,112,128]{2,1,0:T(8,128)(2,1)}, u32[]{:S(2)}, u32[]{:S(2)}) collective-permute-start(bf16[16,112,128]{2,1,0:T(8,128)(2,1)} %broadcast_select_fusion.1), channel_id=1, source_target_pairs={{96,64},{0,32},{97,65},{1,33},{98,66},{2,34},{99,67},{3,35},{100,6... | collective-permute-start | bytes 1376264 | tf_op jit(solution)/shard_map/ppermute | solution.py:379
  73.2 22.1 %collective-permute-start.3 = (bf16[16,112,128]{2,1,0:T(8,128)(2,1)}, bf16[16,112,128]{2,1,0:T(8,128)(2,1)}, u32[]{:S(2)}, u32[]{:S(2)}) collective-permute-start(bf16[16,112,128]{2,1,0:T(8,128)(2,1)} %broadcast_select_fusion.2), channel_id=1, source_target_pairs={{96,64},{0,32},{97,65},{1,33},{98,66},{2,34},{99,67},{3,35},{100,6... | collective-permute-start | bytes 1376264 | tf_op jit(solution)/shard_map/ppermute | solution.py:379
  77.1 41.7 %collective-permute-start.13 = (bf16[2,112,2048]{2,1,0:T(8,128)(2,1)}, bf16[2,112,2048]{2,1,0:T(8,128)(2,1)S(1)}, u32[]{:S(2)}, u32[]{:S(2)}) collective-permute-start(bf16[2,112,2048]{2,1,0:T(8,128)(2,1)} %shard_map.105.refs_4_.refs_7_), channel_id=1, source_target_pairs={{0,1},{1,0},{2,3},{3,2},{4,5},{5,4},{6,7},{7,6},{8,9},{9,8},{10,11... | collective-permute-start | bytes 2752520 | tf_op jit(solution)/shard_map/ppermute | solution.py:284
  95.3 23.5 %collective-permute-start.8 = (bf16[2,112,2048]{2,1,0:T(8,128)(2,1)}, bf16[2,112,2048]{2,1,0:T(8,128)(2,1)S(1)}, u32[]{:S(2)}, u32[]{:S(2)}) collective-permute-start(bf16[2,112,2048]{2,1,0:T(8,128)(2,1)} %shard_map.104.refs_2_.refs_5_), channel_id=1, source_target_pairs={{0,1},{1,0},{2,3},{3,2},{4,5},{5,4},{6,7},{7,6},{8,9},{9,8},{10,11... | collective-permute-start | bytes 2752520 | tf_op jit(solution)/shard_map/ppermute | solution.py:284
  98.5 20.3 %collective-permute-start.4 = (bf16[2,112,2048]{2,1,0:T(8,128)(2,1)}, bf16[2,112,2048]{2,1,0:T(8,128)(2,1)}, u32[]{:S(2)}, u32[]{:S(2)}) collective-permute-start(bf16[2,112,2048]{2,1,0:T(8,128)(2,1)} %shard_map.103.refs_0_.refs_3_), channel_id=1, source_target_pairs={{0,1},{1,0},{2,3},{3,2},{4,5},{5,4},{6,7},{7,6},{8,9},{9,8},{10,11... | collective-permute-start | bytes 2752520 | tf_op jit(solution)/shard_map/ppermute | solution.py:284
  101.5 11.0 %collective-permute-start.15 = (bf16[3,224,512]{2,1,0:T(8,128)(2,1)S(1)}, bf16[3,224,512]{2,1,0:T(8,128)(2,1)}, u32[]{:S(2)}, u32[]{:S(2)}) collective-permute-start(bf16[3,224,512]{2,1,0:T(8,128)(2,1)S(1)} %convert_element_type.462.refs_0_), channel_id=1, source_target_pairs={{0,1},{1,0},{2,3},{3,2},{4,5},{5,4},{6,7},{7,6},{8,9},{9,8},{10,11... | collective-permute-start | bytes 2064392 | tf_op jit(solution)/shard_map/ppermute | solution.py:284
  145.8 24.8 %collective-permute-start.17 = (bf16[1024,512]{1,0:T(8,128)(2,1)S(1)}, bf16[1024,512]{1,0:T(8,128)(2,1)S(1)}, u32[]{:S(2)}, u32[]{:S(2)}) collective-permute-start(bf16[1024,512]{1,0:T(8,128)(2,1)S(1)} %get-tuple-element.37), channel_id=1, source_target_pairs={{0,8},{8,0},{16,24},{24,16},{1,9},{9,1},{17,25},{25,17},{2,10},{10... | collective-permute-start | bytes 3145736 | tf_op jit(solution)/shard_map/ppermute | solution.py:284
  147.2 26.1 %collective-permute-start.21 = (bf16[1024,512]{1,0:T(8,128)(2,1)S(1)}, bf16[1024,512]{1,0:T(8,128)(2,1)S(1)}, u32[]{:S(2)}, u32[]{:S(2)}) collective-permute-start(bf16[1024,512]{1,0:T(8,128)(2,1)S(1)} %get-tuple-element.39), channel_id=1, source_target_pairs={{0,2},{2,0},{4,6},{6,4},{1,3},{3,1},{5,7},{7,5},{8,10},{10,8},{12,... | collective-permute-start | bytes 3145736 | tf_op jit(solution)/shard_map/ppermute | solution.py:284
  148.4 27.6 %collective-permute-start.25 = (bf16[1024,512]{1,0:T(8,128)(2,1)S(1)}, bf16[1024,512]{1,0:T(8,128)(2,1)S(1)}, u32[]{:S(2)}, u32[]{:S(2)}) collective-permute-start(bf16[1024,512]{1,0:T(8,128)(2,1)S(1)} %get-tuple-element.41), channel_id=1, source_target_pairs={{0,24},{8,16},{16,8},{24,0},{1,25},{9,17},{17,9},{25,1},{2,26},{10... | collective-permute-start | bytes 3145736 | tf_op jit(solution)/shard_map/ppermute | solution.py:284
  150.2 26.0 %collective-permute-start.29 = (bf16[1024,512]{1,0:T(8,128)(2,1)S(1)}, bf16[1024,512]{1,0:T(8,128)(2,1)S(1)}, u32[]{:S(2)}, u32[]{:S(2)}) collective-permute-start(bf16[1024,512]{1,0:T(8,128)(2,1)S(1)} %get-tuple-element.43), channel_id=1, source_target_pairs={{0,6},{2,4},{4,2},{6,0},{1,7},{3,5},{5,3},{7,1},{8,14},{10,12},{12... | collective-permute-start | bytes 3145736 | tf_op jit(solution)/shard_map/ppermute | solution.py:284
  170.7 14.0 %collective-permute-start.18 = (bf16[1,4,2,64,512]{4,3,2,1,0:T(8,128)(2,1)S(1)}, bf16[1,4,2,64,512]{4,3,2,1,0:T(8,128)(2,1)S(1)}, u32[]{:S(2)}, u32[]{:S(2)}) collective-permute-start(bf16[1,4,2,64,512]{4,3,2,1,0:T(8,128)(2,1)S(1)} %bitcast.87), channel_id=1, source_target_pairs={{0,24},{8,16},{16,8},{24,0},{1,25},{9,17},{17,9},{25,1},{2,26},{10... | collective-permute-start | bytes 1572872 | tf_op jit(solution)/shard_map/ppermute | solution.py:284
  173.5 13.6 %collective-permute-start.22 = (bf16[1,4,2,64,512]{4,3,2,1,0:T(8,128)(2,1)S(1)}, bf16[1,4,2,64,512]{4,3,2,1,0:T(8,128)(2,1)S(1)}, u32[]{:S(2)}, u32[]{:S(2)}) collective-permute-start(bf16[1,4,2,64,512]{4,3,2,1,0:T(8,128)(2,1)S(1)} %bitcast.86), channel_id=1, source_target_pairs={{0,6},{2,4},{4,2},{6,0},{1,7},{3,5},{5,3},{7,1},{8,14},{10,12},{12... | collective-permute-start | bytes 1572872 | tf_op jit(solution)/shard_map/ppermute | solution.py:284
  176.1 12.1 %collective-permute-start.26 = (bf16[1,4,2,64,512]{4,3,2,1,0:T(8,128)(2,1)S(1)}, bf16[1,4,2,64,512]{4,3,2,1,0:T(8,128)(2,1)S(1)}, u32[]{:S(2)}, u32[]{:S(2)}) collective-permute-start(bf16[1,4,2,64,512]{4,3,2,1,0:T(8,128)(2,1)S(1)} %bitcast.85), channel_id=1, source_target_pairs={{0,8},{8,0},{16,24},{24,16},{1,9},{9,1},{17,25},{25,17},{2,10},{10... | collective-permute-start | bytes 1572872 | tf_op jit(solution)/shard_map/ppermute | solution.py:284
  176.3 13.6 %collective-permute-start.30 = (bf16[1,4,2,64,512]{4,3,2,1,0:T(8,128)(2,1)S(1)}, bf16[1,4,2,64,512]{4,3,2,1,0:T(8,128)(2,1)S(1)}, u32[]{:S(2)}, u32[]{:S(2)}) collective-permute-start(bf16[1,4,2,64,512]{4,3,2,1,0:T(8,128)(2,1)S(1)} %bitcast.84), channel_id=1, source_target_pairs={{0,2},{2,0},{4,6},{6,4},{1,3},{3,1},{5,7},{7,5},{8,10},{10,8},{12,... | collective-permute-start | bytes 1572872 | tf_op jit(solution)/shard_map/ppermute | solution.py:284
  (19 other events, 133.8 us)

commit v4 on v3

--- a/solution.py
+++ b/solution.py
@@ -11,7 +11,7 @@
 Z = ("gr", "fs_0")
 UNITS = 256
 MIB = 1024 * 1024
-LAST_VMEM = 40
+LAST_VMEM = 32
 
 
 COLORS = (
@@ -193,7 +193,7 @@
             shaped(ys, xs * zs * rows, width),
             shaped(ys, xs * zs * rows, experts, dtype=jnp.float32),
         ],
-        (where, tokens, mix), 6e9, 17e6,
+        (where, tokens, mix), 6e9, 17e6, vmem=56,
     )
 
 
@@ -213,7 +213,8 @@
     dims = (((1,), (1,)), ((), ()))
     gate_act = lax.dot_general(normed, gate, dims, preferred_element_type=jnp.float32)
     up_act = lax.dot_general(normed, up, dims, preferred_element_type=jnp.float32)
-    return (gate_act / (1.0 + jnp.exp(-gate_act)) * up_act * mix).astype(jnp.bfloat16)
+    half = 0.5 * gate_act
+    return ((half + half * jnp.tanh(half)) * up_act * mix).astype(jnp.bfloat16)
 
 
 def last_kernel(experts, where_ref, normed_ref, mix_ref, *refs):

time: 214 us -> 212 us (level)
  no operation moved by 1% of the time
where the time goes in v4:
time: 212 us; the launch traced here: 208 us
  starting transfers between devices  82.3 us (39%)
  Pallas kernels  58.2 us (27%)
  waiting for transfers between devices  50.8 us (24%)
  other arithmetic  13.3 us (6%)
  local copies, waits for them, and re-layouts  2.39 us (1%)
    pallas_call x8, Pallas kernels, call(): pl.pallas_call(kernel, out_shape=out_shape, grid_spec=pltpu.PrefetchScala...  58.2 us
    ppermute x25, starting transfers between devices, swap(): return lax.ppermute(array, axis, [(i, i ^ mask) for i in range(peers)])  42.2 us
    ppermute x25, waiting for transfers between devices, swap(): return lax.ppermute(array, axis, [(i, i ^ mask) for i in range(peers)])  36.8 us
    ppermute x3, starting transfers between devices, along_z(): below = lax.ppermute(piece, Z, [(1, 0), (2, 1), (0, 3)])  15.9 us
    all_to_all x2, starting transfers between devices, program(): lax.all_to_all(v, PLANE, split_axis=0, concat_axis=0, tiled=True)  10.8 us
    ppermute x3, starting transfers between devices, along_z(): far = lax.ppermute(passed, Z, [(3, 2), (0, 1)])  9.52 us
    all_to_all x2, waiting for transfers between devices, program(): lax.all_to_all(v, PLANE, split_axis=0, concat_axis=0, tiled=True)  7.5 us
    ppermute x3, waiting for transfers between devices, along_z(): above = lax.ppermute(piece, Z, [(1, 2), (2, 3), (3, 0)])  6.49 us
  transfers between devices with their start and end apart: 36, of which 12 were waited for; matrix products, arithmetic and copies ran while one was open for 7% of the time, Pallas kernels for 13%

profile of v4, /device:TPU:1, one launch (start us, length us, event | category | flops | bytes accessed | tf_op | source)
XLA Modules:
  0.0 207.9 jit_solution(4530693902261942135)
XLA Ops:
  1.3 5.0 %shard_map.102 = (bf16[8,2,112,128]{3,2,1,0:T(8,128)(2,1)}, bf16[8,2,112,128]{3,2,1,0:T(8,128)(2,1)}, bf16[8,112,128]{2,1,0:T(8,128)(2,1)}, bf16[8,112,128]{2,1,0:T(8,128)(2,1)}) custom-call(s32[5]{0:T(128)} %stack.32.where_ref.refs_0_, f32[3,64,1792]{2,1,0:T(8,128)} %gate_ref.1, f32[3,64,1792]{2,1,0:T(8,128)} %up_ref.1, f32[1,64]{1,0:T(1,128)} %bitcast.90), custom_call_target="tpu_custom_call" | custom-call | flops 3000000000 | bytes 6000000 | tf_op jit(solution)/shard_map/pallas_call | solution.py:26
  10.2 5.8 %collective-permute-start.10 = (bf16[16,112,128]{2,1,0:T(8,128)(2,1)S(1)}, bf16[16,112,128]{2,1,0:T(8,128)(2,1)S(1)}, u32[]{:S(2)}, u32[]{:S(2)}) collective-permute-start(bf16[16,112,128]{2,1,0:T(8,128)(2,1)S(1)} %maximum_select_fusion.1), channel_id=1, source_target_pairs={{32,0},{64,32},{0,96},{33,1},{65,33},{1,97},{34,2},{66,34},{2,98},... | collective-permute-start | bytes 1376264 | tf_op jit(solution)/shard_map/ppermute | solution.py:377
  19.6 6.8 %all-to-all-start = ((bf16[16,2,112,128]{3,2,1,0:T(8,128)(2,1)}), bf16[16,2,112,128]{3,2,1,0:T(8,128)(2,1)S(1)}, u32[]{:S(2)}, u32[]{:S(2)}) async-start(bf16[16,2,112,128]{3,2,1,0:T(8,128)(2,1)} %maximum_select_fusion), calls=%async_computation | async-start | bytes 1835008 | tf_op jit(solution)/shard_map/all_to_all | solution.py:361
  26.4 4.2 %collective-permute-done.11 = bf16[16,112,128]{2,1,0:T(8,128)(2,1)S(1)} collective-permute-done((bf16[16,112,128]{2,1,0:T(8,128)(2,1)S(1)}, bf16[16,112,128]{2,1,0:T(8,128)(2,1)S(1)}, u32[]{:S(2)}, u32[]{:S(2)}) %collective-permute-start.11) | collective-permute-done | bytes 458784 | tf_op jit(solution)/shard_map/ppermute | solution.py:378
  33.5 7.5 %all-to-all-done = bf16[16,2,112,128]{3,2,1,0:T(8,128)(2,1)S(1)} async-done(((bf16[16,2,112,128]{3,2,1,0:T(8,128)(2,1)}), bf16[16,2,112,128]{3,2,1,0:T(8,128)(2,1)S(1)}, u32[]{:S(2)}, u32[]{:S(2)}) %all-to-all-start) | async-done | bytes 917536 | tf_op jit(solution)/shard_map/all_to_all | solution.py:361
  41.0 4.9 %collective-permute-start.5 = (bf16[16,112,128]{2,1,0:T(8,128)(2,1)S(1)}, bf16[16,112,128]{2,1,0:T(8,128)(2,1)S(1)}, u32[]{:S(2)}, u32[]{:S(2)}) collective-permute-start(bf16[16,112,128]{2,1,0:T(8,128)(2,1)S(1)} %get-tuple-element.62.refs_0_), channel_id=1, source_target_pairs={{32,0},{64,32},{0,96},{33,1},{65,33},{1,97},{34,2},{66,34},{2,98},... | collective-permute-start | bytes 1376264 | tf_op jit(solution)/shard_map/ppermute | solution.py:377
  48.7 5.2 %collective-permute-start.1 = (bf16[16,112,128]{2,1,0:T(8,128)(2,1)S(1)}, bf16[16,112,128]{2,1,0:T(8,128)(2,1)}, u32[]{:S(2)}, u32[]{:S(2)}) collective-permute-start(bf16[16,112,128]{2,1,0:T(8,128)(2,1)S(1)} %get-tuple-element.63.refs_0_), channel_id=1, source_target_pairs={{32,0},{64,32},{0,96},{33,1},{65,33},{1,97},{34,2},{66,34},{2,98},... | collective-permute-start | bytes 1376264 | tf_op jit(solution)/shard_map/ppermute | solution.py:377
  56.2 4.0 %all-to-all-start.1 = ((bf16[16,2,112,128]{3,2,1,0:T(8,128)(2,1)}), bf16[16,2,112,128]{3,2,1,0:T(8,128)(2,1)S(1)}, u32[]{:S(2)}, u32[]{:S(2)}) async-start(bf16[16,2,112,128]{3,2,1,0:T(8,128)(2,1)} %pad_maximum_fusion), calls=%async_computation.1 | async-start | bytes 1835008 | tf_op jit(solution)/shard_map/all_to_all | solution.py:361
  63.8 5.4 %collective-permute-start.7 = (bf16[16,112,128]{2,1,0:T(8,128)(2,1)}, bf16[16,112,128]{2,1,0:T(8,128)(2,1)}, u32[]{:S(2)}, u32[]{:S(2)}) collective-permute-start(bf16[16,112,128]{2,1,0:T(8,128)(2,1)} %broadcast_select_fusion.1), channel_id=1, source_target_pairs={{96,64},{0,32},{97,65},{1,33},{98,66},{2,34},{99,67},{3,35},{100,6... | collective-permute-start | bytes 1376264 | tf_op jit(solution)/shard_map/ppermute | solution.py:380
  69.1 2.3 %collective-permute-done.2.refs_2_ = bf16[16,112,128]{2,1,0:T(8,128)(2,1)} collective-permute-done((bf16[16,112,128]{2,1,0:T(8,128)(2,1)S(1)}, bf16[16,112,128]{2,1,0:T(8,128)(2,1)}, u32[]{:S(2)}, u32[]{:S(2)}) %collective-permute-start.2) | collective-permute-done | bytes 458784 | tf_op jit(solution)/shard_map/ppermute | solution.py:378
  77.2 15.3 %collective-permute-start.13 = (bf16[2,112,2048]{2,1,0:T(8,128)(2,1)}, bf16[2,112,2048]{2,1,0:T(8,128)(2,1)S(1)}, u32[]{:S(2)}, u32[]{:S(2)}) collective-permute-start(bf16[2,112,2048]{2,1,0:T(8,128)(2,1)} %shard_map.105.refs_4_.refs_7_), channel_id=1, source_target_pairs={{0,1},{1,0},{2,3},{3,2},{4,5},{5,4},{6,7},{7,6},{8,9},{9,8},{10,11... | collective-permute-start | bytes 2752520 | tf_op jit(solution)/shard_map/ppermute | solution.py:285
  92.5 2.9 %shard_map.104.refs_2_.refs_5_ = bf16[2,112,2048]{2,1,0:T(8,128)(2,1)} custom-call(s32[5]{0:T(128)S(1)} %copy-done, bf16[16,112,128]{2,1,0:T(8,128)(2,1)S(1)} %get-tuple-element.62.refs_0_, bf16[16,112,128]{2,1,0:T(8,128)(2,1)S(1)} %collective-permute-done.5.refs_1_, bf16[16,112,128]{2,1,0:T(8,128)(2,1)S(1)} %collective-permute-done.6.refs_2_, ...), custom_call_target="tpu_custom_call" | custom-call | flops 1000000000 | bytes 3000000 | tf_op jit(solution)/shard_map/pallas_call | solution.py:26
  95.4 3.2 %shard_map.103.refs_0_.refs_3_ = bf16[2,112,2048]{2,1,0:T(8,128)(2,1)} custom-call(s32[5]{0:T(128)S(1)} %copy-done, bf16[16,112,128]{2,1,0:T(8,128)(2,1)S(1)} %get-tuple-element.63.refs_0_, bf16[16,112,128]{2,1,0:T(8,128)(2,1)} %collective-permute-done.1.refs_1_, bf16[16,112,128]{2,1,0:T(8,128)(2,1)} %collective-permute-done.2.refs_2_, ...), custom_call_target="tpu_custom_call" | custom-call | flops 1000000000 | bytes 3000000 | tf_op jit(solution)/shard_map/pallas_call | solution.py:26
  98.5 3.0 %collective-permute-start.4 = (bf16[2,112,2048]{2,1,0:T(8,128)(2,1)}, bf16[2,112,2048]{2,1,0:T(8,128)(2,1)}, u32[]{:S(2)}, u32[]{:S(2)}) collective-permute-start(bf16[2,112,2048]{2,1,0:T(8,128)(2,1)} %shard_map.103.refs_0_.refs_3_), channel_id=1, source_target_pairs={{0,1},{1,0},{2,3},{3,2},{4,5},{5,4},{6,7},{7,6},{8,9},{9,8},{10,11... | collective-permute-start | bytes 2752520 | tf_op jit(solution)/shard_map/ppermute | solution.py:285
  103.4 9.1 %shard_map.108 = (bf16[4,512,2048]{2,1,0:T(8,128)(2,1)}, f32[4,512,3]{2,1,0:T(8,128)}) custom-call(s32[5]{0:T(128)} %stack.32.where_ref.refs_0_, bf16[2,4,4,64,2048]{4,3,2,1,0:T(8,128)(2,1)} %bitcast.89, f32[2,4,4,64,3]{4,3,2,1,0:T(8,128)} %bitcast.83), custom_call_target="tpu_custom_call" | custom-call | flops 6000000000 | bytes 17000000 | tf_op jit(solution)/shard_map/pallas_call | solution.py:26
  112.6 4.7 %shard_map.107 = (bf16[3,224,2048]{2,1,0:T(8,128)(2,1)}, bf16[3,256,2048]{2,1,0:T(8,128)(2,1)S(1)}) custom-call(s32[5]{0:T(128)S(1)} %copy-done.1, bf16[3,224,512]{2,1,0:T(8,128)(2,1)S(1)} %convert_element_type.462.refs_0_, bf16[3,224,512]{2,1,0:T(8,128)(2,1)} %collective-permute-done.14.refs_1_, bf16[3,224,512]{2,1,0:T(8,128)(2,1)} %collective-permute-done.15.refs_2_, ...), custom_call_target="tpu_custom_call" | custom-call | flops 2000000000 | bytes 8000000 | tf_op jit(solution)/shard_map/pallas_call | solution.py:26
  117.3 26.0 %shard_map.109 = (bf16[1024,512]{1,0:T(8,128)(2,1)S(1)}, bf16[1024,512]{1,0:T(8,128)(2,1)S(1)}, bf16[1024,512]{1,0:T(8,128)(2,1)S(1)}, bf16[1024,512]{1,0:T(8,12...) custom-call(s32[5]{0:T(128)S(1)} %copy-done.1, ...), custom_call_target="tpu_custom_call" | custom-call | flops 19327352832 | bytes 25000000 | tf_op jit(solution)/shard_map/pallas_call | solution.py:26
  149.7 18.5 %collective-permute-done.17 = bf16[1024,512]{1,0:T(8,128)(2,1)S(1)} collective-permute-done((bf16[1024,512]{1,0:T(8,128)(2,1)S(1)}, bf16[1024,512]{1,0:T(8,128)(2,1)S(1)}, u32[]{:S(2)}, u32[]{:S(2)}) %collective-permute-start.17) | collective-permute-done | bytes 1048608 | tf_op jit(solution)/shard_map/ppermute | solution.py:285
  168.3 2.6 %collective-permute-start.18 = (bf16[1,4,2,64,512]{4,3,2,1,0:T(8,128)(2,1)S(1)}, bf16[1,4,2,64,512]{4,3,2,1,0:T(8,128)(2,1)S(1)}, u32[]{:S(2)}, u32[]{:S(2)}) collective-permute-start(bf16[1,4,2,64,512]{4,3,2,1,0:T(8,128)(2,1)S(1)} %bitcast.87), channel_id=1, source_target_pairs={{0,24},{8,16},{16,8},{24,0},{1,25},{9,17},{17,9},{25,1},{2,26},{10... | collective-permute-start | bytes 1572872 | tf_op jit(solution)/shard_map/ppermute | solution.py:285
  171.0 2.5 %collective-permute-start.22 = (bf16[1,4,2,64,512]{4,3,2,1,0:T(8,128)(2,1)S(1)}, bf16[1,4,2,64,512]{4,3,2,1,0:T(8,128)(2,1)S(1)}, u32[]{:S(2)}, u32[]{:S(2)}) collective-permute-start(bf16[1,4,2,64,512]{4,3,2,1,0:T(8,128)(2,1)S(1)} %bitcast.86), channel_id=1, source_target_pairs={{0,6},{2,4},{4,2},{6,0},{1,7},{3,5},{5,3},{7,1},{8,14},{10,12},{12... | collective-permute-start | bytes 1572872 | tf_op jit(solution)/shard_map/ppermute | solution.py:285
  174.2 8.1 %collective-permute-done.18 = bf16[1,4,2,64,512]{4,3,2,1,0:T(8,128)(2,1)S(1)} collective-permute-done((bf16[1,4,2,64,512]{4,3,2,1,0:T(8,128)(2,1)S(1)}, bf16[1,4,2,64,512]{4,3,2,1,0:T(8,128)(2,1)S(1)}, u32[]{:S(2)}, u32[]{:S(2)}) %collective-permute-start.18) | collective-permute-done | bytes 524320 | tf_op jit(solution)/shard_map/ppermute | solution.py:285
  188.7 2.7 %collective-permute-done.19 = bf16[1,2,2,64,512]{4,3,2,1,0:T(8,128)(2,1)S(1)} collective-permute-done((bf16[1,2,2,64,512]{4,3,2,1,0:T(8,128)(2,1)S(1)}, bf16[1,2,2,64,512]{4,3,2,1,0:T(8,128)(2,1)S(1)}, u32[]{:S(2)}, u32[]{:S(2)}) %collective-permute-start.19) | collective-permute-done | bytes 262176 | tf_op jit(solution)/shard_map/ppermute | solution.py:285
  199.6 2.3 %collective-permute-start.33 = (bf16[64,2048]{1,0:T(8,128)(2,1)S(1)}, bf16[64,2048]{1,0:T(8,128)(2,1)S(1)}, u32[]{:S(2)}, u32[]{:S(2)}) collective-permute-start(bf16[64,2048]{1,0:T(8,128)(2,1)S(1)} %pad_maximum_fusion.5), channel_id=1, source_target_pairs={{0,32},{32,0},{1,33},{33,1},{2,34},{34,2},{3,35},{35,3},{4,36},{36... | collective-permute-start | bytes 786440 | tf_op jit(solution)/shard_map/ppermute | solution.py:285
  201.8 5.3 %shard_map.106 = (bf16[3,224,2048]{2,1,0:T(8,128)(2,1)}, bf16[3,224,2048]{2,1,0:T(8,128)(2,1)}) custom-call(s32[5]{0:T(128)S(1)} %copy-done.1, bf16[2,112,2048]{2,1,0:T(8,128)(2,1)} %shard_map.103.refs_0_.refs_3_, bf16[2,112,2048]{2,1,0:T(8,128)(2,1)} %collective-permute-done.4.refs_1_.refs_4_, bf16[2,112,2048]{2,1,0:T(8,128)(2,1)} %shard_map.104.refs_2_.refs_5_, ...), custom_call_target="tpu_custom_call" | custom-call | flops 4000000000 | bytes 11000000 | tf_op jit(solution)/shard_map/pallas_call | solution.py:26
  (114 shorter events, 49.6 us)
Async XLA Ops:
  10.2 16.1 %collective-permute-start.10 = (bf16[16,112,128]{2,1,0:T(8,128)(2,1)S(1)}, bf16[16,112,128]{2,1,0:T(8,128)(2,1)S(1)}, u32[]{:S(2)}, u32[]{:S(2)}) collective-permute-start(bf16[16,112,128]{2,1,0:T(8,128)(2,1)S(1)} %maximum_select_fusion.1), channel_id=1, source_target_pairs={{32,0},{64,32},{0,96},{33,1},{65,33},{1,97},{34,2},{66,34},{2,98},... | collective-permute-start | bytes 1376264 | tf_op jit(solution)/shard_map/ppermute | solution.py:377
  16.0 14.5 %collective-permute-start.11 = (bf16[16,112,128]{2,1,0:T(8,128)(2,1)S(1)}, bf16[16,112,128]{2,1,0:T(8,128)(2,1)S(1)}, u32[]{:S(2)}, u32[]{:S(2)}) collective-permute-start(bf16[16,112,128]{2,1,0:T(8,128)(2,1)S(1)} %maximum_select_fusion.1), channel_id=1, source_target_pairs={{32,64},{64,96},{96,0},{33,65},{65,97},{97,1},{34,66},{66,98},{98,... | collective-permute-start | bytes 1376264 | tf_op jit(solution)/shard_map/ppermute | solution.py:378
  19.6 21.4 %all-to-all-start = ((bf16[16,2,112,128]{3,2,1,0:T(8,128)(2,1)}), bf16[16,2,112,128]{3,2,1,0:T(8,128)(2,1)S(1)}, u32[]{:S(2)}, u32[]{:S(2)}) async-start(bf16[16,2,112,128]{3,2,1,0:T(8,128)(2,1)} %maximum_select_fusion), calls=%async_computation | async-start | bytes 1835008 | tf_op jit(solution)/shard_map/all_to_all | solution.py:361
  31.4 15.9 %collective-permute-start.12 = (bf16[16,112,128]{2,1,0:T(8,128)(2,1)}, bf16[16,112,128]{2,1,0:T(8,128)(2,1)}, u32[]{:S(2)}, u32[]{:S(2)}) collective-permute-start(bf16[16,112,128]{2,1,0:T(8,128)(2,1)} %broadcast_select_fusion), channel_id=1, source_target_pairs={{96,64},{0,32},{97,65},{1,33},{98,66},{2,34},{99,67},{3,35},{100,6... | collective-permute-start | bytes 1376264 | tf_op jit(solution)/shard_map/ppermute | solution.py:380
  41.0 21.9 %collective-permute-start.5 = (bf16[16,112,128]{2,1,0:T(8,128)(2,1)S(1)}, bf16[16,112,128]{2,1,0:T(8,128)(2,1)S(1)}, u32[]{:S(2)}, u32[]{:S(2)}) collective-permute-start(bf16[16,112,128]{2,1,0:T(8,128)(2,1)S(1)} %get-tuple-element.62.refs_0_), channel_id=1, source_target_pairs={{32,0},{64,32},{0,96},{33,1},{65,33},{1,97},{34,2},{66,34},{2,98},... | collective-permute-start | bytes 1376264 | tf_op jit(solution)/shard_map/ppermute | solution.py:377
  46.0 17.0 %collective-permute-start.6 = (bf16[16,112,128]{2,1,0:T(8,128)(2,1)S(1)}, bf16[16,112,128]{2,1,0:T(8,128)(2,1)S(1)}, u32[]{:S(2)}, u32[]{:S(2)}) collective-permute-start(bf16[16,112,128]{2,1,0:T(8,128)(2,1)S(1)} %get-tuple-element.62.refs_0_), channel_id=1, source_target_pairs={{32,64},{64,96},{96,0},{33,65},{65,97},{97,1},{34,66},{66,98},{98,... | collective-permute-start | bytes 1376264 | tf_op jit(solution)/shard_map/ppermute | solution.py:378
  48.7 20.5 %collective-permute-start.1 = (bf16[16,112,128]{2,1,0:T(8,128)(2,1)S(1)}, bf16[16,112,128]{2,1,0:T(8,128)(2,1)}, u32[]{:S(2)}, u32[]{:S(2)}) collective-permute-start(bf16[16,112,128]{2,1,0:T(8,128)(2,1)S(1)} %get-tuple-element.63.refs_0_), channel_id=1, source_target_pairs={{32,0},{64,32},{0,96},{33,1},{65,33},{1,97},{34,2},{66,34},{2,98},... | collective-permute-start | bytes 1376264 | tf_op jit(solution)/shard_map/ppermute | solution.py:377
  53.9 17.5 %collective-permute-start.2 = (bf16[16,112,128]{2,1,0:T(8,128)(2,1)S(1)}, bf16[16,112,128]{2,1,0:T(8,128)(2,1)}, u32[]{:S(2)}, u32[]{:S(2)}) collective-permute-start(bf16[16,112,128]{2,1,0:T(8,128)(2,1)S(1)} %get-tuple-element.63.refs_0_), channel_id=1, source_target_pairs={{32,64},{64,96},{96,0},{33,65},{65,97},{97,1},{34,66},{66,98},{98,... | collective-permute-start | bytes 1376264 | tf_op jit(solution)/shard_map/ppermute | solution.py:378
  56.2 19.1 %all-to-all-start.1 = ((bf16[16,2,112,128]{3,2,1,0:T(8,128)(2,1)}), bf16[16,2,112,128]{3,2,1,0:T(8,128)(2,1)S(1)}, u32[]{:S(2)}, u32[]{:S(2)}) async-start(bf16[16,2,112,128]{3,2,1,0:T(8,128)(2,1)} %pad_maximum_fusion), calls=%async_computation.1 | async-start | bytes 1835008 | tf_op jit(solution)/shard_map/all_to_all | solution.py:361
  61.7 39.9 %collective-permute-start.14 = (bf16[3,224,512]{2,1,0:T(8,128)(2,1)S(1)}, bf16[3,224,512]{2,1,0:T(8,128)(2,1)}, u32[]{:S(2)}, u32[]{:S(2)}) collective-permute-start(bf16[3,224,512]{2,1,0:T(8,128)(2,1)S(1)} %convert_element_type.462.refs_0_), channel_id=1, source_target_pairs={{0,64},{64,0},{1,65},{65,1},{2,66},{66,2},{3,67},{67,3},{4,68},{68... | collective-permute-start | bytes 2064392 | tf_op jit(solution)/shard_map/ppermute | solution.py:285
  63.8 28.7 %collective-permute-start.7 = (bf16[16,112,128]{2,1,0:T(8,128)(2,1)}, bf16[16,112,128]{2,1,0:T(8,128)(2,1)}, u32[]{:S(2)}, u32[]{:S(2)}) collective-permute-start(bf16[16,112,128]{2,1,0:T(8,128)(2,1)} %broadcast_select_fusion.1), channel_id=1, source_target_pairs={{96,64},{0,32},{97,65},{1,33},{98,66},{2,34},{99,67},{3,35},{100,6... | collective-permute-start | bytes 1376264 | tf_op jit(solution)/shard_map/ppermute | solution.py:380
  73.3 22.1 %collective-permute-start.3 = (bf16[16,112,128]{2,1,0:T(8,128)(2,1)}, bf16[16,112,128]{2,1,0:T(8,128)(2,1)}, u32[]{:S(2)}, u32[]{:S(2)}) collective-permute-start(bf16[16,112,128]{2,1,0:T(8,128)(2,1)} %broadcast_select_fusion.2), channel_id=1, source_target_pairs={{96,64},{0,32},{97,65},{1,33},{98,66},{2,34},{99,67},{3,35},{100,6... | collective-permute-start | bytes 1376264 | tf_op jit(solution)/shard_map/ppermute | solution.py:380
  77.2 40.1 %collective-permute-start.13 = (bf16[2,112,2048]{2,1,0:T(8,128)(2,1)}, bf16[2,112,2048]{2,1,0:T(8,128)(2,1)S(1)}, u32[]{:S(2)}, u32[]{:S(2)}) collective-permute-start(bf16[2,112,2048]{2,1,0:T(8,128)(2,1)} %shard_map.105.refs_4_.refs_7_), channel_id=1, source_target_pairs={{0,1},{1,0},{2,3},{3,2},{4,5},{5,4},{6,7},{7,6},{8,9},{9,8},{10,11... | collective-permute-start | bytes 2752520 | tf_op jit(solution)/shard_map/ppermute | solution.py:285
  95.4 21.9 %collective-permute-start.8 = (bf16[2,112,2048]{2,1,0:T(8,128)(2,1)}, bf16[2,112,2048]{2,1,0:T(8,128)(2,1)S(1)}, u32[]{:S(2)}, u32[]{:S(2)}) collective-permute-start(bf16[2,112,2048]{2,1,0:T(8,128)(2,1)} %shard_map.104.refs_2_.refs_5_), channel_id=1, source_target_pairs={{0,1},{1,0},{2,3},{3,2},{4,5},{5,4},{6,7},{7,6},{8,9},{9,8},{10,11... | collective-permute-start | bytes 2752520 | tf_op jit(solution)/shard_map/ppermute | solution.py:285
  98.5 18.8 %collective-permute-start.4 = (bf16[2,112,2048]{2,1,0:T(8,128)(2,1)}, bf16[2,112,2048]{2,1,0:T(8,128)(2,1)}, u32[]{:S(2)}, u32[]{:S(2)}) collective-permute-start(bf16[2,112,2048]{2,1,0:T(8,128)(2,1)} %shard_map.103.refs_0_.refs_3_), channel_id=1, source_target_pairs={{0,1},{1,0},{2,3},{3,2},{4,5},{5,4},{6,7},{7,6},{8,9},{9,8},{10,11... | collective-permute-start | bytes 2752520 | tf_op jit(solution)/shard_map/ppermute | solution.py:285
  101.6 11.0 %collective-permute-start.15 = (bf16[3,224,512]{2,1,0:T(8,128)(2,1)S(1)}, bf16[3,224,512]{2,1,0:T(8,128)(2,1)}, u32[]{:S(2)}, u32[]{:S(2)}) collective-permute-start(bf16[3,224,512]{2,1,0:T(8,128)(2,1)S(1)} %convert_element_type.462.refs_0_), channel_id=1, source_target_pairs={{0,1},{1,0},{2,3},{3,2},{4,5},{5,4},{6,7},{7,6},{8,9},{9,8},{10,11... | collective-permute-start | bytes 2064392 | tf_op jit(solution)/shard_map/ppermute | solution.py:285
  143.4 24.8 %collective-permute-start.17 = (bf16[1024,512]{1,0:T(8,128)(2,1)S(1)}, bf16[1024,512]{1,0:T(8,128)(2,1)S(1)}, u32[]{:S(2)}, u32[]{:S(2)}) collective-permute-start(bf16[1024,512]{1,0:T(8,128)(2,1)S(1)} %get-tuple-element.37), channel_id=1, source_target_pairs={{0,8},{8,0},{16,24},{24,16},{1,9},{9,1},{17,25},{25,17},{2,10},{10... | collective-permute-start | bytes 3145736 | tf_op jit(solution)/shard_map/ppermute | solution.py:285
  144.8 26.1 %collective-permute-start.21 = (bf16[1024,512]{1,0:T(8,128)(2,1)S(1)}, bf16[1024,512]{1,0:T(8,128)(2,1)S(1)}, u32[]{:S(2)}, u32[]{:S(2)}) collective-permute-start(bf16[1024,512]{1,0:T(8,128)(2,1)S(1)} %get-tuple-element.39), channel_id=1, source_target_pairs={{0,2},{2,0},{4,6},{6,4},{1,3},{3,1},{5,7},{7,5},{8,10},{10,8},{12,... | collective-permute-start | bytes 3145736 | tf_op jit(solution)/shard_map/ppermute | solution.py:285
  146.0 27.6 %collective-permute-start.25 = (bf16[1024,512]{1,0:T(8,128)(2,1)S(1)}, bf16[1024,512]{1,0:T(8,128)(2,1)S(1)}, u32[]{:S(2)}, u32[]{:S(2)}) collective-permute-start(bf16[1024,512]{1,0:T(8,128)(2,1)S(1)} %get-tuple-element.41), channel_id=1, source_target_pairs={{0,24},{8,16},{16,8},{24,0},{1,25},{9,17},{17,9},{25,1},{2,26},{10... | collective-permute-start | bytes 3145736 | tf_op jit(solution)/shard_map/ppermute | solution.py:285
  147.8 26.0 %collective-permute-start.29 = (bf16[1024,512]{1,0:T(8,128)(2,1)S(1)}, bf16[1024,512]{1,0:T(8,128)(2,1)S(1)}, u32[]{:S(2)}, u32[]{:S(2)}) collective-permute-start(bf16[1024,512]{1,0:T(8,128)(2,1)S(1)} %get-tuple-element.43), channel_id=1, source_target_pairs={{0,6},{2,4},{4,2},{6,0},{1,7},{3,5},{5,3},{7,1},{8,14},{10,12},{12... | collective-permute-start | bytes 3145736 | tf_op jit(solution)/shard_map/ppermute | solution.py:285
  168.3 14.0 %collective-permute-start.18 = (bf16[1,4,2,64,512]{4,3,2,1,0:T(8,128)(2,1)S(1)}, bf16[1,4,2,64,512]{4,3,2,1,0:T(8,128)(2,1)S(1)}, u32[]{:S(2)}, u32[]{:S(2)}) collective-permute-start(bf16[1,4,2,64,512]{4,3,2,1,0:T(8,128)(2,1)S(1)} %bitcast.87), channel_id=1, source_target_pairs={{0,24},{8,16},{16,8},{24,0},{1,25},{9,17},{17,9},{25,1},{2,26},{10... | collective-permute-start | bytes 1572872 | tf_op jit(solution)/shard_map/ppermute | solution.py:285
  171.0 13.6 %collective-permute-start.22 = (bf16[1,4,2,64,512]{4,3,2,1,0:T(8,128)(2,1)S(1)}, bf16[1,4,2,64,512]{4,3,2,1,0:T(8,128)(2,1)S(1)}, u32[]{:S(2)}, u32[]{:S(2)}) collective-permute-start(bf16[1,4,2,64,512]{4,3,2,1,0:T(8,128)(2,1)S(1)} %bitcast.86), channel_id=1, source_target_pairs={{0,6},{2,4},{4,2},{6,0},{1,7},{3,5},{5,3},{7,1},{8,14},{10,12},{12... | collective-permute-start | bytes 1572872 | tf_op jit(solution)/shard_map/ppermute | solution.py:285
  173.7 12.1 %collective-permute-start.26 = (bf16[1,4,2,64,512]{4,3,2,1,0:T(8,128)(2,1)S(1)}, bf16[1,4,2,64,512]{4,3,2,1,0:T(8,128)(2,1)S(1)}, u32[]{:S(2)}, u32[]{:S(2)}) collective-permute-start(bf16[1,4,2,64,512]{4,3,2,1,0:T(8,128)(2,1)S(1)} %bitcast.85), channel_id=1, source_target_pairs={{0,8},{8,0},{16,24},{24,16},{1,9},{9,1},{17,25},{25,17},{2,10},{10... | collective-permute-start | bytes 1572872 | tf_op jit(solution)/shard_map/ppermute | solution.py:285
  173.9 13.6 %collective-permute-start.30 = (bf16[1,4,2,64,512]{4,3,2,1,0:T(8,128)(2,1)S(1)}, bf16[1,4,2,64,512]{4,3,2,1,0:T(8,128)(2,1)S(1)}, u32[]{:S(2)}, u32[]{:S(2)}) collective-permute-start(bf16[1,4,2,64,512]{4,3,2,1,0:T(8,128)(2,1)S(1)} %bitcast.84), channel_id=1, source_target_pairs={{0,2},{2,0},{4,6},{6,4},{1,3},{3,1},{5,7},{7,5},{8,10},{10,8},{12,... | collective-permute-start | bytes 1572872 | tf_op jit(solution)/shard_map/ppermute | solution.py:285
  (19 other events, 137.1 us)

commit v5 on v2

--- a/solution.py
+++ b/solution.py
@@ -11,14 +11,16 @@
 Z = ("gr", "fs_0")
 UNITS = 256
 MIB = 1024 * 1024
-LAST_VMEM = 40
+LAST_VMEM = 32
 
 
 COLORS = (
-    ((1, 1), (1, 3), (2, 1), (2, 3)),
-    ((2, 1), (2, 3), (1, 1), (1, 3)),
-    ((1, 3), (1, 1), (2, 3), (2, 1)),
-    ((2, 3), (2, 1), (1, 3), (1, 1)),
+    (((1, 1), (1, 3), (2, 1), (2, 3)), 384),
+    (((2, 1), (2, 3), (1, 1), (1, 3)), 384),
+    (((1, 3), (1, 1), (2, 3), (2, 1)), 384),
+    (((2, 3), (2, 1), (1, 3), (1, 1)), 384),
+    (((0, 1), (1, 1), (1, 3), (2, 3), (2, 1)), 256),
+    (((0, 1), (2, 1), (2, 3), (1, 3), (1, 1)), 256),
 )
 
 
@@ -232,36 +234,48 @@
     rows = jnp.concatenate(hidden, axis=1)
     block = rows.shape[0]
     ys = pl.num_programs(0)
-    width = outs[0].shape[1]
-    for color, exchanges in enumerate(COLORS):
-        at = slice(color * width, (color + 1) * width)
-        product = jnp.dot(rows, down_ref[:, at], preferred_element_type=jnp.float32)
-        product = product.astype(jnp.bfloat16)
-        send_ref, keep_ref = outs[2 * color : 2 * color + 2]
-        axis, mask = exchanges[0]
-        if axis == 1:
-            kept = (yy == 0) | (yy == 4 - mask)
-            later = jnp.where((yy == 4 - mask) | (yy == 2), block, 0)
-            to = pl.ds(pl.multiple_of(later, block), block)
-
-            @pl.when(kept)
-            def _():
-                keep_ref[to, :] = product
-
-            @pl.when(jnp.logical_not(kept))
-            def _():
-                send_ref[to, :] = product
-
-        else:
-            part = block // 4
-            for xx, ref, k in ((0, keep_ref, 0), (4 - mask, keep_ref, 1), (mask, send_ref, 0), (2, send_ref, 1)):
-                to = pl.ds(pl.multiple_of((k * ys + yy) * part, part), part)
-                ref[to, :] = product[xx * part : (xx + 1) * part]
+    start, place = 0, 0
+    for color in range(0, len(COLORS), 2):
+        columns = sum(width for _, width in COLORS[color : color + 2])
+        at = slice(start, start + columns)
+        start += columns
+        both = jnp.dot(rows, down_ref[:, at], preferred_element_type=jnp.float32)
+        both = both.astype(jnp.bfloat16)
+        used = 0
+        for exchanges, width in COLORS[color : color + 2]:
+            product = both[:, used : used + width]
+            used += width
+            axis, mask = exchanges[0]
+            count = 3 if axis else 2
+            send_ref, keep_refs = outs[place], outs[place + 1 : place + count]
+            place += count
+            moves = ((0, keep_refs[0], 0), (4 - mask, keep_refs[-1], 0), (mask, send_ref, 0), (2, send_ref, 1))
+            if axis == 1:
+                for at_y, ref, k in moves:
+
+                    @pl.when(yy == at_y)
+                    def _():
+                        ref[k * block : (k + 1) * block, :] = product
+
+            elif axis == 2:
+                part = block // 4
+                for xx, ref, k in moves:
+                    to = pl.ds(pl.multiple_of((k * ys + yy) * part, part), part)
+                    ref[to, :] = product[xx * part : (xx + 1) * part]
+            else:
+                part = block // 8
+                for index in range(8):
+                    ref = send_ref if index % 2 else keep_refs[0]
+                    to = pl.ds(pl.multiple_of((yy * 4 + index // 2) * part, part), part)
+                    ref[to, :] = product[index * part : (index + 1) * part]
 
 
 def last(where, normed, mix, early, sides, down):
     ys, rows, width = normed.shape
-    half = (ys * rows // 2, width // len(COLORS))
+    outs = []
+    for exchanges, columns in COLORS:
+        half, quarter = (ys * rows // 2, columns), (ys * rows // 4, columns)
+        outs += [half, quarter, quarter] if exchanges[0][0] else [half, half]
     at = lambda i, w: (i, 0, 0)
     side = whole(sides[0].shape)
     weight = pltpu.VMEM((UNITS, width), jnp.bfloat16)
@@ -269,7 +283,7 @@
         last_kernel, (ys,),
         [pl.BlockSpec((1, rows, width), at), pl.BlockSpec((1, rows, mix.shape[-1]), at)]
         + [pl.BlockSpec((1, rows, UNITS), at)] + [side] * 4 + [whole(down.shape)],
-        [whole(half)] * (2 * len(COLORS)), [shaped(*half)] * (2 * len(COLORS)),
+        [whole(out) for out in outs], [shaped(*out) for out in outs],
         (where, normed, mix, early, *sides, down), 14 * ys * rows * width * UNITS, 25e6,
         scratch=(weight,) * 4, vmem=LAST_VMEM,
     )
@@ -288,7 +302,7 @@
 
 
 class Sums:
-    def __init__(self, send, keep, exchanges):
+    def __init__(self, send, keeps, exchanges):
         axis, mask = exchanges[0]
         self.axes = (axis, *(a for a in (1, 2, 0) if a != axis))
         sizes = [2 if a == 0 else 4 for a in self.axes]
@@ -298,13 +312,16 @@
         self.offsets = [[0, 1, 2, 3] if a else [0, 1] for a in self.axes]
         self.offsets[0] = [0, 4 - mask] if axis else [0]
         places = [list(range(size)) for size in sizes]
-        self.terms = [(keep.reshape(shape), places), (came, [list(p) for p in places])]
+        keeps = [keep.reshape(1, *shape[1:]) for keep in keeps]
+        self.terms = [(keeps, places), (came, [list(p) for p in places])]
 
     def at(self, dim, index):
         parts = []
         for array, places in self.terms:
             for d, place in enumerate(places):
-                if d == dim:
+                if isinstance(array, list):
+                    array = array[place[index if dim == 0 else 0]]
+                elif d == dim:
                     array = lax.slice_in_dim(array, place[index], place[index] + 1, axis=d)
                 elif len(place) < array.shape[d]:
                     array = lax.slice_in_dim(array, place[0], place[0] + 1, axis=d)
@@ -348,15 +365,17 @@
     blocks = jnp.where(
         tp == 0, jnp.concatenate([own, came], axis=0), jnp.concatenate([came, own], axis=0)
     )
+    combine = mixing(route[0], route_weight[0], experts)
+    blocks, combine = lax.optimization_barrier((blocks, combine))
     mine = lax.all_to_all(blocks, PLANE, split_axis=0, concat_axis=0, tiled=True)
 
     down_own = down_master.astype(jnp.bfloat16)
     down_far = swap(down_own, "gr", 1)
-    down_own_core, down_far_core = other_core(down_own), other_core(down_far)
-
-    _, width = tokens.shape[1:]
+    down_own_core = other_core(down_own)
+    down_far_core = other_core(down_far)
+
+    count, width = tokens.shape[1:]
     places = [lax.axis_size(a) for a in FS]
-    combine = mixing(route[0], route_weight[0], experts)
     normed, mix = norm(
         where, tokens.reshape(*places, -1, width), combine.reshape(*places, -1, experts)
     )
@@ -375,16 +394,22 @@
         sides += [own, other_core(own)]
     early = hidden_units(where, normed, mix, sides[0], sides[1], 0)
     outs = last(where, normed, mix, early, sides[2:], down_padded.reshape(-1, width))
-    sums = []
-    for color, exchanges in enumerate(COLORS):
-        sums.append(Sums(outs[2 * color], outs[2 * color + 1], exchanges))
-    for step in range(1, 4):
-        for color, exchanges in zip(sums, COLORS):
-            color.exchange(*exchanges[step])
-    sent = jnp.concatenate([c.block(2, 1).astype(jnp.bfloat16) for c in sums], axis=1)
-    came = swap(sent, "fs_0", 1)
-    mine = jnp.concatenate([c.block(2, 0) for c in sums], axis=1)
-    mixed = added([mine, came]).astype(jnp.bfloat16)[None]
+    sums, place = [], 0
+    for exchanges, _ in COLORS:
+        count = 3 if exchanges[0][0] else 2
+        sums.append(Sums(outs[place], outs[place + 1 : place + count], exchanges))
+        place += count
+    for step in range(1, 5):
+        for color, (exchanges, _) in enumerate(COLORS):
+            if step < len(exchanges):
+                sums[color].exchange(*exchanges[step])
+    columns = []
+    for pair in (sums[0:2], sums[2:4]):
+        sent = jnp.concatenate([c.block(2, 1).astype(jnp.bfloat16) for c in pair], axis=1)
+        came = swap(sent, "fs_0", 1)
+        columns.append(added([jnp.concatenate([c.block(2, 0) for c in pair], axis=1), came]))
+    columns += [c.block(0, 0) for c in sums[4:]]
+    mixed = jnp.concatenate(columns, axis=1).astype(jnp.bfloat16)[None]
     gate_t, up_t = assemble(where, sides)
     return (jnp.swapaxes(gate_t, 1, 2), jnp.swapaxes(up_t, 1, 2), down_out, mixed)
 

time: 215 us -> 246 us (1.14)
  waiting for transfers between devices: 90.6 us -> 110 us
  starting transfers between devices: 56.9 us -> 70.7 us
    ppermute x24 -> x35, waiting for transfers between devices: 40.3 us -> 59.2 us  [swap(): return lax.ppermute(array, axis, [(i, i ^ mask) for i in range(peers)])]
    ppermute x24 -> x35, starting transfers between devices: 27.7 us -> 41.7 us  [swap(): return lax.ppermute(array, axis, [(i, i ^ mask) for i in range(peers)])]
  transfers between devices with their start and end apart: 34 -> 45, of which waited for: 19 -> 21; matrix products, arithmetic and copies ran while one was open for 2% -> 2% of each run, Pallas kernels for 13% -> 11%
where the time goes in v5:
time: 246 us; the launch traced here: 245 us
  waiting for transfers between devices  110 us (45%)
  starting transfers between devices  70.7 us (29%)
  Pallas kernels  55.1 us (22%)
  other arithmetic  5.55 us (2%)
  local copies, waits for them, and re-layouts  3.01 us (1%)
    ppermute x35, waiting for transfers between devices, swap(): return lax.ppermute(array, axis, [(i, i ^ mask) for i in range(peers)])  59.2 us
    pallas_call x9, Pallas kernels, call(): pl.pallas_call(kernel, out_shape=out_shape, grid_spec=pltpu.PrefetchScala...  55.1 us
    ppermute x35, starting transfers between devices, swap(): return lax.ppermute(array, axis, [(i, i ^ mask) for i in range(peers)])  41.7 us
    ppermute x3, waiting for transfers between devices, program(): above = lax.ppermute(piece, Z, [(1, 2), (2, 3), (3, 0)])  24 us
    ppermute x3, waiting for transfers between devices, program(): far = lax.ppermute(passed, Z, [(3, 2), (0, 1)])  15.7 us
    ppermute x3, starting transfers between devices, program(): below = lax.ppermute(piece, Z, [(1, 0), (2, 1), (0, 3)])  10.3 us
    all_to_all x1, waiting for transfers between devices, program(): lax.all_to_all(blocks, PLANE, split_axis=0, concat_axis=0, tiled=True)  9.36 us
    all_to_all x1, starting transfers between devices, program(): lax.all_to_all(blocks, PLANE, split_axis=0, concat_axis=0, tiled=True)  7.48 us
  transfers between devices with their start and end apart: 45, of which 21 were waited for; matrix products, arithmetic and copies ran while one was open for 2% of the time, Pallas kernels for 11%

profile of v5, /device:TPU:66, one launch (start us, length us, event | category | flops | bytes accessed | tf_op | source)
XLA Modules:
  0.0 245.2 jit_solution(15855759100416950326)
XLA Ops:
  1.3 4.9 %shard_map.102 = (bf16[8,3,112,128]{3,2,1,0:T(8,128)(2,1)}, bf16[8,3,112,128]{3,2,1,0:T(8,128)(2,1)}) custom-call(s32[5]{0:T(128)} %stack.23.where_ref.refs_0_, f32[3,64,1792]{2,1,0:T(8,128)} %gate_ref.1, f32[3,64,1792]{2,1,0:T(8,128)} %up_ref.1, f32[1,64]{1,0:T(1,128)} %bitcast.112), custom_call_target="tpu_custom_call" | custom-call | flops 3000000000 | bytes 6000000 | tf_op jit(solution)/shard_map/pallas_call | solution.py:28
  11.1 7.5 %all-to-all-start = ((bf16[16,3,112,128]{3,2,1,0:T(8,128)(2,1)}), bf16[16,3,112,128]{3,2,1,0:T(8,128)(2,1)S(1)}, u32[]{:S(2)}, u32[]{:S(2)}) async-start(bf16[16,3,112,128]{3,2,1,0:T(8,128)(2,1)} %maximum_select_fusion), calls=%async_computation | async-start | bytes 2752512 | tf_op jit(solution)/shard_map/all_to_all | solution.py:370
  20.0 9.0 %shard_map.103 = (bf16[4,512,2048]{2,1,0:T(8,128)(2,1)}, f32[4,512,3]{2,1,0:T(8,128)}) custom-call(s32[5]{0:T(128)} %stack.23.where_ref.refs_0_, bf16[2,4,4,64,2048]{4,3,2,1,0:T(8,128)(2,1)} %bitcast.111, f32[2,4,4,64,3]{4,3,2,1,0:T(8,128)} %bitcast.95), custom_call_target="tpu_custom_call" | custom-call | flops 6000000000 | bytes 17000000 | tf_op jit(solution)/shard_map/pallas_call | solution.py:28
  29.0 9.4 %all-to-all-done = bf16[16,3,112,128]{3,2,1,0:T(8,128)(2,1)S(1)} async-done(((bf16[16,3,112,128]{3,2,1,0:T(8,128)(2,1)}), bf16[16,3,112,128]{3,2,1,0:T(8,128)(2,1)S(1)}, u32[]{:S(2)}, u32[]{:S(2)}) %all-to-all-start) | async-done | bytes 1376288 | tf_op jit(solution)/shard_map/all_to_all | solution.py:370
  39.2 3.5 %collective-permute-start.2 = (bf16[16,112,128]{2,1,0:T(8,128)(2,1)}, bf16[16,112,128]{2,1,0:T(8,128)(2,1)S(1)}, u32[]{:S(2)}, u32[]{:S(2)}) collective-permute-start(bf16[16,112,128]{2,1,0:T(8,128)(2,1)} %get-tuple-element.74.own_ref), channel_id=1, source_target_pairs={{32,64},{64,96},{96,0},{33,65},{65,97},{97,1},{34,66},{66,98},{98,... | collective-permute-start | bytes 1376264 | tf_op jit(solution)/shard_map/ppermute | solution.py:390
  47.0 4.0 %collective-permute-start.5 = (bf16[16,112,128]{2,1,0:T(8,128)(2,1)S(1)}, bf16[16,112,128]{2,1,0:T(8,128)(2,1)S(1)}, u32[]{:S(2)}, u32[]{:S(2)}) collective-permute-start(bf16[16,112,128]{2,1,0:T(8,128)(2,1)S(1)} %get-tuple-element.73.own_ref), channel_id=1, source_target_pairs={{32,0},{64,32},{0,96},{33,1},{65,33},{1,97},{34,2},{66,34},{2,98},... | collective-permute-start | bytes 1376264 | tf_op jit(solution)/shard_map/ppermute | solution.py:389
  54.0 15.5 %collective-permute-done.2.up_ref = bf16[16,112,128]{2,1,0:T(8,128)(2,1)S(1)} collective-permute-done((bf16[16,112,128]{2,1,0:T(8,128)(2,1)}, bf16[16,112,128]{2,1,0:T(8,128)(2,1)S(1)}, u32[]{:S(2)}, u32[]{:S(2)}) %collective-permute-start.2) | collective-permute-done | bytes 458784 | tf_op jit(solution)/shard_map/ppermute | solution.py:390
  71.3 4.0 %collective-permute-start.9 = (bf16[16,112,128]{2,1,0:T(8,128)(2,1)S(1)}, bf16[16,112,128]{2,1,0:T(8,128)(2,1)S(1)}, u32[]{:S(2)}, u32[]{:S(2)}) collective-permute-start(bf16[16,112,128]{2,1,0:T(8,128)(2,1)S(1)} %get-tuple-element.72.own_ref), channel_id=1, source_target_pairs={{32,0},{64,32},{0,96},{33,1},{65,33},{1,97},{34,2},{66,34},{2,98},... | collective-permute-start | bytes 1376264 | tf_op jit(solution)/shard_map/ppermute | solution.py:389
  75.4 3.9 %collective-permute-done.6.up_ref = bf16[16,112,128]{2,1,0:T(8,128)(2,1)S(1)} collective-permute-done((bf16[16,112,128]{2,1,0:T(8,128)(2,1)S(1)}, bf16[16,112,128]{2,1,0:T(8,128)(2,1)S(1)}, u32[]{:S(2)}, u32[]{:S(2)}) %collective-permute-start.6) | collective-permute-done | bytes 458784 | tf_op jit(solution)/shard_map/ppermute | solution.py:390
  82.1 4.7 %collective-permute-done.10.up_ref = bf16[16,112,128]{2,1,0:T(8,128)(2,1)S(1)} collective-permute-done((bf16[16,112,128]{2,1,0:T(8,128)(2,1)S(1)}, bf16[16,112,128]{2,1,0:T(8,128)(2,1)S(1)}, u32[]{:S(2)}, u32[]{:S(2)}) %collective-permute-start.10) | collective-permute-done | bytes 458784 | tf_op jit(solution)/shard_map/ppermute | solution.py:390
  89.3 5.2 %collective-permute-done.3.far_ref = bf16[16,112,128]{2,1,0:T(8,128)(2,1)S(1)} collective-permute-done((bf16[16,112,128]{2,1,0:T(8,128)(2,1)S(1)}, bf16[16,112,128]{2,1,0:T(8,128)(2,1)S(1)}, u32[]{:S(2)}, u32[]{:S(2)}) %collective-permute-start.3) | collective-permute-done | bytes 458784 | tf_op jit(solution)/shard_map/ppermute | solution.py:392
  97.2 6.6 %collective-permute-done.7.far_ref = bf16[16,112,128]{2,1,0:T(8,128)(2,1)S(1)} collective-permute-done((bf16[16,112,128]{2,1,0:T(8,128)(2,1)S(1)}, bf16[16,112,128]{2,1,0:T(8,128)(2,1)S(1)}, u32[]{:S(2)}, u32[]{:S(2)}) %collective-permute-start.7) | collective-permute-done | bytes 458784 | tf_op jit(solution)/shard_map/ppermute | solution.py:392
  104.8 3.9 %collective-permute-done.11.far_ref = bf16[16,112,128]{2,1,0:T(8,128)(2,1)S(1)} collective-permute-done((bf16[16,112,128]{2,1,0:T(8,128)(2,1)S(1)}, bf16[16,112,128]{2,1,0:T(8,128)(2,1)S(1)}, u32[]{:S(2)}, u32[]{:S(2)}) %collective-permute-start.11) | collective-permute-done | bytes 458784 | tf_op jit(solution)/shard_map/ppermute | solution.py:392
  109.9 3.9 %shard_map.108 = (bf16[3,224,2048]{2,1,0:T(8,128)(2,1)}, bf16[3,256,2048]{2,1,0:T(8,128)(2,1)S(1)}) custom-call(s32[5]{0:T(128)S(1)} %copy-done, bf16[3,224,512]{2,1,0:T(8,128)(2,1)S(1)} %convert_element_type.662.refs_0_, bf16[3,224,512]{2,1,0:T(8,128)(2,1)} %collective-permute-done.13.refs_1_, bf16[3,224,512]{2,1,0:T(8,128)(2,1)S(1)} %collective-permute-done.14.refs_2_, ...), custom_call_target="tpu_custom_call" | custom-call | flops 2000000000 | bytes 8000000 | tf_op jit(solution)/shard_map/pallas_call | solution.py:28
  113.8 7.9 %shard_map.109.early_ref = bf16[4,512,256]{2,1,0:T(8,128)(2,1)S(1)} custom-call(s32[5]{0:T(128)S(1)} %copy-done, bf16[4,512,2048]{2,1,0:T(8,128)(2,1)} %get-tuple-element.41.refs_1_.normed_ref, f32[4,512,3]{2,1,0:T(8,128)S(1)} %copy-done.1, bf16[2,112,2048]{2,1,0:T(8,128)(2,1)S(1)} %shard_map.104.refs_0_.refs_3_, ...), custom_call_target="tpu_custom_call" | custom-call | flops 4294967296 | bytes 12000000 | tf_op jit(solution)/shard_map/pallas_call | solution.py:28
  121.8 22.2 %shard_map.110 = (bf16[1024,384]{1,0:T(8,128)(2,1)S(1)}, bf16[512,384]{1,0:T(8,128)(2,1)S(1)}, bf16[512,384]{1,0:T(8,128)(2,1)S(1)}, bf16[1024,384]{1,0:T(8,128)...) custom-call(s32[5]{0:T(128)S(1)} %copy-done, ...), custom_call_target="tpu_custom_call" | custom-call | flops 15032385536 | bytes 25000000 | tf_op jit(solution)/shard_map/pallas_call | solution.py:28
  150.3 8.6 %collective-permute-done.34 = bf16[1024,256]{1,0:T(8,128)(2,1)S(1)} collective-permute-done((bf16[1024,256]{1,0:T(8,128)(2,1)S(1)}, bf16[1024,256]{1,0:T(8,128)(2,1)S(1)}, u32[]{:S(2)}, u32[]{:S(2)}) %collective-permute-start.34) | collective-permute-done | bytes 524320 | tf_op jit(solution)/shard_map/ppermute | solution.py:294
  159.2 10.4 %collective-permute-done.39 = bf16[1024,256]{1,0:T(8,128)(2,1)S(1)} collective-permute-done((bf16[1024,256]{1,0:T(8,128)(2,1)S(1)}, bf16[1024,256]{1,0:T(8,128)(2,1)S(1)}, u32[]{:S(2)}, u32[]{:S(2)}) %collective-permute-start.39) | collective-permute-done | bytes 524320 | tf_op jit(solution)/shard_map/ppermute | solution.py:294
  179.3 3.9 %collective-permute-start.41 = (bf16[1,4,1,64,256]{4,3,2,1,0:T(8,128)(2,1)S(1)}, bf16[1,4,1,64,256]{4,3,2,1,0:T(8,128)(2,1)S(1)}, u32[]{:S(2)}, u32[]{:S(2)}) collective-permute-start(bf16[1,4,1,64,256]{4,3,2,1,0:T(8,128)(2,1)S(1)} %add_convert_fusion.4), channel_id=1, source_target_pairs={{0,6},{2,4},{4,2},{6,0},{1,7},{3,5},{5,3},{7,1},{8,14},{10,12},{12... | collective-permute-start | bytes 393224 | tf_op jit(solution)/shard_map/ppermute | solution.py:294
  184.7 11.6 %collective-permute-done.29 = bf16[1024,384]{1,0:T(8,128)(2,1)S(1)} collective-permute-done((bf16[1024,384]{1,0:T(8,128)(2,1)S(1)}, bf16[1024,384]{1,0:T(8,128)(2,1)S(1)}, u32[]{:S(2)}, u32[]{:S(2)}) %collective-permute-start.29) | collective-permute-done | bytes 786464 | tf_op jit(solution)/shard_map/ppermute | solution.py:294
  202.1 5.2 %collective-permute-done.37 = bf16[1,1,2,64,256]{4,3,2,1,0:T(8,128)(2,1)S(1)} collective-permute-done((bf16[1,1,2,64,256]{4,3,2,1,0:T(8,128)(2,1)S(1)}, bf16[1,1,2,64,256]{4,3,2,1,0:T(8,128)(2,1)S(1)}, u32[]{:S(2)}, u32[]{:S(2)}) %collective-permute-start.37) | collective-permute-done | bytes 65568 | tf_op jit(solution)/shard_map/ppermute | solution.py:294
  208.6 4.2 %collective-permute-done.42 = bf16[1,2,1,64,256]{4,3,2,1,0:T(8,128)(2,1)S(1)} collective-permute-done((bf16[1,2,1,64,256]{4,3,2,1,0:T(8,128)(2,1)S(1)}, bf16[1,2,1,64,256]{4,3,2,1,0:T(8,128)(2,1)S(1)}, u32[]{:S(2)}, u32[]{:S(2)}) %collective-permute-start.42) | collective-permute-done | bytes 65568 | tf_op jit(solution)/shard_map/ppermute | solution.py:294
  216.7 4.2 %collective-permute-done.43 = bf16[1,1,1,64,256]{4,3,2,1,0:T(8,128)(2,1)S(1)} collective-permute-done((bf16[1,1,1,64,256]{4,3,2,1,0:T(8,128)(2,1)S(1)}, bf16[1,1,1,64,256]{4,3,2,1,0:T(8,128)(2,1)S(1)}, u32[]{:S(2)}, u32[]{:S(2)}) %collective-permute-start.43) | collective-permute-done | bytes 32800 | tf_op jit(solution)/shard_map/ppermute | solution.py:294
  240.4 4.0 %collective-permute-done.33 = bf16[64,768]{1,0:T(8,128)(2,1)S(1)} collective-permute-done((bf16[64,768]{1,0:T(8,128)(2,1)S(1)}, bf16[64,768]{1,0:T(8,128)(2,1)S(1)}, u32[]{:S(2)}, u32[]{:S(2)}) %collective-permute-start.33) | collective-permute-done | bytes 98336 | tf_op jit(solution)/shard_map/ppermute | solution.py:294
  (139 shorter events, 75.8 us)
Async XLA Ops:
  11.1 27.2 %all-to-all-start = ((bf16[16,3,112,128]{3,2,1,0:T(8,128)(2,1)}), bf16[16,3,112,128]{3,2,1,0:T(8,128)(2,1)S(1)}, u32[]{:S(2)}, u32[]{:S(2)}) async-start(bf16[16,3,112,128]{3,2,1,0:T(8,128)(2,1)} %maximum_select_fusion), calls=%async_computation | async-start | bytes 2752512 | tf_op jit(solution)/shard_map/all_to_all | solution.py:370
  39.2 30.2 %collective-permute-start.2 = (bf16[16,112,128]{2,1,0:T(8,128)(2,1)}, bf16[16,112,128]{2,1,0:T(8,128)(2,1)S(1)}, u32[]{:S(2)}, u32[]{:S(2)}) collective-permute-start(bf16[16,112,128]{2,1,0:T(8,128)(2,1)} %get-tuple-element.74.own_ref), channel_id=1, source_target_pairs={{32,64},{64,96},{96,0},{33,65},{65,97},{97,1},{34,66},{66,98},{98,... | collective-permute-start | bytes 1376264 | tf_op jit(solution)/shard_map/ppermute | solution.py:390
  42.7 28.6 %collective-permute-start.1 = (bf16[16,112,128]{2,1,0:T(8,128)(2,1)}, bf16[16,112,128]{2,1,0:T(8,128)(2,1)S(1)}, u32[]{:S(2)}, u32[]{:S(2)}) collective-permute-start(bf16[16,112,128]{2,1,0:T(8,128)(2,1)} %get-tuple-element.74.own_ref), channel_id=1, source_target_pairs={{32,0},{64,32},{0,96},{33,1},{65,33},{1,97},{34,2},{66,34},{2,98},... | collective-permute-start | bytes 1376264 | tf_op jit(solution)/shard_map/ppermute | solution.py:389
  45.1 34.2 %collective-permute-start.6 = (bf16[16,112,128]{2,1,0:T(8,128)(2,1)S(1)}, bf16[16,112,128]{2,1,0:T(8,128)(2,1)S(1)}, u32[]{:S(2)}, u32[]{:S(2)}) collective-permute-start(bf16[16,112,128]{2,1,0:T(8,128)(2,1)S(1)} %get-tuple-element.73.own_ref), channel_id=1, source_target_pairs={{32,64},{64,96},{96,0},{33,65},{65,97},{97,1},{34,66},{66,98},{98,... | collective-permute-start | bytes 1376264 | tf_op jit(solution)/shard_map/ppermute | solution.py:390
  47.0 33.7 %collective-permute-start.5 = (bf16[16,112,128]{2,1,0:T(8,128)(2,1)S(1)}, bf16[16,112,128]{2,1,0:T(8,128)(2,1)S(1)}, u32[]{:S(2)}, u32[]{:S(2)}) collective-permute-start(bf16[16,112,128]{2,1,0:T(8,128)(2,1)S(1)} %get-tuple-element.73.own_ref), channel_id=1, source_target_pairs={{32,0},{64,32},{0,96},{33,1},{65,33},{1,97},{34,2},{66,34},{2,98},... | collective-permute-start | bytes 1376264 | tf_op jit(solution)/shard_map/ppermute | solution.py:389
  51.1 46.0 %collective-permute-start.13 = (bf16[3,224,512]{2,1,0:T(8,128)(2,1)S(1)}, bf16[3,224,512]{2,1,0:T(8,128)(2,1)}, u32[]{:S(2)}, u32[]{:S(2)}) collective-permute-start(bf16[3,224,512]{2,1,0:T(8,128)(2,1)S(1)} %convert_element_type.662.refs_0_), channel_id=1, source_target_pairs={{0,64},{64,0},{1,65},{65,1},{2,66},{66,2},{3,67},{67,3},{4,68},{68... | collective-permute-start | bytes 2064392 | tf_op jit(solution)/shard_map/ppermute | solution.py:294
  69.4 17.3 %collective-permute-start.10 = (bf16[16,112,128]{2,1,0:T(8,128)(2,1)S(1)}, bf16[16,112,128]{2,1,0:T(8,128)(2,1)S(1)}, u32[]{:S(2)}, u32[]{:S(2)}) collective-permute-start(bf16[16,112,128]{2,1,0:T(8,128)(2,1)S(1)} %get-tuple-element.72.own_ref), channel_id=1, source_target_pairs={{32,64},{64,96},{96,0},{33,65},{65,97},{97,1},{34,66},{66,98},{98,... | collective-permute-start | bytes 1376264 | tf_op jit(solution)/shard_map/ppermute | solution.py:390
  71.3 16.6 %collective-permute-start.9 = (bf16[16,112,128]{2,1,0:T(8,128)(2,1)S(1)}, bf16[16,112,128]{2,1,0:T(8,128)(2,1)S(1)}, u32[]{:S(2)}, u32[]{:S(2)}) collective-permute-start(bf16[16,112,128]{2,1,0:T(8,128)(2,1)S(1)} %get-tuple-element.72.own_ref), channel_id=1, source_target_pairs={{32,0},{64,32},{0,96},{33,1},{65,33},{1,97},{34,2},{66,34},{2,98},... | collective-permute-start | bytes 1376264 | tf_op jit(solution)/shard_map/ppermute | solution.py:389
  80.8 23.0 %collective-permute-start.7 = (bf16[16,112,128]{2,1,0:T(8,128)(2,1)S(1)}, bf16[16,112,128]{2,1,0:T(8,128)(2,1)S(1)}, u32[]{:S(2)}, u32[]{:S(2)}) collective-permute-start(bf16[16,112,128]{2,1,0:T(8,128)(2,1)S(1)} %broadcast_select_fusion.1), channel_id=1, source_target_pairs={{96,64},{0,32},{97,65},{1,33},{98,66},{2,34},{99,67},{3,35},{100,6... | collective-permute-start | bytes 1376264 | tf_op jit(solution)/shard_map/ppermute | solution.py:392
  88.0 20.7 %collective-permute-start.11 = (bf16[16,112,128]{2,1,0:T(8,128)(2,1)S(1)}, bf16[16,112,128]{2,1,0:T(8,128)(2,1)S(1)}, u32[]{:S(2)}, u32[]{:S(2)}) collective-permute-start(bf16[16,112,128]{2,1,0:T(8,128)(2,1)S(1)} %broadcast_select_fusion), channel_id=1, source_target_pairs={{96,64},{0,32},{97,65},{1,33},{98,66},{2,34},{99,67},{3,35},{100,6... | collective-permute-start | bytes 1376264 | tf_op jit(solution)/shard_map/ppermute | solution.py:392
  96.5 17.4 %collective-permute-start.4 = (bf16[2,112,2048]{2,1,0:T(8,128)(2,1)S(1)}, bf16[2,112,2048]{2,1,0:T(8,128)(2,1)S(1)}, u32[]{:S(2)}, u32[]{:S(2)}) collective-permute-start(bf16[2,112,2048]{2,1,0:T(8,128)(2,1)S(1)} %shard_map.104.refs_0_.refs_3_), channel_id=1, source_target_pairs={{0,1},{1,0},{2,3},{3,2},{4,5},{5,4},{6,7},{7,6},{8,9},{9,8},{10,11... | collective-permute-start | bytes 2752520 | tf_op jit(solution)/shard_map/ppermute | solution.py:294
  104.7 17.1 %collective-permute-start.8 = (bf16[2,112,2048]{2,1,0:T(8,128)(2,1)S(1)}, bf16[2,112,2048]{2,1,0:T(8,128)(2,1)S(1)}, u32[]{:S(2)}, u32[]{:S(2)}) collective-permute-start(bf16[2,112,2048]{2,1,0:T(8,128)(2,1)S(1)} %shard_map.105.refs_2_.refs_0_), channel_id=1, source_target_pairs={{0,1},{1,0},{2,3},{3,2},{4,5},{5,4},{6,7},{7,6},{8,9},{9,8},{10,11... | collective-permute-start | bytes 2752520 | tf_op jit(solution)/shard_map/ppermute | solution.py:294
  144.1 25.5 %collective-permute-start.39 = (bf16[1024,256]{1,0:T(8,128)(2,1)S(1)}, bf16[1024,256]{1,0:T(8,128)(2,1)S(1)}, u32[]{:S(2)}, u32[]{:S(2)}) collective-permute-start(bf16[1024,256]{1,0:T(8,128)(2,1)S(1)} %get-tuple-element.59), channel_id=1, source_target_pairs={{0,32},{32,0},{1,33},{33,1},{2,34},{34,2},{3,35},{35,3},{4,36},{36... | collective-permute-start | bytes 1572872 | tf_op jit(solution)/shard_map/ppermute | solution.py:294
  146.1 33.2 %collective-permute-start.16 = (bf16[1024,384]{1,0:T(8,128)(2,1)S(1)}, bf16[1024,384]{1,0:T(8,128)(2,1)S(1)}, u32[]{:S(2)}, u32[]{:S(2)}) collective-permute-start(bf16[1024,384]{1,0:T(8,128)(2,1)S(1)} %get-tuple-element.45), channel_id=1, source_target_pairs={{0,8},{8,0},{16,24},{24,16},{1,9},{9,1},{17,25},{25,17},{2,10},{10... | collective-permute-start | bytes 2359304 | tf_op jit(solution)/shard_map/ppermute | solution.py:294
  146.2 37.1 %collective-permute-start.20 = (bf16[1024,384]{1,0:T(8,128)(2,1)S(1)}, bf16[1024,384]{1,0:T(8,128)(2,1)S(1)}, u32[]{:S(2)}, u32[]{:S(2)}) collective-permute-start(bf16[1024,384]{1,0:T(8,128)(2,1)S(1)} %get-tuple-element.48), channel_id=1, source_target_pairs={{0,2},{2,0},{4,6},{6,4},{1,3},{3,1},{5,7},{7,5},{8,10},{10,8},{12,... | collective-permute-start | bytes 2359304 | tf_op jit(solution)/shard_map/ppermute | solution.py:294
  148.8 35.5 %collective-permute-start.25 = (bf16[1024,384]{1,0:T(8,128)(2,1)S(1)}, bf16[1024,384]{1,0:T(8,128)(2,1)S(1)}, u32[]{:S(2)}, u32[]{:S(2)}) collective-permute-start(bf16[1024,384]{1,0:T(8,128)(2,1)S(1)} %get-tuple-element.51), channel_id=1, source_target_pairs={{0,24},{8,16},{16,8},{24,0},{1,25},{9,17},{17,9},{25,1},{2,26},{10... | collective-permute-start | bytes 2359304 | tf_op jit(solution)/shard_map/ppermute | solution.py:294
  159.0 16.9 %collective-permute-start.35 = (bf16[1,2,4,64,256]{4,3,2,1,0:T(8,128)(2,1)S(1)}, bf16[1,2,4,64,256]{4,3,2,1,0:T(8,128)(2,1)S(1)}, u32[]{:S(2)}, u32[]{:S(2)}) collective-permute-start(bf16[1,2,4,64,256]{4,3,2,1,0:T(8,128)(2,1)S(1)} %pad_maximum_fusion), channel_id=1, source_target_pairs={{0,8},{8,0},{16,24},{24,16},{1,9},{9,1},{17,25},{25,17},{2,10},{10... | collective-permute-start | bytes 786440 | tf_op jit(solution)/shard_map/ppermute | solution.py:294
  175.9 20.4 %collective-permute-start.29 = (bf16[1024,384]{1,0:T(8,128)(2,1)S(1)}, bf16[1024,384]{1,0:T(8,128)(2,1)S(1)}, u32[]{:S(2)}, u32[]{:S(2)}) collective-permute-start(bf16[1024,384]{1,0:T(8,128)(2,1)S(1)} %get-tuple-element.54), channel_id=1, source_target_pairs={{0,6},{2,4},{4,2},{6,0},{1,7},{3,5},{5,3},{7,1},{8,14},{10,12},{12... | collective-permute-start | bytes 2359304 | tf_op jit(solution)/shard_map/ppermute | solution.py:294
  178.6 18.0 %collective-permute-start.36 = (bf16[1,1,4,64,256]{4,3,2,1,0:T(8,128)(2,1)S(1)}, bf16[1,1,4,64,256]{4,3,2,1,0:T(8,128)(2,1)S(1)}, u32[]{:S(2)}, u32[]{:S(2)}) collective-permute-start(bf16[1,1,4,64,256]{4,3,2,1,0:T(8,128)(2,1)S(1)} %add_convert_fusion.7), channel_id=1, source_target_pairs={{0,24},{8,16},{16,8},{24,0},{1,25},{9,17},{17,9},{25,1},{2,26},{10... | collective-permute-start | bytes 393224 | tf_op jit(solution)/shard_map/ppermute | solution.py:294
  179.3 20.0 %collective-permute-start.41 = (bf16[1,4,1,64,256]{4,3,2,1,0:T(8,128)(2,1)S(1)}, bf16[1,4,1,64,256]{4,3,2,1,0:T(8,128)(2,1)S(1)}, u32[]{:S(2)}, u32[]{:S(2)}) collective-permute-start(bf16[1,4,1,64,256]{4,3,2,1,0:T(8,128)(2,1)S(1)} %add_convert_fusion.4), channel_id=1, source_target_pairs={{0,6},{2,4},{4,2},{6,0},{1,7},{3,5},{5,3},{7,1},{8,14},{10,12},{12... | collective-permute-start | bytes 393224 | tf_op jit(solution)/shard_map/ppermute | solution.py:294
  183.4 37.6 %collective-permute-start.17 = (bf16[1,4,2,64,384]{4,3,2,1,0:T(8,128)(2,1)S(1)}, bf16[1,4,2,64,384]{4,3,2,1,0:T(8,128)(2,1)S(1)}, u32[]{:S(2)}, u32[]{:S(2)}) collective-permute-start(bf16[1,4,2,64,384]{4,3,2,1,0:T(8,128)(2,1)S(1)} %bitcast.109), channel_id=1, source_target_pairs={{0,24},{8,16},{16,8},{24,0},{1,25},{9,17},{17,9},{25,1},{2,26},{10... | collective-permute-start | bytes 1179656 | tf_op jit(solution)/shard_map/ppermute | solution.py:294
  184.4 38.3 %collective-permute-start.21 = (bf16[1,4,2,64,384]{4,3,2,1,0:T(8,128)(2,1)S(1)}, bf16[1,4,2,64,384]{4,3,2,1,0:T(8,128)(2,1)S(1)}, u32[]{:S(2)}, u32[]{:S(2)}) collective-permute-start(bf16[1,4,2,64,384]{4,3,2,1,0:T(8,128)(2,1)S(1)} %bitcast.108), channel_id=1, source_target_pairs={{0,6},{2,4},{4,2},{6,0},{1,7},{3,5},{5,3},{7,1},{8,14},{10,12},{12... | collective-permute-start | bytes 1179656 | tf_op jit(solution)/shard_map/ppermute | solution.py:294
  196.3 26.9 %collective-permute-start.26 = (bf16[1,4,2,64,384]{4,3,2,1,0:T(8,128)(2,1)S(1)}, bf16[1,4,2,64,384]{4,3,2,1,0:T(8,128)(2,1)S(1)}, u32[]{:S(2)}, u32[]{:S(2)}) collective-permute-start(bf16[1,4,2,64,384]{4,3,2,1,0:T(8,128)(2,1)S(1)} %bitcast.107), channel_id=1, source_target_pairs={{0,8},{8,0},{16,24},{24,16},{1,9},{9,1},{17,25},{25,17},{2,10},{10... | collective-permute-start | bytes 1179656 | tf_op jit(solution)/shard_map/ppermute | solution.py:294
  196.6 29.2 %collective-permute-start.30 = (bf16[1,4,2,64,384]{4,3,2,1,0:T(8,128)(2,1)S(1)}, bf16[1,4,2,64,384]{4,3,2,1,0:T(8,128)(2,1)S(1)}, u32[]{:S(2)}, u32[]{:S(2)}) collective-permute-start(bf16[1,4,2,64,384]{4,3,2,1,0:T(8,128)(2,1)S(1)} %bitcast.106), channel_id=1, source_target_pairs={{0,2},{2,0},{4,6},{6,4},{1,3},{3,1},{5,7},{7,5},{8,10},{10,8},{12,... | collective-permute-start | bytes 1179656 | tf_op jit(solution)/shard_map/ppermute | solution.py:294
  (26 other events, 211.0 us)

commit v6 on v2

--- a/solution.py
+++ b/solution.py
@@ -11,7 +11,7 @@
 Z = ("gr", "fs_0")
 UNITS = 256
 MIB = 1024 * 1024
-LAST_VMEM = 40
+LAST_VMEM = 32
 
 
 COLORS = (
@@ -72,11 +72,17 @@
     )
 
 
-def unpack_kernel(where_ref, own_ref, down_ref, up_ref, far_ref, out_ref):
+def unpack_kernel(where_ref, *refs):
+    own_ref, out_ref = refs[0], refs[-1]
     z = where_ref[0]
     sources, half, lanes = own_ref.shape
     left = lax.broadcasted_iota(jnp.int32, (half, lanes), 1) < lanes // 2
-    pick = ((own_ref, down_ref, far_ref, up_ref), (down_ref, far_ref, up_ref, own_ref))
+    if len(refs) == 5:
+        _, below, above, far = refs[:-1]
+        pick = ((own_ref, below, far, above), (below, far, above, own_ref))
+    else:
+        _, outer, inner = refs[:-1]
+        pick = ((own_ref, inner, outer, outer), (outer, outer, inner, own_ref))
     for plane in range(4):
 
         @pl.when(z == plane)
@@ -97,7 +103,7 @@
     sources, half, lanes = pieces[0].shape
     shape = (2, half, sources * lanes)
     return call(
-        unpack_kernel, (1,), [whole(pieces[0].shape)] * 4, whole(shape),
+        unpack_kernel, (1,), [whole(pieces[0].shape)] * len(pieces), whole(shape),
         shaped(*shape), (where, *pieces), 1e9, 3e6, vmem=12,
     )
 
@@ -237,31 +243,36 @@
         at = slice(color * width, (color + 1) * width)
         product = jnp.dot(rows, down_ref[:, at], preferred_element_type=jnp.float32)
         product = product.astype(jnp.bfloat16)
-        send_ref, keep_ref = outs[2 * color : 2 * color + 2]
+        send_ref, keep_refs = outs[3 * color], outs[3 * color + 1 : 3 * color + 3]
         axis, mask = exchanges[0]
         if axis == 1:
-            kept = (yy == 0) | (yy == 4 - mask)
-            later = jnp.where((yy == 4 - mask) | (yy == 2), block, 0)
-            to = pl.ds(pl.multiple_of(later, block), block)
-
-            @pl.when(kept)
-            def _():
-                keep_ref[to, :] = product
-
-            @pl.when(jnp.logical_not(kept))
-            def _():
-                send_ref[to, :] = product
+            for at_y, ref, start in (
+                (0, keep_refs[0], 0),
+                (4 - mask, keep_refs[1], 0),
+                (mask, send_ref, 0),
+                (2, send_ref, block),
+            ):
+
+                @pl.when(yy == at_y)
+                def _():
+                    ref[start : start + block, :] = product
 
         else:
             part = block // 4
-            for xx, ref, k in ((0, keep_ref, 0), (4 - mask, keep_ref, 1), (mask, send_ref, 0), (2, send_ref, 1)):
+            for xx, ref, k in (
+                (0, keep_refs[0], 0),
+                (4 - mask, keep_refs[1], 0),
+                (mask, send_ref, 0),
+                (2, send_ref, 1),
+            ):
                 to = pl.ds(pl.multiple_of((k * ys + yy) * part, part), part)
                 ref[to, :] = product[xx * part : (xx + 1) * part]
 
 
 def last(where, normed, mix, early, sides, down):
     ys, rows, width = normed.shape
-    half = (ys * rows // 2, width // len(COLORS))
+    quarter = (ys * rows // 4, width // len(COLORS))
+    outs = [(2 * quarter[0], quarter[1]), quarter, quarter] * len(COLORS)
     at = lambda i, w: (i, 0, 0)
     side = whole(sides[0].shape)
     weight = pltpu.VMEM((UNITS, width), jnp.bfloat16)
@@ -269,7 +280,7 @@
         last_kernel, (ys,),
         [pl.BlockSpec((1, rows, width), at), pl.BlockSpec((1, rows, mix.shape[-1]), at)]
         + [pl.BlockSpec((1, rows, UNITS), at)] + [side] * 4 + [whole(down.shape)],
-        [whole(half)] * (2 * len(COLORS)), [shaped(*half)] * (2 * len(COLORS)),
+        [whole(out) for out in outs], [shaped(*out) for out in outs],
         (where, normed, mix, early, *sides, down), 14 * ys * rows * width * UNITS, 25e6,
         scratch=(weight,) * 4, vmem=LAST_VMEM,
     )
@@ -288,7 +299,7 @@
 
 
 class Sums:
-    def __init__(self, send, keep, exchanges):
+    def __init__(self, send, keeps, exchanges):
         axis, mask = exchanges[0]
         self.axes = (axis, *(a for a in (1, 2, 0) if a != axis))
         sizes = [2 if a == 0 else 4 for a in self.axes]
@@ -298,13 +309,16 @@
         self.offsets = [[0, 1, 2, 3] if a else [0, 1] for a in self.axes]
         self.offsets[0] = [0, 4 - mask] if axis else [0]
         places = [list(range(size)) for size in sizes]
-        self.terms = [(keep.reshape(shape), places), (came, [list(p) for p in places])]
+        keeps = [keep.reshape(1, *shape[1:]) for keep in keeps]
+        self.terms = [(keeps, places), (came, [list(p) for p in places])]
 
     def at(self, dim, index):
         parts = []
         for array, places in self.terms:
             for d, place in enumerate(places):
-                if d == dim:
+                if isinstance(array, list):
+                    array = array[place[index if dim == 0 else 0]]
+                elif d == dim:
                     array = lax.slice_in_dim(array, place[index], place[index] + 1, axis=d)
                 elif len(place) < array.shape[d]:
                     array = lax.slice_in_dim(array, place[0], place[0] + 1, axis=d)
@@ -348,15 +362,17 @@
     blocks = jnp.where(
         tp == 0, jnp.concatenate([own, came], axis=0), jnp.concatenate([came, own], axis=0)
     )
+    combine = mixing(route[0], route_weight[0], experts)
+    blocks, combine = lax.optimization_barrier((blocks, combine))
     mine = lax.all_to_all(blocks, PLANE, split_axis=0, concat_axis=0, tiled=True)
 
     down_own = down_master.astype(jnp.bfloat16)
     down_far = swap(down_own, "gr", 1)
-    down_own_core, down_far_core = other_core(down_own), other_core(down_far)
+    down_own_core = other_core(down_own)
+    down_far_core = other_core(down_far)
 
     _, width = tokens.shape[1:]
     places = [lax.axis_size(a) for a in FS]
-    combine = mixing(route[0], route_weight[0], experts)
     normed, mix = norm(
         where, tokens.reshape(*places, -1, width), combine.reshape(*places, -1, experts)
     )
@@ -367,24 +383,30 @@
     sides = []
     for e in range(experts):
         piece = mine[:, e]
-        below = lax.ppermute(piece, Z, [(1, 0), (2, 1), (0, 3)])
-        above = lax.ppermute(piece, Z, [(1, 2), (2, 3), (3, 0)])
-        passed = jnp.where(z == 3, below, above)
-        far = lax.ppermute(passed, Z, [(3, 2), (0, 1)])
-        own = unpack(where, (piece, below, above, far))
+        forwarded = e < experts - 1
+        outer = [(1, 0), (2, 1), (0, 3)] if forwarded else [(1, 0), (2, 3), (0, 2), (3, 1)]
+        inner = [(1, 2), (2, 3), (3, 0)] if forwarded else [(1, 2), (2, 1)]
+        pieces = [piece, lax.ppermute(piece, Z, outer)]
+        pieces.append(lax.ppermute(piece, Z, inner))
+        if forwarded:
+            passed = jnp.where(z == 3, *pieces[1:])
+            pieces.append(lax.ppermute(passed, Z, [(3, 2), (0, 1)]))
+        own = unpack(where, pieces)
         sides += [own, other_core(own)]
     early = hidden_units(where, normed, mix, sides[0], sides[1], 0)
     outs = last(where, normed, mix, early, sides[2:], down_padded.reshape(-1, width))
     sums = []
     for color, exchanges in enumerate(COLORS):
-        sums.append(Sums(outs[2 * color], outs[2 * color + 1], exchanges))
+        sums.append(Sums(outs[3 * color], outs[3 * color + 1 : 3 * color + 3], exchanges))
     for step in range(1, 4):
         for color, exchanges in zip(sums, COLORS):
             color.exchange(*exchanges[step])
-    sent = jnp.concatenate([c.block(2, 1).astype(jnp.bfloat16) for c in sums], axis=1)
-    came = swap(sent, "fs_0", 1)
-    mine = jnp.concatenate([c.block(2, 0) for c in sums], axis=1)
-    mixed = added([mine, came]).astype(jnp.bfloat16)[None]
+    columns = []
+    for pair in (sums[:2], sums[2:]):
+        sent = jnp.concatenate([c.block(2, 1).astype(jnp.bfloat16) for c in pair], axis=1)
+        came = swap(sent, "fs_0", 1)
+        columns.append(added([jnp.concatenate([c.block(2, 0) for c in pair], axis=1), came]))
+    mixed = jnp.concatenate(columns, axis=1).astype(jnp.bfloat16)[None]
     gate_t, up_t = assemble(where, sides)
     return (jnp.swapaxes(gate_t, 1, 2), jnp.swapaxes(up_t, 1, 2), down_out, mixed)
 

time: 215 us -> 204 us (0.949)
  the two profiles are of different devices: /device:TPU:66 before, /device:TPU:1 now
where the time goes in v6:
time: 204 us; the launch traced here: 202 us
  starting transfers between devices  86.5 us (42%)
  Pallas kernels  53.3 us (26%)
  waiting for transfers between devices  52.4 us (26%)
  other arithmetic  5.4 us (3%)
  local copies, waits for them, and re-layouts  2.97 us (1%)
    pallas_call x9, Pallas kernels, call(): pl.pallas_call(kernel, out_shape=out_shape, grid_spec=pltpu.PrefetchScala...  53.3 us
    ppermute x25, waiting for transfers between devices, swap(): return lax.ppermute(array, axis, [(i, i ^ mask) for i in range(peers)])  40.1 us
    ppermute x25, starting transfers between devices, swap(): return lax.ppermute(array, axis, [(i, i ^ mask) for i in range(peers)])  37.9 us
    ppermute x3, starting transfers between devices, program(): pieces = [piece, lax.ppermute(piece, Z, outer)]  20.1 us
    ppermute x2, starting transfers between devices, program(): pieces.append(lax.ppermute(passed, Z, [(3, 2), (0, 1)]))  18.3 us
    all_to_all x1, waiting for transfers between devices, program(): lax.all_to_all(blocks, PLANE, split_axis=0, concat_axis=0, tiled=True)  10.8 us
    all_to_all x1, starting transfers between devices, program(): lax.all_to_all(blocks, PLANE, split_axis=0, concat_axis=0, tiled=True)  6.87 us
  transfers between devices with their start and end apart: 34, of which 12 were waited for; matrix products, arithmetic and copies ran while one was open for 2% of the time, Pallas kernels for 14%

profile of v6, /device:TPU:1, one launch (start us, length us, event | category | flops | bytes accessed | tf_op | source)
XLA Modules:
  0.0 201.6 jit_solution(17754021037490437841)
XLA Ops:
  1.2 4.9 %shard_map.102 = (bf16[8,3,112,128]{3,2,1,0:T(8,128)(2,1)}, bf16[8,3,112,128]{3,2,1,0:T(8,128)(2,1)}) custom-call(s32[5]{0:T(128)} %stack.23.where_ref.refs_0_, f32[3,64,1792]{2,1,0:T(8,128)} %gate_ref.1, f32[3,64,1792]{2,1,0:T(8,128)} %up_ref.1, f32[1,64]{1,0:T(1,128)} %bitcast.84), custom_call_target="tpu_custom_call" | custom-call | flops 3000000000 | bytes 6000000 | tf_op jit(solution)/shard_map/pallas_call | solution.py:26
  9.5 2.6 %maximum_select_fusion = bf16[16,3,112,128]{3,2,1,0:T(8,128)(2,1)} fusion(bf16[8,3,112,128]{3,2,1,0:T(8,128)(2,1)S(1)} %collective-permute-done, bf16[8,3,112,128]{3,2,1,0:T(8,128)(2,1)} %get-tuple-element.28, pred[]{:T(512)S(6)} %eq.22), kind=kLoop, calls=%fused_computation | loop fusion | flops 2064384 | bytes 2752513 | tf_op jit(solution)/shard_map/jit(_where)/select_n | solution.py:362
  12.1 6.9 %all-to-all-start = ((bf16[16,3,112,128]{3,2,1,0:T(8,128)(2,1)}), bf16[16,3,112,128]{3,2,1,0:T(8,128)(2,1)S(1)}, u32[]{:S(2)}, u32[]{:S(2)}) async-start(bf16[16,3,112,128]{3,2,1,0:T(8,128)(2,1)} %maximum_select_fusion), calls=%async_computation | async-start | bytes 2752512 | tf_op jit(solution)/shard_map/all_to_all | solution.py:367
  20.3 9.0 %shard_map.103 = (bf16[4,512,2048]{2,1,0:T(8,128)(2,1)}, f32[4,512,3]{2,1,0:T(8,128)}) custom-call(s32[5]{0:T(128)} %stack.23.where_ref.refs_0_, bf16[2,4,4,64,2048]{4,3,2,1,0:T(8,128)(2,1)} %bitcast.83, f32[2,4,4,64,3]{4,3,2,1,0:T(8,128)} %bitcast.77), custom_call_target="tpu_custom_call" | custom-call | flops 6000000000 | bytes 17000000 | tf_op jit(solution)/shard_map/pallas_call | solution.py:26
  29.4 10.8 %all-to-all-done = bf16[16,3,112,128]{3,2,1,0:T(8,128)(2,1)S(1)} async-done(((bf16[16,3,112,128]{3,2,1,0:T(8,128)(2,1)}), bf16[16,3,112,128]{3,2,1,0:T(8,128)(2,1)S(1)}, u32[]{:S(2)}, u32[]{:S(2)}) %all-to-all-start) | async-done | bytes 1376288 | tf_op jit(solution)/shard_map/all_to_all | solution.py:367
  42.3 6.3 %collective-permute-start.1 = (bf16[16,112,128]{2,1,0:T(8,128)(2,1)}, bf16[16,112,128]{2,1,0:T(8,128)(2,1)S(1)}, u32[]{:S(2)}, u32[]{:S(2)}) collective-permute-start(bf16[16,112,128]{2,1,0:T(8,128)(2,1)} %get-tuple-element.70.refs_0_), channel_id=1, source_target_pairs={{32,0},{64,32},{0,96},{33,1},{65,33},{1,97},{34,2},{66,34},{2,98},... | collective-permute-start | bytes 1376264 | tf_op jit(solution)/shard_map/ppermute | solution.py:389
  49.9 5.2 %collective-permute-start.5 = (bf16[16,112,128]{2,1,0:T(8,128)(2,1)S(1)}, bf16[16,112,128]{2,1,0:T(8,128)(2,1)S(1)}, u32[]{:S(2)}, u32[]{:S(2)}) collective-permute-start(bf16[16,112,128]{2,1,0:T(8,128)(2,1)S(1)} %get-tuple-element.69.refs_0_), channel_id=1, source_target_pairs={{32,0},{64,32},{0,96},{33,1},{65,33},{1,97},{34,2},{66,34},{2,98},... | collective-permute-start | bytes 1376264 | tf_op jit(solution)/shard_map/ppermute | solution.py:389
  57.1 15.0 %collective-permute-start.3 = (bf16[16,112,128]{2,1,0:T(8,128)(2,1)S(1)}, bf16[16,112,128]{2,1,0:T(8,128)(2,1)S(1)}, u32[]{:S(2)}, u32[]{:S(2)}) collective-permute-start(bf16[16,112,128]{2,1,0:T(8,128)(2,1)S(1)} %broadcast_select_fusion.1), channel_id=1, source_target_pairs={{96,64},{0,32},{97,65},{1,33},{98,66},{2,34},{99,67},{3,35},{100,6... | collective-permute-start | bytes 1376264 | tf_op jit(solution)/shard_map/ppermute | solution.py:393
  72.8 8.6 %collective-permute-start.9 = (bf16[16,112,128]{2,1,0:T(8,128)(2,1)S(1)}, bf16[16,112,128]{2,1,0:T(8,128)(2,1)S(1)}, u32[]{:S(2)}, u32[]{:S(2)}) collective-permute-start(bf16[16,112,128]{2,1,0:T(8,128)(2,1)S(1)} %get-tuple-element.68.refs_0_), channel_id=1, source_target_pairs={{32,0},{64,96},{0,64},{96,32},{33,1},{65,97},{1,65},{97,33},{34,2}... | collective-permute-start | bytes 1376264 | tf_op jit(solution)/shard_map/ppermute | solution.py:389
  81.5 3.3 %collective-permute-start.7 = (bf16[16,112,128]{2,1,0:T(8,128)(2,1)S(1)}, bf16[16,112,128]{2,1,0:T(8,128)(2,1)S(1)}, u32[]{:S(2)}, u32[]{:S(2)}) collective-permute-start(bf16[16,112,128]{2,1,0:T(8,128)(2,1)S(1)} %broadcast_select_fusion), channel_id=1, source_target_pairs={{96,64},{0,32},{97,65},{1,33},{98,66},{2,34},{99,67},{3,35},{100,6... | collective-permute-start | bytes 1376264 | tf_op jit(solution)/shard_map/ppermute | solution.py:393
  86.8 11.6 %collective-permute-start.4 = (bf16[2,112,2048]{2,1,0:T(8,128)(2,1)S(1)}, bf16[2,112,2048]{2,1,0:T(8,128)(2,1)S(1)}, u32[]{:S(2)}, u32[]{:S(2)}) collective-permute-start(bf16[2,112,2048]{2,1,0:T(8,128)(2,1)S(1)} %shard_map.104.refs_0_.refs_3_), channel_id=1, source_target_pairs={{0,1},{1,0},{2,3},{3,2},{4,5},{5,4},{6,7},{7,6},{8,9},{9,8},{10,11... | collective-permute-start | bytes 2752520 | tf_op jit(solution)/shard_map/ppermute | solution.py:291
  99.8 2.6 %collective-permute-start.11 = (bf16[2,112,2048]{2,1,0:T(8,128)(2,1)S(1)}, bf16[2,112,2048]{2,1,0:T(8,128)(2,1)S(1)}, u32[]{:S(2)}, u32[]{:S(2)}) collective-permute-start(bf16[2,112,2048]{2,1,0:T(8,128)(2,1)S(1)} %shard_map.106.refs_4_.refs_2_), channel_id=1, source_target_pairs={{0,1},{1,0},{2,3},{3,2},{4,5},{5,4},{6,7},{7,6},{8,9},{9,8},{10,11... | collective-permute-start | bytes 2752520 | tf_op jit(solution)/shard_map/ppermute | solution.py:291
  103.3 4.5 %collective-permute-start.8 = (bf16[2,112,2048]{2,1,0:T(8,128)(2,1)S(1)}, bf16[2,112,2048]{2,1,0:T(8,128)(2,1)S(1)}, u32[]{:S(2)}, u32[]{:S(2)}) collective-permute-start(bf16[2,112,2048]{2,1,0:T(8,128)(2,1)S(1)} %shard_map.105.refs_2_.refs_0_), channel_id=1, source_target_pairs={{0,1},{1,0},{2,3},{3,2},{4,5},{5,4},{6,7},{7,6},{8,9},{9,8},{10,11... | collective-permute-start | bytes 2752520 | tf_op jit(solution)/shard_map/ppermute | solution.py:291
  107.8 3.9 %shard_map.108 = (bf16[3,224,2048]{2,1,0:T(8,128)(2,1)}, bf16[3,256,2048]{2,1,0:T(8,128)(2,1)S(1)}) custom-call(s32[5]{0:T(128)S(1)} %copy-done, bf16[3,224,512]{2,1,0:T(8,128)(2,1)S(1)} %convert_element_type.470.refs_0_, bf16[3,224,512]{2,1,0:T(8,128)(2,1)} %collective-permute-done.12.refs_1_, bf16[3,224,512]{2,1,0:T(8,128)(2,1)S(1)} %collective-permute-done.13.refs_2_, ...), custom_call_target="tpu_custom_call" | custom-call | flops 2000000000 | bytes 8000000 | tf_op jit(solution)/shard_map/pallas_call | solution.py:26
  111.7 7.9 %shard_map.109.early_ref = bf16[4,512,256]{2,1,0:T(8,128)(2,1)S(1)} custom-call(s32[5]{0:T(128)S(1)} %copy-done, bf16[4,512,2048]{2,1,0:T(8,128)(2,1)} %get-tuple-element.37.refs_1_.normed_ref, f32[4,512,3]{2,1,0:T(8,128)S(1)} %copy-done.1, bf16[2,112,2048]{2,1,0:T(8,128)(2,1)S(1)} %shard_map.104.refs_0_.refs_3_, ...), custom_call_target="tpu_custom_call" | custom-call | flops 4294967296 | bytes 12000000 | tf_op jit(solution)/shard_map/pallas_call | solution.py:26
  119.6 20.4 %shard_map.110 = (bf16[1024,512]{1,0:T(8,128)(2,1)S(1)}, bf16[512,512]{1,0:T(8,128)(2,1)S(1)}, bf16[512,512]{1,0:T(8,128)(2,1)S(1)}, bf16[1024,512]{1,0:T(8,128)...) custom-call(s32[5]{0:T(128)S(1)} %copy-done, ...), custom_call_target="tpu_custom_call" | custom-call | flops 15032385536 | bytes 25000000 | tf_op jit(solution)/shard_map/pallas_call | solution.py:26
  141.0 2.9 %collective-permute-start.28 = (bf16[1024,512]{1,0:T(8,128)(2,1)S(1)}, bf16[1024,512]{1,0:T(8,128)(2,1)S(1)}, u32[]{:S(2)}, u32[]{:S(2)}) collective-permute-start(bf16[1024,512]{1,0:T(8,128)(2,1)S(1)} %get-tuple-element.50), channel_id=1, source_target_pairs={{0,6},{2,4},{4,2},{6,0},{1,7},{3,5},{5,3},{7,1},{8,14},{10,12},{12... | collective-permute-start | bytes 3145736 | tf_op jit(solution)/shard_map/ppermute | solution.py:291
  143.9 3.3 %shard_map.107 = (bf16[3,224,2048]{2,1,0:T(8,128)(2,1)}, bf16[3,224,2048]{2,1,0:T(8,128)(2,1)}) custom-call(s32[5]{0:T(128)S(1)} %copy-done, bf16[2,112,2048]{2,1,0:T(8,128)(2,1)S(1)} %shard_map.104.refs_0_.refs_3_, bf16[2,112,2048]{2,1,0:T(8,128)(2,1)S(1)} %collective-permute-done.4.refs_1_.refs_4_, bf16[2,112,2048]{2,1,0:T(8,128)(2,1)S(1)} %shard_map.105.refs_2_.refs_0_, ...), custom_call_target="tpu_custom_call" | custom-call | flops 4000000000 | bytes 11000000 | tf_op jit(solution)/shard_map/pallas_call | solution.py:26
  147.3 17.6 %collective-permute-done.15 = bf16[1024,512]{1,0:T(8,128)(2,1)S(1)} collective-permute-done((bf16[1024,512]{1,0:T(8,128)(2,1)S(1)}, bf16[1024,512]{1,0:T(8,128)(2,1)S(1)}, u32[]{:S(2)}, u32[]{:S(2)}) %collective-permute-start.15) | collective-permute-done | bytes 1048608 | tf_op jit(solution)/shard_map/ppermute | solution.py:291
  168.6 10.3 %collective-permute-done.16 = bf16[1,4,2,64,512]{4,3,2,1,0:T(8,128)(2,1)S(1)} collective-permute-done((bf16[1,4,2,64,512]{4,3,2,1,0:T(8,128)(2,1)S(1)}, bf16[1,4,2,64,512]{4,3,2,1,0:T(8,128)(2,1)S(1)}, u32[]{:S(2)}, u32[]{:S(2)}) %collective-permute-start.16) | collective-permute-done | bytes 524320 | tf_op jit(solution)/shard_map/ppermute | solution.py:291
  185.3 2.8 %collective-permute-start.18 = (bf16[1,1,2,64,512]{4,3,2,1,0:T(8,128)(2,1)S(1)}, bf16[1,1,2,64,512]{4,3,2,1,0:T(8,128)(2,1)S(1)}, u32[]{:S(2)}, u32[]{:S(2)}) collective-permute-start(bf16[1,1,2,64,512]{4,3,2,1,0:T(8,128)(2,1)S(1)} %add_convert_fusion.13), channel_id=1, source_target_pairs={{0,6},{2,4},{4,2},{6,0},{1,7},{3,5},{5,3},{7,1},{8,14},{10,12},{12... | collective-permute-start | bytes 393224 | tf_op jit(solution)/shard_map/ppermute | solution.py:291
  191.2 2.4 %collective-permute-done.22 = bf16[1,1,2,64,512]{4,3,2,1,0:T(8,128)(2,1)S(1)} collective-permute-done((bf16[1,1,2,64,512]{4,3,2,1,0:T(8,128)(2,1)S(1)}, bf16[1,1,2,64,512]{4,3,2,1,0:T(8,128)(2,1)S(1)}, u32[]{:S(2)}, u32[]{:S(2)}) %collective-permute-start.22) | collective-permute-done | bytes 131104 | tf_op jit(solution)/shard_map/ppermute | solution.py:291
  193.7 2.3 %collective-permute-start.23 = (bf16[64,1024]{1,0:T(8,128)(2,1)S(1)}, bf16[64,1024]{1,0:T(8,128)(2,1)S(1)}, u32[]{:S(2)}, u32[]{:S(2)}) collective-permute-start(bf16[64,1024]{1,0:T(8,128)(2,1)S(1)} %pad_maximum_fusion.5), channel_id=1, source_target_pairs={{0,32},{32,0},{1,33},{33,1},{2,34},{34,2},{3,35},{35,3},{4,36},{36... | collective-permute-start | bytes 393224 | tf_op jit(solution)/shard_map/ppermute | solution.py:291
  198.4 2.5 %collective-permute-done.32 = bf16[64,1024]{1,0:T(8,128)(2,1)S(1)} collective-permute-done((bf16[64,1024]{1,0:T(8,128)(2,1)S(1)}, bf16[64,1024]{1,0:T(8,128)(2,1)S(1)}, u32[]{:S(2)}, u32[]{:S(2)}) %collective-permute-start.32) | collective-permute-done | bytes 131104 | tf_op jit(solution)/shard_map/ppermute | solution.py:291
  (102 shorter events, 32.9 us)
Async XLA Ops:
  12.1 28.1 %all-to-all-start = ((bf16[16,3,112,128]{3,2,1,0:T(8,128)(2,1)}), bf16[16,3,112,128]{3,2,1,0:T(8,128)(2,1)S(1)}, u32[]{:S(2)}, u32[]{:S(2)}) async-start(bf16[16,3,112,128]{3,2,1,0:T(8,128)(2,1)} %maximum_select_fusion), calls=%async_computation | async-start | bytes 2752512 | tf_op jit(solution)/shard_map/all_to_all | solution.py:367
  41.0 14.8 %collective-permute-start.2 = (bf16[16,112,128]{2,1,0:T(8,128)(2,1)}, bf16[16,112,128]{2,1,0:T(8,128)(2,1)S(1)}, u32[]{:S(2)}, u32[]{:S(2)}) collective-permute-start(bf16[16,112,128]{2,1,0:T(8,128)(2,1)} %get-tuple-element.70.refs_0_), channel_id=1, source_target_pairs={{32,64},{64,96},{96,0},{33,65},{65,97},{97,1},{34,66},{66,98},{98,... | collective-permute-start | bytes 1376264 | tf_op jit(solution)/shard_map/ppermute | solution.py:390
  42.3 14.7 %collective-permute-start.1 = (bf16[16,112,128]{2,1,0:T(8,128)(2,1)}, bf16[16,112,128]{2,1,0:T(8,128)(2,1)S(1)}, u32[]{:S(2)}, u32[]{:S(2)}) collective-permute-start(bf16[16,112,128]{2,1,0:T(8,128)(2,1)} %get-tuple-element.70.refs_0_), channel_id=1, source_target_pairs={{32,0},{64,32},{0,96},{33,1},{65,33},{1,97},{34,2},{66,34},{2,98},... | collective-permute-start | bytes 1376264 | tf_op jit(solution)/shard_map/ppermute | solution.py:389
  48.6 24.2 %collective-permute-start.6 = (bf16[16,112,128]{2,1,0:T(8,128)(2,1)S(1)}, bf16[16,112,128]{2,1,0:T(8,128)(2,1)S(1)}, u32[]{:S(2)}, u32[]{:S(2)}) collective-permute-start(bf16[16,112,128]{2,1,0:T(8,128)(2,1)S(1)} %get-tuple-element.69.refs_0_), channel_id=1, source_target_pairs={{32,64},{64,96},{96,0},{33,65},{65,97},{97,1},{34,66},{66,98},{98,... | collective-permute-start | bytes 1376264 | tf_op jit(solution)/shard_map/ppermute | solution.py:390
  49.9 31.5 %collective-permute-start.5 = (bf16[16,112,128]{2,1,0:T(8,128)(2,1)S(1)}, bf16[16,112,128]{2,1,0:T(8,128)(2,1)S(1)}, u32[]{:S(2)}, u32[]{:S(2)}) collective-permute-start(bf16[16,112,128]{2,1,0:T(8,128)(2,1)S(1)} %get-tuple-element.69.refs_0_), channel_id=1, source_target_pairs={{32,0},{64,32},{0,96},{33,1},{65,33},{1,97},{34,2},{66,34},{2,98},... | collective-permute-start | bytes 1376264 | tf_op jit(solution)/shard_map/ppermute | solution.py:389
  55.2 43.1 %collective-permute-start.12 = (bf16[3,224,512]{2,1,0:T(8,128)(2,1)S(1)}, bf16[3,224,512]{2,1,0:T(8,128)(2,1)}, u32[]{:S(2)}, u32[]{:S(2)}) collective-permute-start(bf16[3,224,512]{2,1,0:T(8,128)(2,1)S(1)} %convert_element_type.470.refs_0_), channel_id=1, source_target_pairs={{0,64},{64,0},{1,65},{65,1},{2,66},{66,2},{3,67},{67,3},{4,68},{68... | collective-permute-start | bytes 2064392 | tf_op jit(solution)/shard_map/ppermute | solution.py:291
  57.1 27.7 %collective-permute-start.3 = (bf16[16,112,128]{2,1,0:T(8,128)(2,1)S(1)}, bf16[16,112,128]{2,1,0:T(8,128)(2,1)S(1)}, u32[]{:S(2)}, u32[]{:S(2)}) collective-permute-start(bf16[16,112,128]{2,1,0:T(8,128)(2,1)S(1)} %broadcast_select_fusion.1), channel_id=1, source_target_pairs={{96,64},{0,32},{97,65},{1,33},{98,66},{2,34},{99,67},{3,35},{100,6... | collective-permute-start | bytes 1376264 | tf_op jit(solution)/shard_map/ppermute | solution.py:393
  72.1 26.3 %collective-permute-start.10 = (bf16[16,112,128]{2,1,0:T(8,128)(2,1)S(1)}, bf16[16,112,128]{2,1,0:T(8,128)(2,1)S(1)}, u32[]{:S(2)}, u32[]{:S(2)}) collective-permute-start(bf16[16,112,128]{2,1,0:T(8,128)(2,1)S(1)} %get-tuple-element.68.refs_0_), channel_id=1, source_target_pairs={{32,64},{64,32},{33,65},{65,33},{34,66},{66,34},{35,67},{67,35},{3... | collective-permute-start | bytes 1376264 | tf_op jit(solution)/shard_map/ppermute | solution.py:390
  72.8 26.0 %collective-permute-start.9 = (bf16[16,112,128]{2,1,0:T(8,128)(2,1)S(1)}, bf16[16,112,128]{2,1,0:T(8,128)(2,1)S(1)}, u32[]{:S(2)}, u32[]{:S(2)}) collective-permute-start(bf16[16,112,128]{2,1,0:T(8,128)(2,1)S(1)} %get-tuple-element.68.refs_0_), channel_id=1, source_target_pairs={{32,0},{64,96},{0,64},{96,32},{33,1},{65,97},{1,65},{97,33},{34,2}... | collective-permute-start | bytes 1376264 | tf_op jit(solution)/shard_map/ppermute | solution.py:389
  81.5 20.8 %collective-permute-start.7 = (bf16[16,112,128]{2,1,0:T(8,128)(2,1)S(1)}, bf16[16,112,128]{2,1,0:T(8,128)(2,1)S(1)}, u32[]{:S(2)}, u32[]{:S(2)}) collective-permute-start(bf16[16,112,128]{2,1,0:T(8,128)(2,1)S(1)} %broadcast_select_fusion), channel_id=1, source_target_pairs={{96,64},{0,32},{97,65},{1,33},{98,66},{2,34},{99,67},{3,35},{100,6... | collective-permute-start | bytes 1376264 | tf_op jit(solution)/shard_map/ppermute | solution.py:393
  86.8 24.9 %collective-permute-start.4 = (bf16[2,112,2048]{2,1,0:T(8,128)(2,1)S(1)}, bf16[2,112,2048]{2,1,0:T(8,128)(2,1)S(1)}, u32[]{:S(2)}, u32[]{:S(2)}) collective-permute-start(bf16[2,112,2048]{2,1,0:T(8,128)(2,1)S(1)} %shard_map.104.refs_0_.refs_3_), channel_id=1, source_target_pairs={{0,1},{1,0},{2,3},{3,2},{4,5},{5,4},{6,7},{7,6},{8,9},{9,8},{10,11... | collective-permute-start | bytes 2752520 | tf_op jit(solution)/shard_map/ppermute | solution.py:291
  98.3 9.5 %collective-permute-start.13 = (bf16[3,224,512]{2,1,0:T(8,128)(2,1)S(1)}, bf16[3,224,512]{2,1,0:T(8,128)(2,1)S(1)}, u32[]{:S(2)}, u32[]{:S(2)}) collective-permute-start(bf16[3,224,512]{2,1,0:T(8,128)(2,1)S(1)} %convert_element_type.470.refs_0_), channel_id=1, source_target_pairs={{0,1},{1,0},{2,3},{3,2},{4,5},{5,4},{6,7},{7,6},{8,9},{9,8},{10,11... | collective-permute-start | bytes 2064392 | tf_op jit(solution)/shard_map/ppermute | solution.py:291
  98.4 9.4 %collective-permute-start.14 = (bf16[3,224,512]{2,1,0:T(8,128)(2,1)}, bf16[3,224,512]{2,1,0:T(8,128)(2,1)S(1)}, u32[]{:S(2)}, u32[]{:S(2)}) collective-permute-start(bf16[3,224,512]{2,1,0:T(8,128)(2,1)} %collective-permute-done.12.refs_1_), channel_id=1, source_target_pairs={{0,1},{1,0},{2,3},{3,2},{4,5},{5,4},{6,7},{7,6},{8,9},{9,8},{10,11... | collective-permute-start | bytes 2064392 | tf_op jit(solution)/shard_map/ppermute | solution.py:291
  99.8 19.8 %collective-permute-start.11 = (bf16[2,112,2048]{2,1,0:T(8,128)(2,1)S(1)}, bf16[2,112,2048]{2,1,0:T(8,128)(2,1)S(1)}, u32[]{:S(2)}, u32[]{:S(2)}) collective-permute-start(bf16[2,112,2048]{2,1,0:T(8,128)(2,1)S(1)} %shard_map.106.refs_4_.refs_2_), channel_id=1, source_target_pairs={{0,1},{1,0},{2,3},{3,2},{4,5},{5,4},{6,7},{7,6},{8,9},{9,8},{10,11... | collective-permute-start | bytes 2752520 | tf_op jit(solution)/shard_map/ppermute | solution.py:291
  103.3 16.3 %collective-permute-start.8 = (bf16[2,112,2048]{2,1,0:T(8,128)(2,1)S(1)}, bf16[2,112,2048]{2,1,0:T(8,128)(2,1)S(1)}, u32[]{:S(2)}, u32[]{:S(2)}) collective-permute-start(bf16[2,112,2048]{2,1,0:T(8,128)(2,1)S(1)} %shard_map.105.refs_2_.refs_0_), channel_id=1, source_target_pairs={{0,1},{1,0},{2,3},{3,2},{4,5},{5,4},{6,7},{7,6},{8,9},{9,8},{10,11... | collective-permute-start | bytes 2752520 | tf_op jit(solution)/shard_map/ppermute | solution.py:291
  140.1 24.8 %collective-permute-start.15 = (bf16[1024,512]{1,0:T(8,128)(2,1)S(1)}, bf16[1024,512]{1,0:T(8,128)(2,1)S(1)}, u32[]{:S(2)}, u32[]{:S(2)}) collective-permute-start(bf16[1024,512]{1,0:T(8,128)(2,1)S(1)} %get-tuple-element.41), channel_id=1, source_target_pairs={{0,8},{8,0},{16,24},{24,16},{1,9},{9,1},{17,25},{25,17},{2,10},{10... | collective-permute-start | bytes 3145736 | tf_op jit(solution)/shard_map/ppermute | solution.py:291
  140.2 25.6 %collective-permute-start.19 = (bf16[1024,512]{1,0:T(8,128)(2,1)S(1)}, bf16[1024,512]{1,0:T(8,128)(2,1)S(1)}, u32[]{:S(2)}, u32[]{:S(2)}) collective-permute-start(bf16[1024,512]{1,0:T(8,128)(2,1)S(1)} %get-tuple-element.44), channel_id=1, source_target_pairs={{0,2},{2,0},{4,6},{6,4},{1,3},{3,1},{5,7},{7,5},{8,10},{10,8},{12,... | collective-permute-start | bytes 3145736 | tf_op jit(solution)/shard_map/ppermute | solution.py:291
  140.3 26.0 %collective-permute-start.24 = (bf16[1024,512]{1,0:T(8,128)(2,1)S(1)}, bf16[1024,512]{1,0:T(8,128)(2,1)S(1)}, u32[]{:S(2)}, u32[]{:S(2)}) collective-permute-start(bf16[1024,512]{1,0:T(8,128)(2,1)S(1)} %get-tuple-element.47), channel_id=1, source_target_pairs={{0,24},{8,16},{16,8},{24,0},{1,25},{9,17},{17,9},{25,1},{2,26},{10... | collective-permute-start | bytes 3145736 | tf_op jit(solution)/shard_map/ppermute | solution.py:291
  141.0 25.9 %collective-permute-start.28 = (bf16[1024,512]{1,0:T(8,128)(2,1)S(1)}, bf16[1024,512]{1,0:T(8,128)(2,1)S(1)}, u32[]{:S(2)}, u32[]{:S(2)}) collective-permute-start(bf16[1024,512]{1,0:T(8,128)(2,1)S(1)} %get-tuple-element.50), channel_id=1, source_target_pairs={{0,6},{2,4},{4,2},{6,0},{1,7},{3,5},{5,3},{7,1},{8,14},{10,12},{12... | collective-permute-start | bytes 3145736 | tf_op jit(solution)/shard_map/ppermute | solution.py:291
  165.0 13.9 %collective-permute-start.16 = (bf16[1,4,2,64,512]{4,3,2,1,0:T(8,128)(2,1)S(1)}, bf16[1,4,2,64,512]{4,3,2,1,0:T(8,128)(2,1)S(1)}, u32[]{:S(2)}, u32[]{:S(2)}) collective-permute-start(bf16[1,4,2,64,512]{4,3,2,1,0:T(8,128)(2,1)S(1)} %bitcast.81), channel_id=1, source_target_pairs={{0,24},{8,16},{16,8},{24,0},{1,25},{9,17},{17,9},{25,1},{2,26},{10... | collective-permute-start | bytes 1572872 | tf_op jit(solution)/shard_map/ppermute | solution.py:291
  165.9 13.6 %collective-permute-start.20 = (bf16[1,4,2,64,512]{4,3,2,1,0:T(8,128)(2,1)S(1)}, bf16[1,4,2,64,512]{4,3,2,1,0:T(8,128)(2,1)S(1)}, u32[]{:S(2)}, u32[]{:S(2)}) collective-permute-start(bf16[1,4,2,64,512]{4,3,2,1,0:T(8,128)(2,1)S(1)} %bitcast.80), channel_id=1, source_target_pairs={{0,6},{2,4},{4,2},{6,0},{1,7},{3,5},{5,3},{7,1},{8,14},{10,12},{12... | collective-permute-start | bytes 1572872 | tf_op jit(solution)/shard_map/ppermute | solution.py:291
  166.5 13.6 %collective-permute-start.25 = (bf16[1,4,2,64,512]{4,3,2,1,0:T(8,128)(2,1)S(1)}, bf16[1,4,2,64,512]{4,3,2,1,0:T(8,128)(2,1)S(1)}, u32[]{:S(2)}, u32[]{:S(2)}) collective-permute-start(bf16[1,4,2,64,512]{4,3,2,1,0:T(8,128)(2,1)S(1)} %bitcast.79), channel_id=1, source_target_pairs={{0,8},{8,0},{16,24},{24,16},{1,9},{9,1},{17,25},{25,17},{2,10},{10... | collective-permute-start | bytes 1572872 | tf_op jit(solution)/shard_map/ppermute | solution.py:291
  167.1 14.3 %collective-permute-start.29 = (bf16[1,4,2,64,512]{4,3,2,1,0:T(8,128)(2,1)S(1)}, bf16[1,4,2,64,512]{4,3,2,1,0:T(8,128)(2,1)S(1)}, u32[]{:S(2)}, u32[]{:S(2)}) collective-permute-start(bf16[1,4,2,64,512]{4,3,2,1,0:T(8,128)(2,1)S(1)} %bitcast.78), channel_id=1, source_target_pairs={{0,2},{2,0},{4,6},{6,4},{1,3},{3,1},{5,7},{7,5},{8,10},{10,8},{12,... | collective-permute-start | bytes 1572872 | tf_op jit(solution)/shard_map/ppermute | solution.py:291
  180.2 9.5 %collective-permute-start.26 = (bf16[1,2,2,64,512]{4,3,2,1,0:T(8,128)(2,1)S(1)}, bf16[1,2,2,64,512]{4,3,2,1,0:T(8,128)(2,1)S(1)}, u32[]{:S(2)}, u32[]{:S(2)}) collective-permute-start(bf16[1,2,2,64,512]{4,3,2,1,0:T(8,128)(2,1)S(1)} %pad_maximum_fusion.2), channel_id=1, source_target_pairs={{0,6},{2,4},{4,2},{6,0},{1,7},{3,5},{5,3},{7,1},{8,14},{10,12},{12... | collective-permute-start | bytes 786440 | tf_op jit(solution)/shard_map/ppermute | solution.py:291
  (15 other events, 124.6 us)

commit v7 on v6

--- a/solution.py
+++ b/solution.py
@@ -72,17 +72,11 @@
     )
 
 
-def unpack_kernel(where_ref, *refs):
-    own_ref, out_ref = refs[0], refs[-1]
+def unpack_kernel(where_ref, own_ref, down_ref, up_ref, far_ref, out_ref):
     z = where_ref[0]
     sources, half, lanes = own_ref.shape
     left = lax.broadcasted_iota(jnp.int32, (half, lanes), 1) < lanes // 2
-    if len(refs) == 5:
-        _, below, above, far = refs[:-1]
-        pick = ((own_ref, below, far, above), (below, far, above, own_ref))
-    else:
-        _, outer, inner = refs[:-1]
-        pick = ((own_ref, inner, outer, outer), (outer, outer, inner, own_ref))
+    pick = ((own_ref, down_ref, far_ref, up_ref), (down_ref, far_ref, up_ref, own_ref))
     for plane in range(4):
 
         @pl.when(z == plane)
@@ -103,7 +97,7 @@
     sources, half, lanes = pieces[0].shape
     shape = (2, half, sources * lanes)
     return call(
-        unpack_kernel, (1,), [whole(pieces[0].shape)] * len(pieces), whole(shape),
+        unpack_kernel, (1,), [whole(pieces[0].shape)] * 4, whole(shape),
         shaped(*shape), (where, *pieces), 1e9, 3e6, vmem=12,
     )
 
@@ -368,8 +362,7 @@
 
     down_own = down_master.astype(jnp.bfloat16)
     down_far = swap(down_own, "gr", 1)
-    down_own_core = other_core(down_own)
-    down_far_core = other_core(down_far)
+    down_own_core, down_far_core = other_core(down_own), other_core(down_far)
 
     _, width = tokens.shape[1:]
     places = [lax.axis_size(a) for a in FS]
@@ -383,15 +376,11 @@
     sides = []
     for e in range(experts):
         piece = mine[:, e]
-        forwarded = e < experts - 1
-        outer = [(1, 0), (2, 1), (0, 3)] if forwarded else [(1, 0), (2, 3), (0, 2), (3, 1)]
-        inner = [(1, 2), (2, 3), (3, 0)] if forwarded else [(1, 2), (2, 1)]
-        pieces = [piece, lax.ppermute(piece, Z, outer)]
-        pieces.append(lax.ppermute(piece, Z, inner))
-        if forwarded:
-            passed = jnp.where(z == 3, *pieces[1:])
-            pieces.append(lax.ppermute(passed, Z, [(3, 2), (0, 1)]))
-        own = unpack(where, pieces)
+        below = lax.ppermute(piece, Z, [(1, 0), (2, 1), (0, 3)])
+        above = lax.ppermute(piece, Z, [(1, 2), (2, 3), (3, 0)])
+        passed = jnp.where(z == 3, below, above)
+        far = lax.ppermute(passed, Z, [(3, 2), (0, 1)])
+        own = unpack(where, (piece, below, above, far))
         sides += [own, other_core(own)]
     early = hidden_units(where, normed, mix, sides[0], sides[1], 0)
     outs = last(where, normed, mix, early, sides[2:], down_padded.reshape(-1, width))

time: 204 us -> 210 us (1.029)
  waiting for transfers between devices: 52.4 us -> 57.3 us
    ppermute x8 -> x9, waiting for transfers between devices: 1.54 us -> 10.3 us  [the longest x3 9.09 us: program(): above = lax.ppermute(piece, Z, [(1, 2), (2, 3), (3, 0)])]
    ppermute x25, waiting for transfers between devices: 40.1 us -> 36.1 us  [swap(): return lax.ppermute(array, axis, [(i, i ^ mask) for i in range(peers)])]
    ppermute x8 -> x9, starting transfers between devices: 41.7 us -> 42.6 us  [the longest x3 22.1 us: program(): far = lax.ppermute(passed, Z, [(3, 2), (0, 1)])]
  transfers between devices with their start and end apart: 34 -> 35, of which waited for: 12 -> 14; matrix products, arithmetic and copies ran while one was open for 2% -> 2% of each run, Pallas kernels for 14% -> 14%
where the time goes in v7:
time: 210 us; the launch traced here: 207 us
  starting transfers between devices  86.4 us (41%)
  waiting for transfers between devices  57.3 us (27%)
  Pallas kernels  53.3 us (25%)
  other arithmetic  5.45 us (3%)
  local copies, waits for them, and re-layouts  3.05 us (1%)
    pallas_call x9, Pallas kernels, call(): pl.pallas_call(kernel, out_shape=out_shape, grid_spec=pltpu.PrefetchScala...  53.3 us
    ppermute x25, starting transfers between devices, swap(): return lax.ppermute(array, axis, [(i, i ^ mask) for i in range(peers)])  36.9 us
    ppermute x25, waiting for transfers between devices, swap(): return lax.ppermute(array, axis, [(i, i ^ mask) for i in range(peers)])  36.1 us
    ppermute x3, starting transfers between devices, program(): far = lax.ppermute(passed, Z, [(3, 2), (0, 1)])  22.1 us
    ppermute x3, starting transfers between devices, program(): below = lax.ppermute(piece, Z, [(1, 0), (2, 1), (0, 3)])  16.7 us
    all_to_all x1, waiting for transfers between devices, program(): lax.all_to_all(blocks, PLANE, split_axis=0, concat_axis=0, tiled=True)  10.8 us
    ppermute x3, waiting for transfers between devices, program(): above = lax.ppermute(piece, Z, [(1, 2), (2, 3), (3, 0)])  9.09 us
    all_to_all x1, starting transfers between devices, program(): lax.all_to_all(blocks, PLANE, split_axis=0, concat_axis=0, tiled=True)  6.87 us
  transfers between devices with their start and end apart: 35, of which 14 were waited for; matrix products, arithmetic and copies ran while one was open for 2% of the time, Pallas kernels for 14%

profile of v7, /device:TPU:1, one launch (start us, length us, event | category | flops | bytes accessed | tf_op | source)
XLA Modules:
  0.0 206.6 jit_solution(17309424229247571966)
XLA Ops:
  1.3 4.9 %shard_map.102 = (bf16[8,3,112,128]{3,2,1,0:T(8,128)(2,1)}, bf16[8,3,112,128]{3,2,1,0:T(8,128)(2,1)}) custom-call(s32[5]{0:T(128)} %stack.23.where_ref.refs_0_, f32[3,64,1792]{2,1,0:T(8,128)} %gate_ref.1, f32[3,64,1792]{2,1,0:T(8,128)} %up_ref.1, f32[1,64]{1,0:T(1,128)} %bitcast.84), custom_call_target="tpu_custom_call" | custom-call | flops 3000000000 | bytes 6000000 | tf_op jit(solution)/shard_map/pallas_call | solution.py:26
  9.6 2.6 %maximum_select_fusion = bf16[16,3,112,128]{3,2,1,0:T(8,128)(2,1)} fusion(bf16[8,3,112,128]{3,2,1,0:T(8,128)(2,1)S(1)} %collective-permute-done, bf16[8,3,112,128]{3,2,1,0:T(8,128)(2,1)} %get-tuple-element.28, pred[]{:T(512)S(6)} %eq.23), kind=kLoop, calls=%fused_computation | loop fusion | flops 2064384 | bytes 2752513 | tf_op jit(solution)/shard_map/jit(_where)/select_n | solution.py:356
  12.2 6.9 %all-to-all-start = ((bf16[16,3,112,128]{3,2,1,0:T(8,128)(2,1)}), bf16[16,3,112,128]{3,2,1,0:T(8,128)(2,1)S(1)}, u32[]{:S(2)}, u32[]{:S(2)}) async-start(bf16[16,3,112,128]{3,2,1,0:T(8,128)(2,1)} %maximum_select_fusion), calls=%async_computation | async-start | bytes 2752512 | tf_op jit(solution)/shard_map/all_to_all | solution.py:361
  20.4 9.0 %shard_map.103 = (bf16[4,512,2048]{2,1,0:T(8,128)(2,1)}, f32[4,512,3]{2,1,0:T(8,128)}) custom-call(s32[5]{0:T(128)} %stack.23.where_ref.refs_0_, bf16[2,4,4,64,2048]{4,3,2,1,0:T(8,128)(2,1)} %bitcast.83, f32[2,4,4,64,3]{4,3,2,1,0:T(8,128)} %bitcast.77), custom_call_target="tpu_custom_call" | custom-call | flops 6000000000 | bytes 17000000 | tf_op jit(solution)/shard_map/pallas_call | solution.py:26
  29.4 10.8 %all-to-all-done = bf16[16,3,112,128]{3,2,1,0:T(8,128)(2,1)S(1)} async-done(((bf16[16,3,112,128]{3,2,1,0:T(8,128)(2,1)}), bf16[16,3,112,128]{3,2,1,0:T(8,128)(2,1)S(1)}, u32[]{:S(2)}, u32[]{:S(2)}) %all-to-all-start) | async-done | bytes 1376288 | tf_op jit(solution)/shard_map/all_to_all | solution.py:361
  42.4 6.3 %collective-permute-start.1 = (bf16[16,112,128]{2,1,0:T(8,128)(2,1)}, bf16[16,112,128]{2,1,0:T(8,128)(2,1)S(1)}, u32[]{:S(2)}, u32[]{:S(2)}) collective-permute-start(bf16[16,112,128]{2,1,0:T(8,128)(2,1)} %get-tuple-element.70.own_ref), channel_id=1, source_target_pairs={{32,0},{64,32},{0,96},{33,1},{65,33},{1,97},{34,2},{66,34},{2,98},... | collective-permute-start | bytes 1376264 | tf_op jit(solution)/shard_map/ppermute | solution.py:379
  50.0 5.2 %collective-permute-start.5 = (bf16[16,112,128]{2,1,0:T(8,128)(2,1)S(1)}, bf16[16,112,128]{2,1,0:T(8,128)(2,1)S(1)}, u32[]{:S(2)}, u32[]{:S(2)}) collective-permute-start(bf16[16,112,128]{2,1,0:T(8,128)(2,1)S(1)} %get-tuple-element.69.own_ref), channel_id=1, source_target_pairs={{32,0},{64,32},{0,96},{33,1},{65,33},{1,97},{34,2},{66,34},{2,98},... | collective-permute-start | bytes 1376264 | tf_op jit(solution)/shard_map/ppermute | solution.py:379
  57.2 5.2 %collective-permute-start.9 = (bf16[16,112,128]{2,1,0:T(8,128)(2,1)S(1)}, bf16[16,112,128]{2,1,0:T(8,128)(2,1)S(1)}, u32[]{:S(2)}, u32[]{:S(2)}) collective-permute-start(bf16[16,112,128]{2,1,0:T(8,128)(2,1)S(1)} %get-tuple-element.68.own_ref), channel_id=1, source_target_pairs={{32,0},{64,32},{0,96},{33,1},{65,33},{1,97},{34,2},{66,34},{2,98},... | collective-permute-start | bytes 1376264 | tf_op jit(solution)/shard_map/ppermute | solution.py:379
  62.5 3.3 %collective-permute-done.6.up_ref = bf16[16,112,128]{2,1,0:T(8,128)(2,1)S(1)} collective-permute-done((bf16[16,112,128]{2,1,0:T(8,128)(2,1)S(1)}, bf16[16,112,128]{2,1,0:T(8,128)(2,1)S(1)}, u32[]{:S(2)}, u32[]{:S(2)}) %collective-permute-start.6) | collective-permute-done | bytes 458784 | tf_op jit(solution)/shard_map/ppermute | solution.py:380
  65.8 15.2 %collective-permute-start.3 = (bf16[16,112,128]{2,1,0:T(8,128)(2,1)S(1)}, bf16[16,112,128]{2,1,0:T(8,128)(2,1)S(1)}, u32[]{:S(2)}, u32[]{:S(2)}) collective-permute-start(bf16[16,112,128]{2,1,0:T(8,128)(2,1)S(1)} %broadcast_select_fusion.2), channel_id=1, source_target_pairs={{96,64},{0,32},{97,65},{1,33},{98,66},{2,34},{99,67},{3,35},{100,6... | collective-permute-start | bytes 1376264 | tf_op jit(solution)/shard_map/ppermute | solution.py:382
  81.0 3.8 %collective-permute-start.7 = (bf16[16,112,128]{2,1,0:T(8,128)(2,1)S(1)}, bf16[16,112,128]{2,1,0:T(8,128)(2,1)S(1)}, u32[]{:S(2)}, u32[]{:S(2)}) collective-permute-start(bf16[16,112,128]{2,1,0:T(8,128)(2,1)S(1)} %broadcast_select_fusion.1), channel_id=1, source_target_pairs={{96,64},{0,32},{97,65},{1,33},{98,66},{2,34},{99,67},{3,35},{100,6... | collective-permute-start | bytes 1376264 | tf_op jit(solution)/shard_map/ppermute | solution.py:382
  84.9 5.5 %collective-permute-done.10.up_ref = bf16[16,112,128]{2,1,0:T(8,128)(2,1)S(1)} collective-permute-done((bf16[16,112,128]{2,1,0:T(8,128)(2,1)S(1)}, bf16[16,112,128]{2,1,0:T(8,128)(2,1)S(1)}, u32[]{:S(2)}, u32[]{:S(2)}) %collective-permute-start.10) | collective-permute-done | bytes 458784 | tf_op jit(solution)/shard_map/ppermute | solution.py:380
  91.6 3.1 %collective-permute-start.11 = (bf16[16,112,128]{2,1,0:T(8,128)(2,1)S(1)}, bf16[16,112,128]{2,1,0:T(8,128)(2,1)S(1)}, u32[]{:S(2)}, u32[]{:S(2)}) collective-permute-start(bf16[16,112,128]{2,1,0:T(8,128)(2,1)S(1)} %broadcast_select_fusion), channel_id=1, source_target_pairs={{96,64},{0,32},{97,65},{1,33},{98,66},{2,34},{99,67},{3,35},{100,6... | collective-permute-start | bytes 1376264 | tf_op jit(solution)/shard_map/ppermute | solution.py:382
  96.7 3.4 %collective-permute-start.4 = (bf16[2,112,2048]{2,1,0:T(8,128)(2,1)S(1)}, bf16[2,112,2048]{2,1,0:T(8,128)(2,1)S(1)}, u32[]{:S(2)}, u32[]{:S(2)}) collective-permute-start(bf16[2,112,2048]{2,1,0:T(8,128)(2,1)S(1)} %shard_map.104.refs_0_.refs_3_), channel_id=1, source_target_pairs={{0,1},{1,0},{2,3},{3,2},{4,5},{5,4},{6,7},{7,6},{8,9},{9,8},{10,11... | collective-permute-start | bytes 2752520 | tf_op jit(solution)/shard_map/ppermute | solution.py:285
  101.5 5.8 %collective-permute-start.8 = (bf16[2,112,2048]{2,1,0:T(8,128)(2,1)S(1)}, bf16[2,112,2048]{2,1,0:T(8,128)(2,1)S(1)}, u32[]{:S(2)}, u32[]{:S(2)}) collective-permute-start(bf16[2,112,2048]{2,1,0:T(8,128)(2,1)S(1)} %shard_map.105.refs_2_.refs_0_), channel_id=1, source_target_pairs={{0,1},{1,0},{2,3},{3,2},{4,5},{5,4},{6,7},{7,6},{8,9},{9,8},{10,11... | collective-permute-start | bytes 2752520 | tf_op jit(solution)/shard_map/ppermute | solution.py:285
  108.3 4.2 %collective-permute-start.12 = (bf16[2,112,2048]{2,1,0:T(8,128)(2,1)S(1)}, bf16[2,112,2048]{2,1,0:T(8,128)(2,1)S(1)}, u32[]{:S(2)}, u32[]{:S(2)}) collective-permute-start(bf16[2,112,2048]{2,1,0:T(8,128)(2,1)S(1)} %shard_map.106.refs_4_.refs_2_), channel_id=1, source_target_pairs={{0,1},{1,0},{2,3},{3,2},{4,5},{5,4},{6,7},{7,6},{8,9},{9,8},{10,11... | collective-permute-start | bytes 2752520 | tf_op jit(solution)/shard_map/ppermute | solution.py:285
  112.5 3.9 %shard_map.108 = (bf16[3,224,2048]{2,1,0:T(8,128)(2,1)}, bf16[3,256,2048]{2,1,0:T(8,128)(2,1)S(1)}) custom-call(s32[5]{0:T(128)S(1)} %copy-done, bf16[3,224,512]{2,1,0:T(8,128)(2,1)S(1)} %convert_element_type.470.refs_0_, bf16[3,224,512]{2,1,0:T(8,128)(2,1)} %collective-permute-done.13.refs_1_, bf16[3,224,512]{2,1,0:T(8,128)(2,1)S(1)} %collective-permute-done.14.refs_2_, ...), custom_call_target="tpu_custom_call" | custom-call | flops 2000000000 | bytes 8000000 | tf_op jit(solution)/shard_map/pallas_call | solution.py:26
  116.4 7.9 %shard_map.109.early_ref = bf16[4,512,256]{2,1,0:T(8,128)(2,1)S(1)} custom-call(s32[5]{0:T(128)S(1)} %copy-done, bf16[4,512,2048]{2,1,0:T(8,128)(2,1)} %get-tuple-element.37.refs_1_.normed_ref, f32[4,512,3]{2,1,0:T(8,128)S(1)} %copy-done.1, bf16[2,112,2048]{2,1,0:T(8,128)(2,1)S(1)} %shard_map.104.refs_0_.refs_3_, ...), custom_call_target="tpu_custom_call" | custom-call | flops 4294967296 | bytes 12000000 | tf_op jit(solution)/shard_map/pallas_call | solution.py:26
  124.3 20.4 %shard_map.110 = (bf16[1024,512]{1,0:T(8,128)(2,1)S(1)}, bf16[512,512]{1,0:T(8,128)(2,1)S(1)}, bf16[512,512]{1,0:T(8,128)(2,1)S(1)}, bf16[1024,512]{1,0:T(8,128)...) custom-call(s32[5]{0:T(128)S(1)} %copy-done, ...), custom_call_target="tpu_custom_call" | custom-call | flops 15032385536 | bytes 25000000 | tf_op jit(solution)/shard_map/pallas_call | solution.py:26
  146.2 3.7 %collective-permute-start.29 = (bf16[1024,512]{1,0:T(8,128)(2,1)S(1)}, bf16[1024,512]{1,0:T(8,128)(2,1)S(1)}, u32[]{:S(2)}, u32[]{:S(2)}) collective-permute-start(bf16[1024,512]{1,0:T(8,128)(2,1)S(1)} %get-tuple-element.50), channel_id=1, source_target_pairs={{0,6},{2,4},{4,2},{6,0},{1,7},{3,5},{5,3},{7,1},{8,14},{10,12},{12... | collective-permute-start | bytes 3145736 | tf_op jit(solution)/shard_map/ppermute | solution.py:285
  149.9 3.3 %shard_map.107 = (bf16[3,224,2048]{2,1,0:T(8,128)(2,1)}, bf16[3,224,2048]{2,1,0:T(8,128)(2,1)}) custom-call(s32[5]{0:T(128)S(1)} %copy-done, bf16[2,112,2048]{2,1,0:T(8,128)(2,1)S(1)} %shard_map.104.refs_0_.refs_3_, bf16[2,112,2048]{2,1,0:T(8,128)(2,1)S(1)} %collective-permute-done.4.refs_1_.refs_4_, bf16[2,112,2048]{2,1,0:T(8,128)(2,1)S(1)} %shard_map.105.refs_2_.refs_0_, ...), custom_call_target="tpu_custom_call" | custom-call | flops 4000000000 | bytes 11000000 | tf_op jit(solution)/shard_map/pallas_call | solution.py:26
  153.2 16.4 %collective-permute-done.16 = bf16[1024,512]{1,0:T(8,128)(2,1)S(1)} collective-permute-done((bf16[1024,512]{1,0:T(8,128)(2,1)S(1)}, bf16[1024,512]{1,0:T(8,128)(2,1)S(1)}, u32[]{:S(2)}, u32[]{:S(2)}) %collective-permute-start.16) | collective-permute-done | bytes 1048608 | tf_op jit(solution)/shard_map/ppermute | solution.py:285
  174.5 9.1 %collective-permute-done.17 = bf16[1,4,2,64,512]{4,3,2,1,0:T(8,128)(2,1)S(1)} collective-permute-done((bf16[1,4,2,64,512]{4,3,2,1,0:T(8,128)(2,1)S(1)}, bf16[1,4,2,64,512]{4,3,2,1,0:T(8,128)(2,1)S(1)}, u32[]{:S(2)}, u32[]{:S(2)}) %collective-permute-start.17) | collective-permute-done | bytes 524320 | tf_op jit(solution)/shard_map/ppermute | solution.py:285
  191.0 2.7 %collective-permute-start.19 = (bf16[1,1,2,64,512]{4,3,2,1,0:T(8,128)(2,1)S(1)}, bf16[1,1,2,64,512]{4,3,2,1,0:T(8,128)(2,1)S(1)}, u32[]{:S(2)}, u32[]{:S(2)}) collective-permute-start(bf16[1,1,2,64,512]{4,3,2,1,0:T(8,128)(2,1)S(1)} %add_convert_fusion.13), channel_id=1, source_target_pairs={{0,6},{2,4},{4,2},{6,0},{1,7},{3,5},{5,3},{7,1},{8,14},{10,12},{12... | collective-permute-start | bytes 393224 | tf_op jit(solution)/shard_map/ppermute | solution.py:285
  (105 shorter events, 43.0 us)
Async XLA Ops:
  12.2 28.1 %all-to-all-start = ((bf16[16,3,112,128]{3,2,1,0:T(8,128)(2,1)}), bf16[16,3,112,128]{3,2,1,0:T(8,128)(2,1)S(1)}, u32[]{:S(2)}, u32[]{:S(2)}) async-start(bf16[16,3,112,128]{3,2,1,0:T(8,128)(2,1)} %maximum_select_fusion), calls=%async_computation | async-start | bytes 2752512 | tf_op jit(solution)/shard_map/all_to_all | solution.py:361
  41.1 14.8 %collective-permute-start.2 = (bf16[16,112,128]{2,1,0:T(8,128)(2,1)}, bf16[16,112,128]{2,1,0:T(8,128)(2,1)S(1)}, u32[]{:S(2)}, u32[]{:S(2)}) collective-permute-start(bf16[16,112,128]{2,1,0:T(8,128)(2,1)} %get-tuple-element.70.own_ref), channel_id=1, source_target_pairs={{32,64},{64,96},{96,0},{33,65},{65,97},{97,1},{34,66},{66,98},{98,... | collective-permute-start | bytes 1376264 | tf_op jit(solution)/shard_map/ppermute | solution.py:380
  42.4 14.8 %collective-permute-start.1 = (bf16[16,112,128]{2,1,0:T(8,128)(2,1)}, bf16[16,112,128]{2,1,0:T(8,128)(2,1)S(1)}, u32[]{:S(2)}, u32[]{:S(2)}) collective-permute-start(bf16[16,112,128]{2,1,0:T(8,128)(2,1)} %get-tuple-element.70.own_ref), channel_id=1, source_target_pairs={{32,0},{64,32},{0,96},{33,1},{65,33},{1,97},{34,2},{66,34},{2,98},... | collective-permute-start | bytes 1376264 | tf_op jit(solution)/shard_map/ppermute | solution.py:379
  48.7 17.1 %collective-permute-start.6 = (bf16[16,112,128]{2,1,0:T(8,128)(2,1)S(1)}, bf16[16,112,128]{2,1,0:T(8,128)(2,1)S(1)}, u32[]{:S(2)}, u32[]{:S(2)}) collective-permute-start(bf16[16,112,128]{2,1,0:T(8,128)(2,1)S(1)} %get-tuple-element.69.own_ref), channel_id=1, source_target_pairs={{32,64},{64,96},{96,0},{33,65},{65,97},{97,1},{34,66},{66,98},{98,... | collective-permute-start | bytes 1376264 | tf_op jit(solution)/shard_map/ppermute | solution.py:380
  50.0 30.9 %collective-permute-start.5 = (bf16[16,112,128]{2,1,0:T(8,128)(2,1)S(1)}, bf16[16,112,128]{2,1,0:T(8,128)(2,1)S(1)}, u32[]{:S(2)}, u32[]{:S(2)}) collective-permute-start(bf16[16,112,128]{2,1,0:T(8,128)(2,1)S(1)} %get-tuple-element.69.own_ref), channel_id=1, source_target_pairs={{32,0},{64,32},{0,96},{33,1},{65,33},{1,97},{34,2},{66,34},{2,98},... | collective-permute-start | bytes 1376264 | tf_op jit(solution)/shard_map/ppermute | solution.py:379
  55.3 44.9 %collective-permute-start.13 = (bf16[3,224,512]{2,1,0:T(8,128)(2,1)S(1)}, bf16[3,224,512]{2,1,0:T(8,128)(2,1)}, u32[]{:S(2)}, u32[]{:S(2)}) collective-permute-start(bf16[3,224,512]{2,1,0:T(8,128)(2,1)S(1)} %convert_element_type.470.refs_0_), channel_id=1, source_target_pairs={{0,64},{64,0},{1,65},{65,1},{2,66},{66,2},{3,67},{67,3},{4,68},{68... | collective-permute-start | bytes 2064392 | tf_op jit(solution)/shard_map/ppermute | solution.py:285
  55.9 34.4 %collective-permute-start.10 = (bf16[16,112,128]{2,1,0:T(8,128)(2,1)S(1)}, bf16[16,112,128]{2,1,0:T(8,128)(2,1)S(1)}, u32[]{:S(2)}, u32[]{:S(2)}) collective-permute-start(bf16[16,112,128]{2,1,0:T(8,128)(2,1)S(1)} %get-tuple-element.68.own_ref), channel_id=1, source_target_pairs={{32,64},{64,96},{96,0},{33,65},{65,97},{97,1},{34,66},{66,98},{98,... | collective-permute-start | bytes 1376264 | tf_op jit(solution)/shard_map/ppermute | solution.py:380
  57.2 34.3 %collective-permute-start.9 = (bf16[16,112,128]{2,1,0:T(8,128)(2,1)S(1)}, bf16[16,112,128]{2,1,0:T(8,128)(2,1)S(1)}, u32[]{:S(2)}, u32[]{:S(2)}) collective-permute-start(bf16[16,112,128]{2,1,0:T(8,128)(2,1)S(1)} %get-tuple-element.68.own_ref), channel_id=1, source_target_pairs={{32,0},{64,32},{0,96},{33,1},{65,33},{1,97},{34,2},{66,34},{2,98},... | collective-permute-start | bytes 1376264 | tf_op jit(solution)/shard_map/ppermute | solution.py:379
  65.8 28.9 %collective-permute-start.3 = (bf16[16,112,128]{2,1,0:T(8,128)(2,1)S(1)}, bf16[16,112,128]{2,1,0:T(8,128)(2,1)S(1)}, u32[]{:S(2)}, u32[]{:S(2)}) collective-permute-start(bf16[16,112,128]{2,1,0:T(8,128)(2,1)S(1)} %broadcast_select_fusion.2), channel_id=1, source_target_pairs={{96,64},{0,32},{97,65},{1,33},{98,66},{2,34},{99,67},{3,35},{100,6... | collective-permute-start | bytes 1376264 | tf_op jit(solution)/shard_map/ppermute | solution.py:382
  81.0 19.6 %collective-permute-start.7 = (bf16[16,112,128]{2,1,0:T(8,128)(2,1)S(1)}, bf16[16,112,128]{2,1,0:T(8,128)(2,1)S(1)}, u32[]{:S(2)}, u32[]{:S(2)}) collective-permute-start(bf16[16,112,128]{2,1,0:T(8,128)(2,1)S(1)} %broadcast_select_fusion.1), channel_id=1, source_target_pairs={{96,64},{0,32},{97,65},{1,33},{98,66},{2,34},{99,67},{3,35},{100,6... | collective-permute-start | bytes 1376264 | tf_op jit(solution)/shard_map/ppermute | solution.py:382
  91.6 15.8 %collective-permute-start.11 = (bf16[16,112,128]{2,1,0:T(8,128)(2,1)S(1)}, bf16[16,112,128]{2,1,0:T(8,128)(2,1)S(1)}, u32[]{:S(2)}, u32[]{:S(2)}) collective-permute-start(bf16[16,112,128]{2,1,0:T(8,128)(2,1)S(1)} %broadcast_select_fusion), channel_id=1, source_target_pairs={{96,64},{0,32},{97,65},{1,33},{98,66},{2,34},{99,67},{3,35},{100,6... | collective-permute-start | bytes 1376264 | tf_op jit(solution)/shard_map/ppermute | solution.py:382
  96.7 19.7 %collective-permute-start.4 = (bf16[2,112,2048]{2,1,0:T(8,128)(2,1)S(1)}, bf16[2,112,2048]{2,1,0:T(8,128)(2,1)S(1)}, u32[]{:S(2)}, u32[]{:S(2)}) collective-permute-start(bf16[2,112,2048]{2,1,0:T(8,128)(2,1)S(1)} %shard_map.104.refs_0_.refs_3_), channel_id=1, source_target_pairs={{0,1},{1,0},{2,3},{3,2},{4,5},{5,4},{6,7},{7,6},{8,9},{9,8},{10,11... | collective-permute-start | bytes 2752520 | tf_op jit(solution)/shard_map/ppermute | solution.py:285
  100.1 12.4 %collective-permute-start.14 = (bf16[3,224,512]{2,1,0:T(8,128)(2,1)S(1)}, bf16[3,224,512]{2,1,0:T(8,128)(2,1)S(1)}, u32[]{:S(2)}, u32[]{:S(2)}) collective-permute-start(bf16[3,224,512]{2,1,0:T(8,128)(2,1)S(1)} %convert_element_type.470.refs_0_), channel_id=1, source_target_pairs={{0,1},{1,0},{2,3},{3,2},{4,5},{5,4},{6,7},{7,6},{8,9},{9,8},{10,11... | collective-permute-start | bytes 2064392 | tf_op jit(solution)/shard_map/ppermute | solution.py:285
  100.2 12.3 %collective-permute-start.15 = (bf16[3,224,512]{2,1,0:T(8,128)(2,1)}, bf16[3,224,512]{2,1,0:T(8,128)(2,1)S(1)}, u32[]{:S(2)}, u32[]{:S(2)}) collective-permute-start(bf16[3,224,512]{2,1,0:T(8,128)(2,1)} %collective-permute-done.13.refs_1_), channel_id=1, source_target_pairs={{0,1},{1,0},{2,3},{3,2},{4,5},{5,4},{6,7},{7,6},{8,9},{9,8},{10,11... | collective-permute-start | bytes 2064392 | tf_op jit(solution)/shard_map/ppermute | solution.py:285
  101.5 22.8 %collective-permute-start.8 = (bf16[2,112,2048]{2,1,0:T(8,128)(2,1)S(1)}, bf16[2,112,2048]{2,1,0:T(8,128)(2,1)S(1)}, u32[]{:S(2)}, u32[]{:S(2)}) collective-permute-start(bf16[2,112,2048]{2,1,0:T(8,128)(2,1)S(1)} %shard_map.105.refs_2_.refs_0_), channel_id=1, source_target_pairs={{0,1},{1,0},{2,3},{3,2},{4,5},{5,4},{6,7},{7,6},{8,9},{9,8},{10,11... | collective-permute-start | bytes 2752520 | tf_op jit(solution)/shard_map/ppermute | solution.py:285
  108.3 16.0 %collective-permute-start.12 = (bf16[2,112,2048]{2,1,0:T(8,128)(2,1)S(1)}, bf16[2,112,2048]{2,1,0:T(8,128)(2,1)S(1)}, u32[]{:S(2)}, u32[]{:S(2)}) collective-permute-start(bf16[2,112,2048]{2,1,0:T(8,128)(2,1)S(1)} %shard_map.106.refs_4_.refs_2_), channel_id=1, source_target_pairs={{0,1},{1,0},{2,3},{3,2},{4,5},{5,4},{6,7},{7,6},{8,9},{9,8},{10,11... | collective-permute-start | bytes 2752520 | tf_op jit(solution)/shard_map/ppermute | solution.py:285
  144.8 24.8 %collective-permute-start.16 = (bf16[1024,512]{1,0:T(8,128)(2,1)S(1)}, bf16[1024,512]{1,0:T(8,128)(2,1)S(1)}, u32[]{:S(2)}, u32[]{:S(2)}) collective-permute-start(bf16[1024,512]{1,0:T(8,128)(2,1)S(1)} %get-tuple-element.41), channel_id=1, source_target_pairs={{0,8},{8,0},{16,24},{24,16},{1,9},{9,1},{17,25},{25,17},{2,10},{10... | collective-permute-start | bytes 3145736 | tf_op jit(solution)/shard_map/ppermute | solution.py:285
  144.9 25.2 %collective-permute-start.20 = (bf16[1024,512]{1,0:T(8,128)(2,1)S(1)}, bf16[1024,512]{1,0:T(8,128)(2,1)S(1)}, u32[]{:S(2)}, u32[]{:S(2)}) collective-permute-start(bf16[1024,512]{1,0:T(8,128)(2,1)S(1)} %get-tuple-element.44), channel_id=1, source_target_pairs={{0,2},{2,0},{4,6},{6,4},{1,3},{3,1},{5,7},{7,5},{8,10},{10,8},{12,... | collective-permute-start | bytes 3145736 | tf_op jit(solution)/shard_map/ppermute | solution.py:285
  145.0 27.3 %collective-permute-start.25 = (bf16[1024,512]{1,0:T(8,128)(2,1)S(1)}, bf16[1024,512]{1,0:T(8,128)(2,1)S(1)}, u32[]{:S(2)}, u32[]{:S(2)}) collective-permute-start(bf16[1024,512]{1,0:T(8,128)(2,1)S(1)} %get-tuple-element.47), channel_id=1, source_target_pairs={{0,24},{8,16},{16,8},{24,0},{1,25},{9,17},{17,9},{25,1},{2,26},{10... | collective-permute-start | bytes 3145736 | tf_op jit(solution)/shard_map/ppermute | solution.py:285
  146.2 26.6 %collective-permute-start.29 = (bf16[1024,512]{1,0:T(8,128)(2,1)S(1)}, bf16[1024,512]{1,0:T(8,128)(2,1)S(1)}, u32[]{:S(2)}, u32[]{:S(2)}) collective-permute-start(bf16[1024,512]{1,0:T(8,128)(2,1)S(1)} %get-tuple-element.50), channel_id=1, source_target_pairs={{0,6},{2,4},{4,2},{6,0},{1,7},{3,5},{5,3},{7,1},{8,14},{10,12},{12... | collective-permute-start | bytes 3145736 | tf_op jit(solution)/shard_map/ppermute | solution.py:285
  169.7 13.9 %collective-permute-start.17 = (bf16[1,4,2,64,512]{4,3,2,1,0:T(8,128)(2,1)S(1)}, bf16[1,4,2,64,512]{4,3,2,1,0:T(8,128)(2,1)S(1)}, u32[]{:S(2)}, u32[]{:S(2)}) collective-permute-start(bf16[1,4,2,64,512]{4,3,2,1,0:T(8,128)(2,1)S(1)} %bitcast.81), channel_id=1, source_target_pairs={{0,24},{8,16},{16,8},{24,0},{1,25},{9,17},{17,9},{25,1},{2,26},{10... | collective-permute-start | bytes 1572872 | tf_op jit(solution)/shard_map/ppermute | solution.py:285
  170.3 13.6 %collective-permute-start.21 = (bf16[1,4,2,64,512]{4,3,2,1,0:T(8,128)(2,1)S(1)}, bf16[1,4,2,64,512]{4,3,2,1,0:T(8,128)(2,1)S(1)}, u32[]{:S(2)}, u32[]{:S(2)}) collective-permute-start(bf16[1,4,2,64,512]{4,3,2,1,0:T(8,128)(2,1)S(1)} %bitcast.80), channel_id=1, source_target_pairs={{0,6},{2,4},{4,2},{6,0},{1,7},{3,5},{5,3},{7,1},{8,14},{10,12},{12... | collective-permute-start | bytes 1572872 | tf_op jit(solution)/shard_map/ppermute | solution.py:285
  172.4 12.4 %collective-permute-start.26 = (bf16[1,4,2,64,512]{4,3,2,1,0:T(8,128)(2,1)S(1)}, bf16[1,4,2,64,512]{4,3,2,1,0:T(8,128)(2,1)S(1)}, u32[]{:S(2)}, u32[]{:S(2)}) collective-permute-start(bf16[1,4,2,64,512]{4,3,2,1,0:T(8,128)(2,1)S(1)} %bitcast.79), channel_id=1, source_target_pairs={{0,8},{8,0},{16,24},{24,16},{1,9},{9,1},{17,25},{25,17},{2,10},{10... | collective-permute-start | bytes 1572872 | tf_op jit(solution)/shard_map/ppermute | solution.py:285
  173.0 14.3 %collective-permute-start.30 = (bf16[1,4,2,64,512]{4,3,2,1,0:T(8,128)(2,1)S(1)}, bf16[1,4,2,64,512]{4,3,2,1,0:T(8,128)(2,1)S(1)}, u32[]{:S(2)}, u32[]{:S(2)}) collective-permute-start(bf16[1,4,2,64,512]{4,3,2,1,0:T(8,128)(2,1)S(1)} %bitcast.78), channel_id=1, source_target_pairs={{0,2},{2,0},{4,6},{6,4},{1,3},{3,1},{5,7},{7,5},{8,10},{10,8},{12,... | collective-permute-start | bytes 1572872 | tf_op jit(solution)/shard_map/ppermute | solution.py:285
  (16 other events, 137.9 us)
